TPU v7x, 512 devices: a whole 4x4x16 slice. The times are simulated.
512 devices in a mesh: tp: 32 (over z, core), dp: 16 (over y, x).
Axes of the slice: x: 4, y: 4, z: 16, core: 2. Of those that a mesh axis runs over, the one named last changes fastest.
Arguments:
- incoming_embeddings: bfloat16 [96, 4096], P('tp', 'dp'), may hold values from -12 to 12
- rescale_factors: bfloat16 [2, 4096], P(None, 'dp'), may hold values from 0.099609375 to 1.8984375
- probe_lift: bfloat16 [2, 4096, 4096], P(None, 'dp', 'tp'), may hold values from -0.09375 to 0.09375
- address_lift: bfloat16 [2, 4096, 4096], P(None, 'dp', 'tp'), may hold values from -0.09375 to 0.09375
- forget_lift: bfloat16 [2, 4096, 4096], P(None, 'dp', 'tp'), may hold values from -0.09375 to 0.09375
- forget_shift: float32 [2, 4096], P(None, 'tp'), may hold values from -6 to 3
- surplus_fade: float32 [2, 96, 4096], P(None, 'dp', 'tp'), may hold values from -0.7 to 0
- content_lift: bfloat16 [2, 4096, 8192], P(None, 'dp', 'tp'), may hold values from -0.09375 to 0.09375
- filter_lift: bfloat16 [2, 4096, 8192], P(None, 'dp', 'tp'), may hold values from -0.09375 to 0.09375
- readback_lift: bfloat16 [2, 8192, 4096], P(None, 'tp', 'dp'), may hold values from -0.0625 to 0.0625
- memory_tensor: float32 [2, 96, 128, 8192], P(None, 'dp', None, 'tp'), may hold values from -6 to 6
Outputs:
- mixed: bfloat16 [96, 4096], P('tp', 'dp')
- new_state: float32 [2, 96, 128, 8192], P(None, 'dp', None, 'tp')
All inputs are finite; a program needn't handle non-finite values.
Results may differ from a plain program's by a relative error of at most 0.0085.
Values may be sent and summed in bfloat16 or wider, within the bound.
No kernel may reach another device: no remote copies, remote signals or barrier semaphores. Data moves between devices by JAX's collectives and lax.ppermute only.
A program may use at most 64 MiB of HBM per device.

v0:
```python
import math

import jax
import jax.numpy as jnp
from jax import lax
from jax.sharding import PartitionSpec as P

D = 4096
DK = 128
BLOCKS = 2


def laid_out(parts, dim):
    shape = list(parts.shape[1:])
    shape[dim] *= parts.shape[0]
    return jnp.moveaxis(parts, 0, dim).reshape(shape)


def from_everyone(shard, axis):
    length = lax.axis_size(axis)
    return lax.all_to_all(
        jnp.broadcast_to(shard[None], (length, *shard.shape)), axis, 0, 0, tiled=True
    )


def gather_directly(shard, axis, dim):
    return laid_out(from_everyone(shard, axis), dim)


def split_up(shard, dim, length):
    shape = shard.shape
    parts = shard.reshape(*shape[:dim], length, shape[dim] // length, *shape[dim + 1 :])
    return jnp.moveaxis(parts, dim, 0)


def sum_at_owner(shard, axis, dim):
    length = lax.axis_size(axis)
    parts = lax.all_to_all(split_up(shard, dim, length), axis, 0, 0, tiled=True)
    return jnp.sum(parts, axis=0)


def in_one_piece(arrays, axis, dim, along):
    widths = [math.prod(a.shape[along:]) for a in arrays]
    both = jnp.concatenate(
        [a.reshape(*a.shape[:along], w) for a, w in zip(arrays, widths)], axis=along
    )
    result = sum_at_owner(both, axis, dim)
    parts = jnp.split(result, [sum(widths[:k]) for k in range(1, len(widths))], axis=along)
    return tuple(
        (b.reshape(*result.shape[:along], *a.shape[along:]) for a, b in zip(arrays, parts))
    )


def shards(
    incoming_embeddings,
    rescale_factors,
    probe_lift,
    address_lift,
    forget_lift,
    forget_shift,
    surplus_fade,
    content_lift,
    filter_lift,
    readback_lift,
    memory_tensor,
):
    key_cols = probe_lift.shape[2]
    value_cols = content_lift.shape[2]
    seq_local = memory_tensor.shape[1]
    heads_here = key_cols // DK
    head_width = value_cols // heads_here
    stream = incoming_embeddings
    collected = []
    for layer_ordinal in range(BLOCKS):
        resid = stream.astype(jnp.float32)
        gain_cols = rescale_factors[layer_ordinal].astype(jnp.float32)
        matrices = jnp.concatenate(
            [
                probe_lift[layer_ordinal],
                address_lift[layer_ordinal],
                forget_lift[layer_ordinal],
                content_lift[layer_ordinal],
                filter_lift[layer_ordinal],
            ],
            axis=1,
        )
        all_rows = gather_directly(stream, "tp", 0)
        all_float = all_rows.astype(jnp.float32)
        hidden = (all_float * gain_cols).astype(jnp.bfloat16)
        row_squares = jnp.sum(all_float * all_float, axis=1)
        partial_terms = jnp.dot(hidden, matrices, preferred_element_type=jnp.float32)
        projected, own_squares = in_one_piece((partial_terms, row_squares), "dp", 0, 1)
        inv_rms = lax.rsqrt(own_squares / D + 1e-06)[:, None]
        projected = projected * inv_rms
        queries = projected[:, :key_cols] * DK ** (-0.5)
        key_vals = projected[:, key_cols : 2 * key_cols]
        forget_preact = projected[:, 2 * key_cols : 3 * key_cols] + forget_shift[layer_ordinal]
        values = projected[:, 3 * key_cols : 3 * key_cols + value_cols]
        gate_vals = projected[:, 3 * key_cols + value_cols :]
        forget_rate_ln = jax.nn.log_sigmoid(forget_preact) / 16.0 + surplus_fade[layer_ordinal]
        old_state = memory_tensor[layer_ordinal].reshape(seq_local, DK, heads_here, head_width)
        decays = jnp.transpose(
            jnp.exp(forget_rate_ln).reshape(seq_local, heads_here, DK), (0, 2, 1)
        )
        key_heads = key_vals.reshape(seq_local, heads_here, DK)
        value_heads = values.reshape(seq_local, heads_here, head_width)
        fresh = old_state * decays[..., None] + jnp.einsum(
            "shk,she->skhe", key_heads, value_heads, precision=lax.Precision.HIGHEST
        )
        readout = jnp.einsum(
            "shk,skhe->she",
            queries.reshape(seq_local, heads_here, DK),
            fresh,
            precision=lax.Precision.HIGHEST,
        ).reshape(seq_local, value_cols)
        gated = (readout * jax.nn.silu(gate_vals)).astype(jnp.bfloat16)
        out_block = readback_lift[layer_ordinal]
        branch_all = jnp.dot(
            gather_directly(gated, "dp", 0), out_block, preferred_element_type=jnp.float32
        )
        branch = sum_at_owner(branch_all, "tp", 0)
        stream = (resid + branch).astype(jnp.bfloat16)
        collected.append(fresh.reshape(seq_local, DK, value_cols))
    return (stream, jnp.stack(collected))


def solution(mesh):
    in_specs = (
        P("tp", "dp"),
        P(None, "dp"),
        P(None, "dp", "tp"),
        P(None, "dp", "tp"),
        P(None, "dp", "tp"),
        P(None, "tp"),
        P(None, "dp", "tp"),
        P(None, "dp", "tp"),
        P(None, "dp", "tp"),
        P(None, "tp", "dp"),
        P(None, "dp", None, "tp"),
    )
    out_specs = (P("tp", "dp"), P(None, "dp", None, "tp"))
    return jax.shard_map(shards, mesh=mesh, in_specs=in_specs, out_specs=out_specs, check_vma=False)
```

profile of v0, /device:TPU:1, one launch (start us, length us, event | category | flops | bytes accessed | tf_op | source)
XLA Modules:
  0.0 150.1 jit_solution(302525243190151597)
XLA Ops:
  0.6 0.0 copy-start.1
  0.6 0.0 copy-start.5
  0.6 1.4 broadcast_in_dim.8
  2.0 16.7 %all-to-all-start = ((bf16[32,3,256]{2,1,0:T(4,128)(2,1)}), bf16[32,3,256]{2,1,0:T(4,128)(2,1)S(1)}, u32[]{:S(2)}, u32[]{:S(2)}) async-start(bf16[32,3,256]{2,1,0:T(4,128)(2,1)} %broadcast_in_dim.8), calls=%async_computation | async-start | bytes 131072 | tf_op jit(solution)/shard_map/all_to_all | solution.py:21
  18.8 0.9 bitcast_dynamic-update-slice_fusion.6
  19.7 0.9 bitcast_dynamic-update-slice_fusion.5
  20.6 0.9 bitcast_dynamic-update-slice_fusion.4
  21.5 1.0 bitcast_dynamic-update-slice_fusion.1
  22.5 0.0 copy-done.1
  22.5 0.0 copy-done.5
  22.5 9.2 %all-to-all-done = bf16[32,3,256]{2,1,0:T(4,128)(2,1)S(1)} async-done(((bf16[32,3,256]{2,1,0:T(4,128)(2,1)}), bf16[32,3,256]{2,1,0:T(4,128)(2,1)S(1)}, u32[]{:S(2)}, u32[]{:S(2)}) %all-to-all-start) | async-done | bytes 49184 | tf_op jit(solution)/shard_map/all_to_all | solution.py:21
  31.8 0.1 multiply_reduce_fusion.1
  31.9 0.1 concatenate.19
  32.0 0.2 copy.25
  32.2 0.2 fusion.8
  32.5 0.0 copy-start.6
  32.5 0.0 copy-start.4
  32.5 0.0 copy-start
  32.5 1.0 copy.26
  33.6 6.9 %all-to-all-start.1 = ((f32[16,6,897]{2,1,0:T(8,128)}), f32[16,6,897]{2,1,0:T(8,128)S(1)}, u32[]{:S(2)}, u32[]{:S(2)}) async-start(f32[16,6,897]{2,1,0:T(8,128)} %copy.26), calls=%async_computation.1 | async-start | bytes 1048576 | tf_op jit(solution)/shard_map/all_to_all | solution.py:38
  40.5 0.0 copy-start.3
  40.5 9.9 %all-to-all-done.1 = f32[16,6,897]{2,1,0:T(8,128)S(1)} async-done(((f32[16,6,897]{2,1,0:T(8,128)}), f32[16,6,897]{2,1,0:T(8,128)S(1)}, u32[]{:S(2)}, u32[]{:S(2)}) %all-to-all-start.1) | async-done | bytes 344480 | tf_op jit(solution)/shard_map/all_to_all | solution.py:38
  50.5 0.1 fusion.45
  50.6 0.1 slice_multiply_fusion.1
  50.7 0.0 copy-done
  50.7 0.6 fusion.2
  51.4 9.3 %all_to_all.40 = bf16[16,6,256]{2,1,0:T(8,128)(2,1)S(1)} all-to-all(bf16[16,6,256]{2,1,0:T(8,128)(2,1)S(1)} %broadcast_in_dim.9), channel_id=1, replica_groups=mesh['tp'=32,'dp'=16] {'dp'}, dimensions={0} | all-to-all | bytes 98304 | tf_op jit(solution)/shard_map/all_to_all | solution.py:21
  60.8 0.1 fusion.18
  60.9 0.1 copy.29
  61.0 22.6 %all_to_all.41 = f32[32,3,256]{2,1,0:T(4,128)S(1)} all-to-all(f32[32,3,256]{2,1,0:T(4,128)S(1)} %copy.29), channel_id=1, replica_groups=mesh['tp'=32,'dp'=16] {'tp'}, dimensions={0} | all-to-all | bytes 196608 | tf_op jit(solution)/shard_map/all_to_all | solution.py:38
  83.7 17.2 %all_to_all.42 = bf16[32,3,256]{2,1,0:T(4,128)(2,1)S(1)} all-to-all(bf16[32,3,256]{2,1,0:T(4,128)(2,1)S(1)} %broadcast_in_dim.10), channel_id=1, replica_groups=mesh['tp'=32,'dp'=16] {'tp'}, dimensions={0} | all-to-all | bytes 98304 | tf_op jit(solution)/shard_map/all_to_all | solution.py:21
  100.9 0.1 multiply_reduce_fusion
  101.0 0.1 concatenate.22
  101.1 0.2 copy.31
  101.4 0.2 fusion.6
  101.6 0.2 copy.32
  101.9 12.7 %all_to_all.43 = f32[16,6,897]{2,1,0:T(8,128)S(1)} all-to-all(f32[16,6,897]{2,1,0:T(8,128)S(1)} %copy.32), channel_id=1, replica_groups=mesh['tp'=32,'dp'=16] {'dp'}, dimensions={0} | all-to-all | bytes 688896 | tf_op jit(solution)/shard_map/all_to_all | solution.py:38
  114.7 0.1 fusion.40
  114.8 0.1 slice_multiply_fusion
  114.9 0.7 fusion
  115.6 9.1 %all_to_all.44 = bf16[16,6,256]{2,1,0:T(8,128)(2,1)S(1)} all-to-all(bf16[16,6,256]{2,1,0:T(8,128)(2,1)S(1)} %broadcast_in_dim.11), channel_id=1, replica_groups=mesh['tp'=32,'dp'=16] {'dp'}, dimensions={0} | all-to-all | bytes 98304 | tf_op jit(solution)/shard_map/all_to_all | solution.py:21
  124.7 0.1 fusion.16
  124.9 0.7 copy.35
  125.6 7.6 %all-to-all-start.7 = ((f32[32,3,256]{2,1,0:T(4,128)}), f32[32,3,256]{2,1,0:T(4,128)S(1)}, u32[]{:S(2)}, u32[]{:S(2)}) async-start(f32[32,3,256]{2,1,0:T(4,128)} %copy.35), calls=%async_computation.7 | async-start | bytes 262144 | tf_op jit(solution)/shard_map/all_to_all | solution.py:38
  133.2 0.5 fusion.4
  133.7 1.2 pad_maximum_fusion
  135.0 14.5 %all-to-all-done.7 = f32[32,3,256]{2,1,0:T(4,128)S(1)} async-done(((f32[32,3,256]{2,1,0:T(4,128)}), f32[32,3,256]{2,1,0:T(4,128)S(1)}, u32[]{:S(2)}, u32[]{:S(2)}) %all-to-all-start.7) | async-done | bytes 98336 | tf_op jit(solution)/shard_map/all_to_all | solution.py:38
  149.5 0.6 add_convert_fusion
  (31 shorter events, 0.6 us)
Async XLA Ops:
  0.6 21.9 %copy-start.1 = (bf16[2,256,256]{2,1,0:T(8,128)(2,1)S(1)}, bf16[2,256,256]{2,1,0:T(8,128)(2,1)}, u32[]{:S(2)}) copy-start(bf16[2,256,256]{2,1,0:T(8,128)(2,1)} %param.19) | copy-start | bytes 786436
  0.6 21.9 %copy-start.5 = (bf16[2,256]{1,0:T(2,128)(2,1)S(1)}, bf16[2,256]{1,0:T(2,128)(2,1)}, u32[]{:S(2)}) copy-start(bf16[2,256]{1,0:T(2,128)(2,1)} %param.12) | copy-start | bytes 3076
  2.0 29.8 %all-to-all-start = ((bf16[32,3,256]{2,1,0:T(4,128)(2,1)}), bf16[32,3,256]{2,1,0:T(4,128)(2,1)S(1)}, u32[]{:S(2)}, u32[]{:S(2)}) async-start(bf16[32,3,256]{2,1,0:T(4,128)(2,1)} %broadcast_in_dim.8), calls=%async_computation | async-start | bytes 131072 | tf_op jit(solution)/shard_map/all_to_all | solution.py:21
  32.5 8.0 %copy-start.6 = (f32[2,128]{1,0:T(2,128)S(1)}, f32[2,128]{1,0:T(2,128)}, u32[]{:S(2)}) copy-start(f32[2,128]{1,0:T(2,128)} %param.16) | copy-start | bytes 3076
  32.5 8.0 %copy-start.4 = (f32[2,6,128]{2,0,1:T(2,128)S(1)}, f32[2,6,128]{2,0,1:T(2,128)}, u32[]{:S(2)}) copy-start(f32[2,6,128]{2,0,1:T(2,128)} %param.17) | copy-start | bytes 18436
  32.5 18.2 %copy-start = (f32[2,6,128,256]{3,2,1,0:T(8,128)S(1)}, f32[2,6,128,256]{3,2,1,0:T(8,128)}, u32[]{:S(2)}) copy-start(f32[2,6,128,256]{3,2,1,0:T(8,128)} %param.21) | copy-start | bytes 4718596
  33.6 27.2 %copy-start.2 = (bf16[2,256,256]{2,1,0:T(8,128)(2,1)S(1)}, bf16[2,256,256]{2,1,0:T(8,128)(2,1)}, u32[]{:S(2)}) copy-start(bf16[2,256,256]{2,1,0:T(8,128)(2,1)} %param.20) | copy-start | bytes 786436
  33.6 16.8 %all-to-all-start.1 = ((f32[16,6,897]{2,1,0:T(8,128)}), f32[16,6,897]{2,1,0:T(8,128)S(1)}, u32[]{:S(2)}, u32[]{:S(2)}) async-start(f32[16,6,897]{2,1,0:T(8,128)} %copy.26), calls=%async_computation.1 | async-start | bytes 1048576 | tf_op jit(solution)/shard_map/all_to_all | solution.py:38
  40.5 43.2 %copy-start.3 = (bf16[3,256]{1,0:T(4,128)(2,1)S(1)}, bf16[3,256]{1,0:T(4,128)(2,1)}, u32[]{:S(2)}) copy-start(bf16[3,256]{1,0:T(4,128)(2,1)} %param.11) | copy-start | bytes 4612
  125.6 23.8 %all-to-all-start.7 = ((f32[32,3,256]{2,1,0:T(4,128)}), f32[32,3,256]{2,1,0:T(4,128)S(1)}, u32[]{:S(2)}, u32[]{:S(2)}) async-start(f32[32,3,256]{2,1,0:T(4,128)} %copy.35), calls=%async_computation.7 | async-start | bytes 262144 | tf_op jit(solution)/shard_map/all_to_all | solution.py:38
where the time goes:
time: 151 us; the launch traced here: 150 us
  blocking collectives  71 us (47%)
  waiting for transfers between devices  33.6 us (22%)
  starting transfers between devices  31.2 us (21%)
  local copies, waits for them, and re-layouts  8.01 us (5%)
  other arithmetic  3.28 us (2%)
  matrix products  2.02 us (1%)
    all_to_all x3, blocking collectives, from_everyone(): lax.all_to_all(jnp.broadcast_to(shard[None], (length, *shard.shape)), axi...  35.7 us
    all_to_all x2, blocking collectives, sum_at_owner(): parts = lax.all_to_all(split_up(shard, dim, length), axis, 0, 0, tiled=True)  35.3 us
    all_to_all x2, waiting for transfers between devices, sum_at_owner(): parts = lax.all_to_all(split_up(shard, dim, length), axis, 0, 0, tiled=True)  24.3 us
    all_to_all x1, starting transfers between devices, from_everyone(): lax.all_to_all(jnp.broadcast_to(shard[None], (length, *shard.shape)), axi...  16.7 us
    all_to_all x2, starting transfers between devices, sum_at_owner(): parts = lax.all_to_all(split_up(shard, dim, length), axis, 0, 0, tiled=True)  14.5 us
    all_to_all x1, waiting for transfers between devices, from_everyone(): lax.all_to_all(jnp.broadcast_to(shard[None], (length, *shard.shape)), axi...  9.23 us
    unnamed x18, local copies, waits for them, and re-layouts  3.74 us
  transfers between devices with their start and end apart: 3, of which 3 were waited for; matrix products, arithmetic and copies ran while one was open for 4% of the time, Pallas kernels for 0%

commit v1 on v0

v1 whole, which is shorter than its diff:
```python
import jax
import jax.numpy as jnp
from jax import lax
from jax.sharding import Mesh, PartitionSpec as P

D = 4096
DK = 128
BLOCKS = 2
PAD = 8
BF = jnp.bfloat16
F32 = jnp.float32
DP = ("y", "x")
TP = ("z", "c")


def exchange(parts, axis):
    return lax.all_to_all(parts, axis, 0, 0, tiled=True)


def everyone(rows, axis):
    return exchange(jnp.broadcast_to(rows[None], (lax.axis_size(axis), *rows.shape)), axis)


def pad_rows(rows):
    return jnp.pad(rows, ((0, PAD - rows.shape[0]), (0, 0)))


def shards(
    incoming_embeddings,
    rescale_factors,
    probe_lift,
    address_lift,
    forget_lift,
    forget_shift,
    surplus_fade,
    content_lift,
    filter_lift,
    readback_lift,
    memory_tensor,
):
    kc = probe_lift.shape[2]
    vc = content_lift.shape[2]
    cols = 3 * kc + 2 * vc
    seqs = memory_tensor.shape[1]
    groups = lax.axis_size(DP)
    core = lax.axis_index("c")
    stream = pad_rows(lax.all_gather(incoming_embeddings, "c", axis=0, tiled=True))
    fresh_all = []
    for b in range(BLOCKS):
        weights = jnp.concatenate(
            [
                probe_lift[b],
                address_lift[b],
                forget_lift[b],
                content_lift[b],
                filter_lift[b],
                jnp.zeros((probe_lift.shape[1], 128), BF),
            ],
            axis=1,
        )
        rows = everyone(stream, "z").astype(F32).reshape(groups * PAD, -1)
        hidden = (rows * rescale_factors[b].astype(F32)).astype(BF)
        squares = jnp.sum(rows * rows, axis=1, keepdims=True)
        partial = jnp.dot(hidden, weights, preferred_element_type=F32)
        column = lax.broadcasted_iota(jnp.int32, partial.shape, 1)
        partial = jnp.where(column == cols, squares, partial).astype(BF)
        parts = exchange(partial.reshape(groups, PAD, -1), DP)
        total = jnp.sum(parts.astype(F32), axis=0)[:seqs]
        inv_rms = lax.rsqrt(total[:, cols : cols + 1] / D + 1e-06)
        projected = total[:, :cols] * inv_rms
        queries = projected[:, :kc] * DK ** (-0.5)
        keys = projected[:, kc : 2 * kc]
        decay_pre = projected[:, 2 * kc : 3 * kc] + forget_shift[b]
        values = projected[:, 3 * kc : 3 * kc + vc]
        gates = projected[:, 3 * kc + vc :]
        decay = jnp.exp(jax.nn.log_sigmoid(decay_pre) / 16.0 + surplus_fade[b])
        fresh = memory_tensor[b] * decay[:, :, None] + keys[:, :, None] * values[:, None, :]
        readout = jnp.sum(queries[:, :, None] * fresh, axis=1)
        gated = (readout * jax.nn.silu(gates)).astype(BF)
        fresh_all.append(fresh)
        gathered = everyone(pad_rows(gated), DP).reshape(groups * PAD, vc)
        branch = jnp.dot(gathered, readback_lift[b], preferred_element_type=F32)
        heads = exchange(branch.astype(BF).reshape(groups, PAD, -1), "z")
        own = jnp.sum(heads.astype(F32), axis=0)
        both = lax.all_gather(own, "c", axis=0)
        stream = (stream.astype(F32) + (both[0] + both[1])).astype(BF)
    third = incoming_embeddings.shape[0]
    mixed = jnp.where(core == 0, stream[:third], stream[third : 2 * third])
    return mixed, jnp.stack(fresh_all)


def solution(mesh):
    sizes = dict(mesh.shape)
    z = sizes["tp"] // 2
    y = x = 4
    fine = Mesh(mesh.devices.reshape(z, 2, y, x), ("z", "c", "y", "x"))
    in_specs = (
        P(TP, DP),
        P(None, DP),
        P(None, DP, TP),
        P(None, DP, TP),
        P(None, DP, TP),
        P(None, TP),
        P(None, DP, TP),
        P(None, DP, TP),
        P(None, DP, TP),
        P(None, TP, DP),
        P(None, DP, None, TP),
    )
    out_specs = (P(TP, DP), P(None, DP, None, TP))
    return jax.shard_map(shards, mesh=fine, in_specs=in_specs, out_specs=out_specs, check_vma=False)
```

time: 151 us -> 141 us (0.934)
  blocking collectives: 71 us -> 57 us
  waiting for transfers between devices: 33.6 us -> 43.1 us
  starting transfers between devices: 31.2 us -> 27.2 us
  local copies, waits for them, and re-layouts: 8.01 us -> 6.11 us
    all_to_all x5 -> x3, blocking collectives: 71 us -> 35.1 us  [exchange(): return lax.all_to_all(parts, axis, 0, 0, tiled=True)]
    all_gather x0 -> x3, blocking collectives: none -> 21.9 us  [the longest x2 13.3 us: shards(): both = lax.all_gather(own, 'c', axis=0)]
    all_to_all x3 -> x5, waiting for transfers between devices: 33.6 us -> 43.1 us  [exchange(): return lax.all_to_all(parts, axis, 0, 0, tiled=True)]
    all_to_all x3 -> x5, starting transfers between devices: 31.2 us -> 27.2 us  [exchange(): return lax.all_to_all(parts, axis, 0, 0, tiled=True)]
    concatenate x7 -> x2, local copies, waits for them, and re-layouts: 1.86 us -> 0.04 us  [shards(): jnp.concatenate([probe_lift[b], address_lift[b], forget_lift[b], content_...]
  transfers between devices with their start and end apart: 3 -> 5, of which waited for: 3 -> 5; matrix products, arithmetic and copies ran while one was open for 4% -> 4% of each run, Pallas kernels for 0% -> 0%
where the time goes in v1:
time: 141 us; the launch traced here: 140 us
  blocking collectives  57 us (40%)
  waiting for transfers between devices  43.1 us (31%)
  starting transfers between devices  27.2 us (19%)
  local copies, waits for them, and re-layouts  6.11 us (4%)
  other arithmetic  3.91 us (3%)
  matrix products  2.12 us (2%)
    all_to_all x5, waiting for transfers between devices, exchange(): return lax.all_to_all(parts, axis, 0, 0, tiled=True)  43.1 us
    all_to_all x3, blocking collectives, exchange(): return lax.all_to_all(parts, axis, 0, 0, tiled=True)  35.1 us
    all_to_all x5, starting transfers between devices, exchange(): return lax.all_to_all(parts, axis, 0, 0, tiled=True)  27.2 us
    all_gather x2, blocking collectives, shards(): both = lax.all_gather(own, 'c', axis=0)  13.3 us
    all_gather x1, blocking collectives, shards(): lax.all_gather(incoming_embeddings, 'c', axis=0, tiled=True)  8.6 us
    unnamed x18, local copies, waits for them, and re-layouts  3.91 us
  transfers between devices with their start and end apart: 5, of which 5 were waited for; matrix products, arithmetic and copies ran while one was open for 4% of the time, Pallas kernels for 0%

profile of v1, /device:TPU:1, one launch (start us, length us, event | category | flops | bytes accessed | tf_op | source)
XLA Modules:
  0.0 140.4 jit_solution(10114174450363275620)
XLA Ops:
  0.6 0.0 copy-start.1
  0.6 0.0 copy-start.4
  0.6 8.6 %all-gather.2 = bf16[2,3,256]{2,1,0:T(4,128)(2,1)S(1)} all-gather(bf16[1,3,256]{2,1,0:T(4,128)(2,1)} %bitcast.89), channel_id=1, replica_groups=mesh['z'=16,'c'=2,'y'=4,'x'=4] {'c'}, dimensions={0}, use_global_device_ids=true | all-gather | bytes 4608 | tf_op jit(solution)/shard_map/all_gather | solution.py:47
  9.3 0.6 broadcast_in_dim.25
  9.9 9.6 %all-to-all-start = ((bf16[16,8,256]{2,1,0:T(8,128)(2,1)}), bf16[16,8,256]{2,1,0:T(8,128)(2,1)S(1)}, u32[]{:S(2)}, u32[]{:S(2)}) async-start(bf16[16,8,256]{2,1,0:T(8,128)(2,1)} %broadcast_in_dim.25), calls=%async_computation | async-start | bytes 131072 | tf_op jit(solution)/shard_map/all_to_all | solution.py:17
  19.5 0.9 bitcast_dynamic-update-slice_fusion.9
  20.4 0.0 copy-start.5
  20.4 0.0 copy-start.3
  20.4 0.9 bitcast_dynamic-update-slice_fusion.8
  21.3 0.0 copy-start
  21.4 1.0 bitcast_dynamic-update-slice_fusion.7
  22.4 1.0 bitcast_dynamic-update-slice_fusion.3
  23.4 0.0 copy-start.2
  23.5 0.0 copy-done.4
  23.5 7.7 %all-to-all-done = bf16[16,8,256]{2,1,0:T(8,128)(2,1)S(1)} async-done(((bf16[16,8,256]{2,1,0:T(8,128)(2,1)}), bf16[16,8,256]{2,1,0:T(8,128)(2,1)S(1)}, u32[]{:S(2)}, u32[]{:S(2)}) %all-to-all-start) | async-done | bytes 65568 | tf_op jit(solution)/shard_map/all_to_all | solution.py:17
  31.2 0.1 fusion.12
  31.3 0.1 broadcast_in_dim.26
  31.4 0.9 fusion.3
  32.3 6.8 %all-to-all-start.1 = ((bf16[16,8,1024]{2,1,0:T(8,128)(2,1)}), bf16[16,8,1024]{2,1,0:T(8,128)(2,1)S(1)}, u32[]{:S(2)}, u32[]{:S(2)}) async-start(bf16[16,8,1024]{2,1,0:T(8,128)(2,1)} %fusion.3), calls=%async_computation.1 | async-start | bytes 524288 | tf_op jit(solution)/shard_map/all_to_all | solution.py:17
  39.1 0.0 copy-done.3
  39.1 7.5 %all-to-all-done.1 = bf16[16,8,1024]{2,1,0:T(8,128)(2,1)S(1)} async-done(((bf16[16,8,1024]{2,1,0:T(8,128)(2,1)}), bf16[16,8,1024]{2,1,0:T(8,128)(2,1)S(1)}, u32[]{:S(2)}, u32[]{:S(2)}) %all-to-all-start.1) | async-done | bytes 262176 | tf_op jit(solution)/shard_map/all_to_all | solution.py:17
  46.7 0.1 fusion.47
  46.8 0.1 slice_multiply_fusion.1
  46.9 0.4 fusion.11
  47.3 9.4 %all_to_all.40 = bf16[16,8,256]{2,1,0:T(8,128)(2,1)S(1)} all-to-all(bf16[16,8,256]{2,1,0:T(8,128)(2,1)S(1)} %broadcast_in_dim.28), channel_id=1, replica_groups=mesh['z'=16,'c'=2,'y'=4,'x'=4] {'y','x'}, dimensions={0} | all-to-all | bytes 131072 | tf_op jit(solution)/shard_map/all_to_all | solution.py:17
  56.8 0.2 fusion.4
  56.9 15.1 %all_to_all.41 = bf16[16,8,256]{2,1,0:T(8,128)(2,1)S(1)} all-to-all(bf16[16,8,256]{2,1,0:T(8,128)(2,1)S(1)} %fusion.4), channel_id=1, replica_groups=mesh['z'=16,'c'=2,'y'=4,'x'=4] {'z'}, dimensions={0} | all-to-all | bytes 131072 | tf_op jit(solution)/shard_map/all_to_all | solution.py:17
  72.1 6.5 %all-gather = f32[16,256]{1,0:T(8,128)S(1)} all-gather(f32[8,256]{1,0:T(8,128)S(1)} %convert_reduce_fusion.3), channel_id=2, replica_groups=mesh['z'=16,'c'=2,'y'=4,'x'=4] {'c'}, dimensions={0}, use_global_device_ids=true | all-gather | bytes 24576 | tf_op jit(solution)/shard_map/all_gather | solution.py:85
  78.6 0.6 broadcast_in_dim.29
  79.3 3.5 %all-to-all-start.4 = ((bf16[16,8,256]{2,1,0:T(8,128)(2,1)}), bf16[16,8,256]{2,1,0:T(8,128)(2,1)S(1)}, u32[]{:S(2)}, u32[]{:S(2)}) async-start(bf16[16,8,256]{2,1,0:T(8,128)(2,1)} %broadcast_in_dim.29), calls=%async_computation.4 | async-start | bytes 131072 | tf_op jit(solution)/shard_map/all_to_all | solution.py:17
  82.8 11.7 %all-to-all-done.4 = bf16[16,8,256]{2,1,0:T(8,128)(2,1)S(1)} async-done(((bf16[16,8,256]{2,1,0:T(8,128)(2,1)}), bf16[16,8,256]{2,1,0:T(8,128)(2,1)S(1)}, u32[]{:S(2)}, u32[]{:S(2)}) %all-to-all-start.4) | async-done | bytes 65568 | tf_op jit(solution)/shard_map/all_to_all | solution.py:17
  94.5 0.1 fusion.15
  94.6 0.1 broadcast_in_dim.30
  94.7 0.2 fusion.2
  95.0 10.5 %all_to_all.42 = bf16[16,8,1024]{2,1,0:T(8,128)(2,1)S(1)} all-to-all(bf16[16,8,1024]{2,1,0:T(8,128)(2,1)S(1)} %fusion.2), channel_id=1, replica_groups=mesh['z'=16,'c'=2,'y'=4,'x'=4] {'y','x'}, dimensions={0} | all-to-all | bytes 524288 | tf_op jit(solution)/shard_map/all_to_all | solution.py:17
  105.5 0.1 fusion.43
  105.6 0.1 slice_multiply_fusion
  105.7 0.4 fusion.8
  106.1 0.6 broadcast_in_dim.32
  106.8 3.5 %all-to-all-start.6 = ((bf16[16,8,256]{2,1,0:T(8,128)(2,1)}), bf16[16,8,256]{2,1,0:T(8,128)(2,1)S(1)}, u32[]{:S(2)}, u32[]{:S(2)}) async-start(bf16[16,8,256]{2,1,0:T(8,128)(2,1)} %broadcast_in_dim.32), calls=%async_computation.6 | async-start | bytes 131072 | tf_op jit(solution)/shard_map/all_to_all | solution.py:17
  110.3 6.4 %all-to-all-done.6 = bf16[16,8,256]{2,1,0:T(8,128)(2,1)S(1)} async-done(((bf16[16,8,256]{2,1,0:T(8,128)(2,1)}), bf16[16,8,256]{2,1,0:T(8,128)(2,1)S(1)}, u32[]{:S(2)}, u32[]{:S(2)}) %all-to-all-start.6) | async-done | bytes 65568 | tf_op jit(solution)/shard_map/all_to_all | solution.py:17
  116.7 0.8 fusion.5
  117.5 3.9 %all-to-all-start.7 = ((bf16[16,8,256]{2,1,0:T(8,128)(2,1)}), bf16[16,8,256]{2,1,0:T(8,128)(2,1)S(1)}, u32[]{:S(2)}, u32[]{:S(2)}) async-start(bf16[16,8,256]{2,1,0:T(8,128)(2,1)} %fusion.5), calls=%async_computation.7 | async-start | bytes 131072 | tf_op jit(solution)/shard_map/all_to_all | solution.py:17
  121.4 0.5 multiply_add_fusion.1
  121.9 1.2 pad_maximum_fusion
  123.2 9.8 %all-to-all-done.7 = bf16[16,8,256]{2,1,0:T(8,128)(2,1)S(1)} async-done(((bf16[16,8,256]{2,1,0:T(8,128)(2,1)}), bf16[16,8,256]{2,1,0:T(8,128)(2,1)S(1)}, u32[]{:S(2)}, u32[]{:S(2)}) %all-to-all-start.7) | async-done | bytes 65568 | tf_op jit(solution)/shard_map/all_to_all | solution.py:17
  133.0 6.8 %all-gather.1 = f32[16,256]{1,0:T(8,128)S(1)} all-gather(f32[8,256]{1,0:T(8,128)S(1)} %convert_reduce_fusion.2), channel_id=3, replica_groups=mesh['z'=16,'c'=2,'y'=4,'x'=4] {'c'}, dimensions={0}, use_global_device_ids=true | all-gather | bytes 24576 | tf_op jit(solution)/shard_map/all_gather | solution.py:85
  139.8 0.6 slice_select_fusion
  (28 shorter events, 0.3 us)
Async XLA Ops:
  0.6 22.8 %copy-start.1 = (bf16[2,256,256]{2,1,0:T(8,128)(2,1)S(1)}, bf16[2,256,256]{2,1,0:T(8,128)(2,1)}, u32[]{:S(2)}) copy-start(bf16[2,256,256]{2,1,0:T(8,128)(2,1)} %param.19) | copy-start | bytes 786436
  0.6 22.9 %copy-start.4 = (bf16[2,256]{1,0:T(2,128)(2,1)S(1)}, bf16[2,256]{1,0:T(2,128)(2,1)}, u32[]{:S(2)}) copy-start(bf16[2,256]{1,0:T(2,128)(2,1)} %param.12) | copy-start | bytes 3076
  9.9 21.3 %all-to-all-start = ((bf16[16,8,256]{2,1,0:T(8,128)(2,1)}), bf16[16,8,256]{2,1,0:T(8,128)(2,1)S(1)}, u32[]{:S(2)}, u32[]{:S(2)}) async-start(bf16[16,8,256]{2,1,0:T(8,128)(2,1)} %broadcast_in_dim.25), calls=%async_computation | async-start | bytes 131072 | tf_op jit(solution)/shard_map/all_to_all | solution.py:17
  20.4 18.7 %copy-start.5 = (f32[2,128]{1,0:T(2,128)S(1)}, f32[2,128]{1,0:T(2,128)}, u32[]{:S(2)}) copy-start(f32[2,128]{1,0:T(2,128)} %param.16) | copy-start | bytes 3076
  20.4 18.7 %copy-start.3 = (f32[2,6,128]{2,0,1:T(2,128)S(1)}, f32[2,6,128]{2,0,1:T(2,128)}, u32[]{:S(2)}) copy-start(f32[2,6,128]{2,0,1:T(2,128)} %param.17) | copy-start | bytes 18436
  21.3 25.5 %copy-start = (f32[2,6,128,256]{3,2,1,0:T(8,128)S(1)}, f32[2,6,128,256]{3,2,1,0:T(8,128)}, u32[]{:S(2)}) copy-start(f32[2,6,128,256]{3,2,1,0:T(8,128)} %param.21) | copy-start | bytes 4718596
  23.4 33.3 %copy-start.2 = (bf16[2,256,256]{2,1,0:T(8,128)(2,1)S(1)}, bf16[2,256,256]{2,1,0:T(8,128)(2,1)}, u32[]{:S(2)}) copy-start(bf16[2,256,256]{2,1,0:T(8,128)(2,1)} %param.20) | copy-start | bytes 786436
  32.3 14.3 %all-to-all-start.1 = ((bf16[16,8,1024]{2,1,0:T(8,128)(2,1)}), bf16[16,8,1024]{2,1,0:T(8,128)(2,1)S(1)}, u32[]{:S(2)}, u32[]{:S(2)}) async-start(bf16[16,8,1024]{2,1,0:T(8,128)(2,1)} %fusion.3), calls=%async_computation.1 | async-start | bytes 524288 | tf_op jit(solution)/shard_map/all_to_all | solution.py:17
  79.3 15.2 %all-to-all-start.4 = ((bf16[16,8,256]{2,1,0:T(8,128)(2,1)}), bf16[16,8,256]{2,1,0:T(8,128)(2,1)S(1)}, u32[]{:S(2)}, u32[]{:S(2)}) async-start(bf16[16,8,256]{2,1,0:T(8,128)(2,1)} %broadcast_in_dim.29), calls=%async_computation.4 | async-start | bytes 131072 | tf_op jit(solution)/shard_map/all_to_all | solution.py:17
  106.8 10.0 %all-to-all-start.6 = ((bf16[16,8,256]{2,1,0:T(8,128)(2,1)}), bf16[16,8,256]{2,1,0:T(8,128)(2,1)S(1)}, u32[]{:S(2)}, u32[]{:S(2)}) async-start(bf16[16,8,256]{2,1,0:T(8,128)(2,1)} %broadcast_in_dim.32), calls=%async_computation.6 | async-start | bytes 131072 | tf_op jit(solution)/shard_map/all_to_all | solution.py:17
  117.5 15.5 %all-to-all-start.7 = ((bf16[16,8,256]{2,1,0:T(8,128)(2,1)}), bf16[16,8,256]{2,1,0:T(8,128)(2,1)S(1)}, u32[]{:S(2)}, u32[]{:S(2)}) async-start(bf16[16,8,256]{2,1,0:T(8,128)(2,1)} %fusion.5), calls=%async_computation.7 | async-start | bytes 131072 | tf_op jit(solution)/shard_map/all_to_all | solution.py:17

commit v2 on v1

--- a/solution.py
+++ b/solution.py
@@ -46,20 +46,34 @@
     core = lax.axis_index("c")
     stream = pad_rows(lax.all_gather(incoming_embeddings, "c", axis=0, tiled=True))
     fresh_all = []
+    ready = [
+        (
+            jnp.concatenate(
+                [
+                    probe_lift[b],
+                    address_lift[b],
+                    forget_lift[b],
+                    content_lift[b],
+                    filter_lift[b],
+                    jnp.zeros((probe_lift.shape[1], 128), BF),
+                ],
+                axis=1,
+            ),
+            rescale_factors[b].astype(F32),
+            forget_shift[b],
+            surplus_fade[b],
+            readback_lift[b],
+            memory_tensor[b],
+        )
+        for b in range(BLOCKS)
+    ]
     for b in range(BLOCKS):
-        weights = jnp.concatenate(
-            [
-                probe_lift[b],
-                address_lift[b],
-                forget_lift[b],
-                content_lift[b],
-                filter_lift[b],
-                jnp.zeros((probe_lift.shape[1], 128), BF),
-            ],
-            axis=1,
-        )
-        rows = everyone(stream, "z").astype(F32).reshape(groups * PAD, -1)
-        hidden = (rows * rescale_factors[b].astype(F32)).astype(BF)
+        rows = everyone(stream, "z")
+        if b == 0:
+            rows, ready, core = lax.optimization_barrier((rows, ready, core))
+        weights, gain, shift, fade, back, memory = ready[b]
+        rows = rows.astype(F32).reshape(groups * PAD, -1)
+        hidden = (rows * gain).astype(BF)
         squares = jnp.sum(rows * rows, axis=1, keepdims=True)
         partial = jnp.dot(hidden, weights, preferred_element_type=F32)
         column = lax.broadcasted_iota(jnp.int32, partial.shape, 1)
@@ -70,16 +84,16 @@
         projected = total[:, :cols] * inv_rms
         queries = projected[:, :kc] * DK ** (-0.5)
         keys = projected[:, kc : 2 * kc]
-        decay_pre = projected[:, 2 * kc : 3 * kc] + forget_shift[b]
+        decay_pre = projected[:, 2 * kc : 3 * kc] + shift
         values = projected[:, 3 * kc : 3 * kc + vc]
         gates = projected[:, 3 * kc + vc :]
-        decay = jnp.exp(jax.nn.log_sigmoid(decay_pre) / 16.0 + surplus_fade[b])
-        fresh = memory_tensor[b] * decay[:, :, None] + keys[:, :, None] * values[:, None, :]
+        decay = jnp.exp(jax.nn.log_sigmoid(decay_pre) / 16.0 + fade)
+        fresh = memory * decay[:, :, None] + keys[:, :, None] * values[:, None, :]
         readout = jnp.sum(queries[:, :, None] * fresh, axis=1)
         gated = (readout * jax.nn.silu(gates)).astype(BF)
         fresh_all.append(fresh)
         gathered = everyone(pad_rows(gated), DP).reshape(groups * PAD, vc)
-        branch = jnp.dot(gathered, readback_lift[b], preferred_element_type=F32)
+        branch = jnp.dot(gathered, back, preferred_element_type=F32)
         heads = exchange(branch.astype(BF).reshape(groups, PAD, -1), "z")
         own = jnp.sum(heads.astype(F32), axis=0)
         both = lax.all_gather(own, "c", axis=0)

time: 141 us -> 139 us (0.986)
  blocking collectives: 57 us -> 96.4 us
  waiting for transfers between devices: 43.1 us -> 16.1 us
  starting transfers between devices: 27.2 us -> 13.4 us
    all_to_all x3 -> x6, blocking collectives: 35.1 us -> 74.5 us  [exchange(): return lax.all_to_all(parts, axis, 0, 0, tiled=True)]
    all_to_all x5 -> x2, waiting for transfers between devices: 43.1 us -> 16.1 us  [exchange(): return lax.all_to_all(parts, axis, 0, 0, tiled=True)]
    all_to_all x5 -> x2, starting transfers between devices: 27.2 us -> 13.4 us  [exchange(): return lax.all_to_all(parts, axis, 0, 0, tiled=True)]
    squeeze x0 -> x4, local copies, waits for them, and re-layouts: none -> 2.39 us  [the longest x1 1.62 us: shards(): memory_tensor[b]]
    unnamed x18 -> x16, local copies, waits for them, and re-layouts: 3.91 us -> 1.74 us
  transfers between devices with their start and end apart: 5 -> 2, of which waited for: 5 -> 2; matrix products, arithmetic and copies ran while one was open for 4% -> 5% of each run, Pallas kernels for 0% -> 0%
where the time goes in v2:
time: 139 us; the launch traced here: 138 us
  blocking collectives  96.4 us (69%)
  waiting for transfers between devices  16.1 us (12%)
  starting transfers between devices  13.4 us (10%)
  local copies, waits for them, and re-layouts  5.84 us (4%)
  other arithmetic  4.28 us (3%)
  matrix products  1.42 us (1%)
    all_to_all x6, blocking collectives, exchange(): return lax.all_to_all(parts, axis, 0, 0, tiled=True)  74.5 us
    all_to_all x2, waiting for transfers between devices, exchange(): return lax.all_to_all(parts, axis, 0, 0, tiled=True)  16.1 us
    all_to_all x2, starting transfers between devices, exchange(): return lax.all_to_all(parts, axis, 0, 0, tiled=True)  13.4 us
    all_gather x2, blocking collectives, shards(): both = lax.all_gather(own, 'c', axis=0)  13.4 us
    all_gather x1, blocking collectives, shards(): lax.all_gather(incoming_embeddings, 'c', axis=0, tiled=True)  8.47 us
  transfers between devices with their start and end apart: 2, of which 2 were waited for; matrix products, arithmetic and copies ran while one was open for 5% of the time, Pallas kernels for 0%

profile of v2, /device:TPU:1, one launch (start us, length us, event | category | flops | bytes accessed | tf_op | source)
XLA Modules:
  0.0 138.3 jit_solution(3403613759328198439)
XLA Ops:
  0.6 8.5 %all-gather.2 = bf16[2,3,256]{2,1,0:T(4,128)(2,1)S(1)} all-gather(bf16[1,3,256]{2,1,0:T(4,128)(2,1)} %bitcast.77), channel_id=1, replica_groups=mesh['z'=16,'c'=2,'y'=4,'x'=4] {'c'}, dimensions={0}, use_global_device_ids=true | all-gather | bytes 4608 | tf_op jit(solution)/shard_map/all_gather | solution.py:47
  9.1 0.6 broadcast_in_dim.25
  9.8 9.6 %all-to-all-start = ((bf16[16,8,256]{2,1,0:T(8,128)(2,1)}), bf16[16,8,256]{2,1,0:T(8,128)(2,1)S(1)}, u32[]{:S(2)}, u32[]{:S(2)}) async-start(bf16[16,8,256]{2,1,0:T(8,128)(2,1)} %broadcast_in_dim.25), calls=%async_computation | async-start | bytes 131072 | tf_op jit(solution)/shard_map/all_to_all | solution.py:17
  19.3 0.9 bitcast_dynamic-update-slice_fusion.6
  20.2 0.8 slice_convert_fusion
  21.0 0.8 slice_bitcast_fusion.4
  21.8 0.8 fusion.40
  22.5 0.0 copy-start.3
  22.5 0.0 copy-start.4
  22.6 0.0 copy-start
  22.6 0.0 copy-start.1
  22.6 1.6 %slice_bitcast_fusion = (f32[6,128,256]{2,1,0:T(8,128)S(1)}, f32[6,128,256]{2,1,0:T(8,128)S(1)}) fusion(f32[2,6,128,256]{3,2,1,0:T(8,128)} %param.21), kind=kLoop, calls=%fused_computation.15 | loop fusion | bytes 3145728 | tf_op jit(solution)/shard_map/squeeze | solution.py:66
  24.2 0.0 copy-start.2
  24.2 0.0 copy-done.3
  24.3 0.0 copy-done.4
  24.3 0.0 copy-done
  24.4 0.0 copy-done.1
  24.5 0.7 copy-done.2
  25.2 5.8 %all-to-all-done = bf16[16,8,256]{2,1,0:T(8,128)(2,1)S(1)} async-done(((bf16[16,8,256]{2,1,0:T(8,128)(2,1)}), bf16[16,8,256]{2,1,0:T(8,128)(2,1)S(1)}, u32[]{:S(2)}, u32[]{:S(2)}) %all-to-all-start) | async-done | bytes 65568 | tf_op jit(solution)/shard_map/all_to_all | solution.py:17
  31.0 0.1 fusion.8
  31.1 0.1 broadcast_in_dim.26
  31.2 0.2 fusion.3
  31.5 14.1 %all_to_all.40 = bf16[16,8,1024]{2,1,0:T(8,128)(2,1)S(1)} all-to-all(bf16[16,8,1024]{2,1,0:T(8,128)(2,1)S(1)} %fusion.3), channel_id=1, replica_groups=mesh['z'=16,'c'=2,'y'=4,'x'=4] {'y','x'}, dimensions={0} | all-to-all | bytes 524288 | tf_op jit(solution)/shard_map/all_to_all | solution.py:17
  45.6 0.1 fusion.39
  45.7 0.1 slice_multiply_fusion.1
  45.8 0.4 fusion.6
  46.3 9.4 %all_to_all.41 = bf16[16,8,256]{2,1,0:T(8,128)(2,1)S(1)} all-to-all(bf16[16,8,256]{2,1,0:T(8,128)(2,1)S(1)} %broadcast_in_dim.28), channel_id=1, replica_groups=mesh['z'=16,'c'=2,'y'=4,'x'=4] {'y','x'}, dimensions={0} | all-to-all | bytes 131072 | tf_op jit(solution)/shard_map/all_to_all | solution.py:17
  55.7 0.2 fusion.4
  55.9 16.9 %all_to_all.42 = bf16[16,8,256]{2,1,0:T(8,128)(2,1)S(1)} all-to-all(bf16[16,8,256]{2,1,0:T(8,128)(2,1)S(1)} %fusion.4), channel_id=1, replica_groups=mesh['z'=16,'c'=2,'y'=4,'x'=4] {'z'}, dimensions={0} | all-to-all | bytes 131072 | tf_op jit(solution)/shard_map/all_to_all | solution.py:17
  72.8 6.6 %all-gather = f32[16,256]{1,0:T(8,128)S(1)} all-gather(f32[8,256]{1,0:T(8,128)S(1)} %convert_reduce_fusion.3), channel_id=2, replica_groups=mesh['z'=16,'c'=2,'y'=4,'x'=4] {'c'}, dimensions={0}, use_global_device_ids=true | all-gather | bytes 24576 | tf_op jit(solution)/shard_map/all_gather | solution.py:99
  79.4 14.3 %all_to_all.43 = bf16[16,8,256]{2,1,0:T(8,128)(2,1)S(1)} all-to-all(bf16[16,8,256]{2,1,0:T(8,128)(2,1)S(1)} %broadcast_in_dim.29), channel_id=1, replica_groups=mesh['z'=16,'c'=2,'y'=4,'x'=4] {'z'}, dimensions={0} | all-to-all | bytes 131072 | tf_op jit(solution)/shard_map/all_to_all | solution.py:17
  93.7 0.1 fusion.11
  93.8 0.1 broadcast_in_dim.30
  93.9 0.2 fusion.2
  94.1 10.4 %all_to_all.44 = bf16[16,8,1024]{2,1,0:T(8,128)(2,1)S(1)} all-to-all(bf16[16,8,1024]{2,1,0:T(8,128)(2,1)S(1)} %fusion.2), channel_id=1, replica_groups=mesh['z'=16,'c'=2,'y'=4,'x'=4] {'y','x'}, dimensions={0} | all-to-all | bytes 524288 | tf_op jit(solution)/shard_map/all_to_all | solution.py:17
  104.6 0.1 fusion.35
  104.7 0.1 slice_multiply_fusion
  104.8 0.4 fusion.7
  105.3 9.4 %all_to_all.45 = bf16[16,8,256]{2,1,0:T(8,128)(2,1)S(1)} all-to-all(bf16[16,8,256]{2,1,0:T(8,128)(2,1)S(1)} %broadcast_in_dim.32), channel_id=1, replica_groups=mesh['z'=16,'c'=2,'y'=4,'x'=4] {'y','x'}, dimensions={0} | all-to-all | bytes 131072 | tf_op jit(solution)/shard_map/all_to_all | solution.py:17
  114.7 0.8 fusion.5
  115.5 3.8 %all-to-all-start.7 = ((bf16[16,8,256]{2,1,0:T(8,128)(2,1)}), bf16[16,8,256]{2,1,0:T(8,128)(2,1)S(1)}, u32[]{:S(2)}, u32[]{:S(2)}) async-start(bf16[16,8,256]{2,1,0:T(8,128)(2,1)} %fusion.5), calls=%async_computation.7 | async-start | bytes 131072 | tf_op jit(solution)/shard_map/all_to_all | solution.py:17
  119.3 1.3 pad_maximum_fusion
  120.7 10.2 %all-to-all-done.7 = bf16[16,8,256]{2,1,0:T(8,128)(2,1)S(1)} async-done(((bf16[16,8,256]{2,1,0:T(8,128)(2,1)}), bf16[16,8,256]{2,1,0:T(8,128)(2,1)S(1)}, u32[]{:S(2)}, u32[]{:S(2)}) %all-to-all-start.7) | async-done | bytes 65568 | tf_op jit(solution)/shard_map/all_to_all | solution.py:17
  130.9 6.8 %all-gather.1 = f32[16,256]{1,0:T(8,128)S(1)} all-gather(f32[8,256]{1,0:T(8,128)S(1)} %convert_reduce_fusion.2), channel_id=3, replica_groups=mesh['z'=16,'c'=2,'y'=4,'x'=4] {'c'}, dimensions={0}, use_global_device_ids=true | all-gather | bytes 24576 | tf_op jit(solution)/shard_map/all_gather | solution.py:99
  137.7 0.6 slice_select_fusion
  (27 shorter events, 0.5 us)
Async XLA Ops:
  9.8 21.3 %all-to-all-start = ((bf16[16,8,256]{2,1,0:T(8,128)(2,1)}), bf16[16,8,256]{2,1,0:T(8,128)(2,1)S(1)}, u32[]{:S(2)}, u32[]{:S(2)}) async-start(bf16[16,8,256]{2,1,0:T(8,128)(2,1)} %broadcast_in_dim.25), calls=%async_computation | async-start | bytes 131072 | tf_op jit(solution)/shard_map/all_to_all | solution.py:17
  22.5 1.7 %copy-start.3 = (bf16[2,256,128]{2,1,0:T(8,128)(2,1)S(1)}, bf16[2,256,128]{2,1,0:T(8,128)(2,1)}, u32[]{:S(2)}) copy-start(bf16[2,256,128]{2,1,0:T(8,128)(2,1)} %param.14) | copy-start | bytes 393220
  22.5 1.7 %copy-start.4 = (bf16[2,256,128]{2,1,0:T(8,128)(2,1)S(1)}, bf16[2,256,128]{2,1,0:T(8,128)(2,1)}, u32[]{:S(2)}) copy-start(bf16[2,256,128]{2,1,0:T(8,128)(2,1)} %param.15) | copy-start | bytes 393220
  22.6 1.8 %copy-start = (bf16[2,256,256]{2,1,0:T(8,128)(2,1)S(1)}, bf16[2,256,256]{2,1,0:T(8,128)(2,1)}, u32[]{:S(2)}) copy-start(bf16[2,256,256]{2,1,0:T(8,128)(2,1)} %param.18) | copy-start | bytes 786436
  22.6 1.8 %copy-start.1 = (bf16[2,256,256]{2,1,0:T(8,128)(2,1)S(1)}, bf16[2,256,256]{2,1,0:T(8,128)(2,1)}, u32[]{:S(2)}) copy-start(bf16[2,256,256]{2,1,0:T(8,128)(2,1)} %param.19) | copy-start | bytes 786436
  24.2 1.0 copy-start.2
  115.5 15.4 %all-to-all-start.7 = ((bf16[16,8,256]{2,1,0:T(8,128)(2,1)}), bf16[16,8,256]{2,1,0:T(8,128)(2,1)S(1)}, u32[]{:S(2)}, u32[]{:S(2)}) async-start(bf16[16,8,256]{2,1,0:T(8,128)(2,1)} %fusion.5), calls=%async_computation.7 | async-start | bytes 131072 | tf_op jit(solution)/shard_map/all_to_all | solution.py:17

commit v3 on v1

v3 whole, which is shorter than its diff:
```python
import functools

import jax
import jax.numpy as jnp
from jax import lax
from jax.experimental import pallas as pl
from jax.experimental.pallas import tpu as pltpu
from jax.sharding import Mesh, PartitionSpec as P

D = 4096
DK = 128
BLOCKS = 2
PAD = 8
LANES = 128
BF = jnp.bfloat16
F32 = jnp.float32
DP = ("y", "x")
TP = ("z", "c")
VMEM = pl.BlockSpec(memory_space=pltpu.VMEM)
SMALL = pltpu.CompilerParams(vmem_limit_bytes=12 * 1024 * 1024)


def exchange(parts, axis):
    return lax.all_to_all(parts, axis, 0, 0, tiled=True)


def project_kernel(b, rows_ref, gain_ref, *refs):
    *weights, out_ref = refs
    groups, pad, width = rows_ref.shape
    rows = rows_ref[...].astype(F32).reshape(groups * pad, width)
    squares = jnp.sum(rows * rows, axis=1, keepdims=True)
    hidden = (rows * gain_ref[b : b + 1, :].astype(F32)).astype(BF)
    at = 0
    for w in weights:
        n = w.shape[2]
        part = jnp.dot(hidden, w[b], preferred_element_type=F32)
        out_ref[:, :, at : at + n] = part.reshape(groups, pad, n).astype(BF)
        at += n
    lane = lax.broadcasted_iota(jnp.int32, (groups * pad, LANES), 1)
    last = jnp.where(lane == 0, squares, 0.0)
    out_ref[:, :, at : at + LANES] = last.reshape(groups, pad, LANES).astype(BF)


def project(b, rows, gain, weights):
    cols = sum(w.shape[2] for w in weights) + LANES
    return pl.pallas_call(
        functools.partial(project_kernel, b),
        out_shape=jax.ShapeDtypeStruct((*rows.shape[:2], cols), BF),
        in_specs=[VMEM] * (2 + len(weights)),
        out_specs=VMEM,
        compiler_params=SMALL,
        name="project",
    )(rows, gain, *weights)


def spread_kernel(rows_ref, out_ref):
    rows = rows_ref[...].astype(F32)
    rows = jnp.concatenate([rows, jnp.zeros((PAD - rows.shape[0], rows.shape[1]), F32)], axis=0)
    out_ref[...] = jnp.broadcast_to(rows[None], out_ref.shape).astype(BF)


def spread(rows, n):
    return pl.pallas_call(
        spread_kernel,
        out_shape=jax.ShapeDtypeStruct((n, PAD, rows.shape[1]), BF),
        in_specs=[VMEM],
        out_specs=VMEM,
        compiler_params=SMALL,
        cost_estimate=pl.CostEstimate(flops=10**10, bytes_accessed=10**7, transcendentals=0),
        name="spread",
    )(rows)


def step_kernel(b, seqs, kc, vc, parts_ref, shift_ref, fade_ref, state_ref, out_ref, d_ref, k_ref, v_ref):
    total = jnp.sum(parts_ref[...].astype(F32), axis=0)
    cols = 3 * kc + 2 * vc
    total = total * lax.rsqrt(total[:, cols : cols + 1] / D + 1e-06)
    queries = total[:seqs, :kc] * DK ** (-0.5)
    keys = total[:seqs, kc : 2 * kc]
    pre = total[:seqs, 2 * kc : 3 * kc] + shift_ref[b : b + 1, :]
    values = total[:seqs, 3 * kc : 3 * kc + vc]
    gates = total[:seqs, 3 * kc + vc : cols]
    log_sigmoid = jnp.minimum(pre, 0.0) - jnp.log1p(jnp.exp(-jnp.abs(pre)))
    decay = jnp.exp(log_sigmoid / 16.0 + fade_ref[:, b, :])
    fresh_part = jnp.sum(queries * keys, axis=1, keepdims=True) * values
    columns = jnp.concatenate([queries * decay, jnp.zeros((PAD - seqs, kc), F32)], axis=0).T
    old = [
        jnp.sum(columns[:, s : s + 1] * state_ref[b, s], axis=0, keepdims=True) for s in range(seqs)
    ]
    readout = jnp.concatenate(old, axis=0) + fresh_part
    gated = readout * (gates / (1.0 + jnp.exp(-gates)))
    gated = jnp.concatenate([gated, jnp.zeros((PAD - seqs, vc), F32)], axis=0)
    out_ref[...] = jnp.broadcast_to(gated[None], out_ref.shape).astype(BF)
    d_ref[...] = decay
    k_ref[...] = keys
    v_ref[...] = values


def step(b, parts, shift, fade, state):
    seqs, _, kc = fade.shape
    vc = state.shape[3]
    return pl.pallas_call(
        functools.partial(step_kernel, b, seqs, kc, vc),
        out_shape=(
            jax.ShapeDtypeStruct((parts.shape[0], PAD, vc), BF),
            jax.ShapeDtypeStruct((seqs, kc), F32),
            jax.ShapeDtypeStruct((seqs, kc), F32),
            jax.ShapeDtypeStruct((seqs, vc), F32),
        ),
        in_specs=[VMEM] * 4,
        out_specs=(VMEM,) * 4,
        compiler_params=SMALL,
        name="step",
    )(parts, shift, fade, state)


def readback_kernel(b, gated_ref, weight_ref, out_ref):
    groups, pad, width = gated_ref.shape
    gated = gated_ref[...].astype(F32).reshape(groups * pad, width).astype(BF)
    branch = jnp.dot(gated, weight_ref[b], preferred_element_type=F32)
    out_ref[...] = branch.reshape(groups, pad, -1).astype(BF)


def readback(b, gated, weight):
    return pl.pallas_call(
        functools.partial(readback_kernel, b),
        out_shape=jax.ShapeDtypeStruct((*gated.shape[:2], weight.shape[2]), BF),
        in_specs=[VMEM] * 2,
        out_specs=VMEM,
        compiler_params=SMALL,
        name="readback",
    )(gated, weight)


def shards(
    incoming_embeddings,
    rescale_factors,
    probe_lift,
    address_lift,
    forget_lift,
    forget_shift,
    surplus_fade,
    content_lift,
    filter_lift,
    readback_lift,
    memory_tensor,
):
    weights = (probe_lift, address_lift, forget_lift, content_lift, filter_lift)
    depth = lax.axis_size("z")
    third = incoming_embeddings.shape[0]
    stream, first_core = lax.optimization_barrier((incoming_embeddings, lax.axis_index("c") == 0))
    stream = lax.all_gather(stream, "c", axis=0, tiled=True)
    fade = jnp.transpose(surplus_fade, (1, 0, 2))
    kept = []
    for b in range(BLOCKS):
        if b == 0:
            rows = exchange(spread(stream, depth), "z")
            stream = jnp.pad(stream, ((0, PAD - stream.shape[0]), (0, 0)))
        else:
            rows = exchange(jnp.broadcast_to(stream[None], (depth, *stream.shape)), "z")
        parts = exchange(project(b, rows, rescale_factors, weights), DP)
        gated, *small = step(b, parts, forget_shift, fade, memory_tensor)
        gathered = exchange(gated, DP)
        if b == BLOCKS - 1:
            kept.append(small)
            gathered, kept = lax.optimization_barrier((gathered, kept))
        else:
            kept.append(small)
        heads = exchange(readback(b, gathered, readback_lift), "z")
        own = jnp.sum(heads.astype(F32), axis=0)
        both = lax.all_gather(own, "c", axis=0)
        stream = (stream.astype(F32) + (both[0] + both[1])).astype(BF)
    fresh = [
        memory_tensor[b] * d[:, :, None] + k[:, :, None] * v[:, None, :]
        for b, (d, k, v) in enumerate(kept)
    ]
    mixed = jnp.where(first_core, stream[:third], stream[third : 2 * third])
    return mixed, jnp.stack(fresh)


def solution(mesh):
    z = mesh.shape["tp"] // 2
    fine = Mesh(mesh.devices.reshape(z, 2, 4, 4), ("z", "c", "y", "x"))
    in_specs = (
        P(TP, DP),
        P(None, DP),
        P(None, DP, TP),
        P(None, DP, TP),
        P(None, DP, TP),
        P(None, TP),
        P(None, DP, TP),
        P(None, DP, TP),
        P(None, DP, TP),
        P(None, TP, DP),
        P(None, DP, None, TP),
    )
    out_specs = (P(TP, DP), P(None, DP, None, TP))
    return jax.shard_map(shards, mesh=fine, in_specs=in_specs, out_specs=out_specs, check_vma=False)
```

time: 141 us -> 136 us (0.965)
  blocking collectives: 57 us -> 116 us
  waiting for transfers between devices: 43.1 us -> 9.83 us
  starting transfers between devices: 27.2 us -> 3.82 us
  local copies, waits for them, and re-layouts: 6.11 us -> 0.08 us
  Pallas kernels: 0 us -> 2.24 us
  matrix products: 2.12 us -> 0 us
  other arithmetic: 3.91 us -> 2.37 us
    all_to_all x3 -> x7, blocking collectives: 35.1 us -> 94.1 us  [exchange(): return lax.all_to_all(parts, axis, 0, 0, tiled=True)]
    all_to_all x5 -> x1, waiting for transfers between devices: 43.1 us -> 9.83 us  [exchange(): return lax.all_to_all(parts, axis, 0, 0, tiled=True)]
    all_to_all x5 -> x1, starting transfers between devices: 27.2 us -> 3.82 us  [exchange(): return lax.all_to_all(parts, axis, 0, 0, tiled=True)]
    unnamed x18 -> x21, local copies, waits for them, and re-layouts: 3.91 us -> 0.07 us
    pallas_call x0 -> x7, Pallas kernels: none -> 2.24 us  [the longest x2 0.94 us: readback(): pl.pallas_call(functools.partial(readback_kernel, b), out_shape=jax.Shape...]
    dot_general x4 -> x0, matrix products: 2.12 us -> none  [the longest x2 1.18 us: shards(): partial = jnp.dot(hidden, weights, preferred_element_type=F32)]
    broadcast_in_dim x6 -> x1, local copies, waits for them, and re-layouts: 2.12 us -> 0.01 us  [shards(): rows = exchange(jnp.broadcast_to(stream[None], (depth, *stream.shape)), 'z')]
  transfers between devices with their start and end apart: 5 -> 1, of which waited for: 5 -> 1; matrix products, arithmetic and copies ran while one was open for 4% -> 1% of each run, Pallas kernels for 0% -> 0%
where the time goes in v3:
time: 136 us; the launch traced here: 135 us
  blocking collectives  116 us (85%)
  waiting for transfers between devices  9.83 us (7%)
  starting transfers between devices  3.82 us (3%)
  other arithmetic  2.37 us (2%)
  Pallas kernels  2.24 us (2%)
    all_to_all x7, blocking collectives, exchange(): return lax.all_to_all(parts, axis, 0, 0, tiled=True)  94.1 us
    all_gather x2, blocking collectives, shards(): both = lax.all_gather(own, 'c', axis=0)  13.3 us
    all_to_all x1, waiting for transfers between devices, exchange(): return lax.all_to_all(parts, axis, 0, 0, tiled=True)  9.83 us
    all_gather x1, blocking collectives, shards(): stream = lax.all_gather(stream, 'c', axis=0, tiled=True)  8.47 us
    all_to_all x1, starting transfers between devices, exchange(): return lax.all_to_all(parts, axis, 0, 0, tiled=True)  3.82 us
  transfers between devices with their start and end apart: 1, of which 1 were waited for; matrix products, arithmetic and copies ran while one was open for 1% of the time, Pallas kernels for 0%

profile of v3, /device:TPU:1, one launch (start us, length us, event | category | flops | bytes accessed | tf_op | source)
XLA Modules:
  0.0 135.1 jit_solution(6079363042655517668)
XLA Ops:
  0.6 8.5 %all-gather.2 = bf16[2,3,256]{2,1,0:T(4,128)(2,1)S(1)} all-gather(bf16[1,3,256]{2,1,0:T(4,128)(2,1)} %bitcast.4), channel_id=1, replica_groups=mesh['z'=16,'c'=2,'y'=4,'x'=4] {'c'}, dimensions={0}, use_global_device_ids=true | all-gather | bytes 4608 | tf_op jit(solution)/shard_map/all_gather | solution.py:152
  9.1 0.0 copy-start.2
  9.1 0.0 copy-start.3
  9.1 0.0 copy-start.4
  9.1 0.0 copy-start.5
  9.2 0.0 copy-start.6
  9.2 0.0 copy-start.9
  9.2 0.0 copy-start
  9.2 0.0 copy-start.7
  9.2 0.0 copy-start.8
  9.2 21.2 %all_to_all.40.rows_ref = bf16[16,8,256]{2,1,0:T(8,128)(2,1)S(1)} all-to-all(bf16[16,8,256]{2,1,0:T(8,128)(2,1)S(1)} %spread.1), channel_id=1, replica_groups=mesh['z'=16,'c'=2,'y'=4,'x'=4] {'z'}, dimensions={0} | all-to-all | bytes 131072 | tf_op jit(solution)/shard_map/all_to_all | solution.py:24
  30.4 0.0 copy-done.2
  30.4 0.0 copy-done.3
  30.4 0.0 copy-done.4
  30.4 0.0 copy-done.5
  30.4 0.0 copy-done.6
  30.4 0.0 copy-done.9
  30.5 0.0 copy-start.1
  30.5 0.2 project.2
  30.7 14.1 %all_to_all.41.parts_ref = bf16[16,8,1024]{2,1,0:T(8,128)(2,1)S(1)} all-to-all(bf16[16,8,1024]{2,1,0:T(8,128)(2,1)S(1)} %project.2), channel_id=1, replica_groups=mesh['z'=16,'c'=2,'y'=4,'x'=4] {'y','x'}, dimensions={0} | all-to-all | bytes 524288 | tf_op jit(solution)/shard_map/all_to_all | solution.py:24
  44.8 0.0 copy-done
  44.8 0.0 copy-done.7
  44.8 0.0 copy-done.8
  44.8 0.4 step.2
  45.2 9.4 %all_to_all.42.gated_ref = bf16[16,8,256]{2,1,0:T(8,128)(2,1)S(1)} all-to-all(bf16[16,8,256]{2,1,0:T(8,128)(2,1)S(1)} %get-tuple-element.21), channel_id=1, replica_groups=mesh['z'=16,'c'=2,'y'=4,'x'=4] {'y','x'}, dimensions={0} | all-to-all | bytes 131072 | tf_op jit(solution)/shard_map/all_to_all | solution.py:24
  54.7 0.0 copy-done.1
  54.7 0.2 readback.2
  54.8 15.1 %all_to_all.43 = bf16[16,8,256]{2,1,0:T(8,128)(2,1)S(1)} all-to-all(bf16[16,8,256]{2,1,0:T(8,128)(2,1)S(1)} %readback.2), channel_id=1, replica_groups=mesh['z'=16,'c'=2,'y'=4,'x'=4] {'z'}, dimensions={0} | all-to-all | bytes 131072 | tf_op jit(solution)/shard_map/all_to_all | solution.py:24
  70.0 6.5 %all-gather = f32[16,256]{1,0:T(8,128)S(1)} all-gather(f32[8,256]{1,0:T(8,128)S(1)} %convert_reduce_fusion.1), channel_id=2, replica_groups=mesh['z'=16,'c'=2,'y'=4,'x'=4] {'c'}, dimensions={0}, use_global_device_ids=true | all-gather | bytes 24576 | tf_op jit(solution)/shard_map/all_gather | solution.py:171
  76.5 14.3 %all_to_all.44.rows_ref = bf16[16,8,256]{2,1,0:T(8,128)(2,1)S(1)} all-to-all(bf16[16,8,256]{2,1,0:T(8,128)(2,1)S(1)} %broadcast_in_dim.2), channel_id=1, replica_groups=mesh['z'=16,'c'=2,'y'=4,'x'=4] {'z'}, dimensions={0} | all-to-all | bytes 131072 | tf_op jit(solution)/shard_map/all_to_all | solution.py:24
  90.8 0.2 project.3
  91.1 10.6 %all_to_all.45.parts_ref = bf16[16,8,1024]{2,1,0:T(8,128)(2,1)S(1)} all-to-all(bf16[16,8,1024]{2,1,0:T(8,128)(2,1)S(1)} %project.3), channel_id=1, replica_groups=mesh['z'=16,'c'=2,'y'=4,'x'=4] {'y','x'}, dimensions={0} | all-to-all | bytes 524288 | tf_op jit(solution)/shard_map/all_to_all | solution.py:24
  101.6 0.4 step.3
  102.0 9.4 %all_to_all.46.gated_ref = bf16[16,8,256]{2,1,0:T(8,128)(2,1)S(1)} all-to-all(bf16[16,8,256]{2,1,0:T(8,128)(2,1)S(1)} %get-tuple-element.22), channel_id=1, replica_groups=mesh['z'=16,'c'=2,'y'=4,'x'=4] {'y','x'}, dimensions={0} | all-to-all | bytes 131072 | tf_op jit(solution)/shard_map/all_to_all | solution.py:24
  111.5 0.8 readback.3
  112.2 3.8 %all-to-all-start.7 = ((bf16[16,8,256]{2,1,0:T(8,128)(2,1)}), bf16[16,8,256]{2,1,0:T(8,128)(2,1)S(1)}, u32[]{:S(2)}, u32[]{:S(2)}) async-start(bf16[16,8,256]{2,1,0:T(8,128)(2,1)} %readback.3), calls=%async_computation.7 | async-start | bytes 131072 | tf_op jit(solution)/shard_map/all_to_all | solution.py:24
  116.1 0.5 multiply_add_fusion.1
  116.6 1.2 pad_maximum_fusion
  117.8 9.8 %all-to-all-done.7 = bf16[16,8,256]{2,1,0:T(8,128)(2,1)S(1)} async-done(((bf16[16,8,256]{2,1,0:T(8,128)(2,1)}), bf16[16,8,256]{2,1,0:T(8,128)(2,1)S(1)}, u32[]{:S(2)}, u32[]{:S(2)}) %all-to-all-start.7) | async-done | bytes 65568 | tf_op jit(solution)/shard_map/all_to_all | solution.py:24
  127.7 6.8 %all-gather.1 = f32[16,256]{1,0:T(8,128)S(1)} all-gather(f32[8,256]{1,0:T(8,128)S(1)} %convert_reduce_fusion), channel_id=3, replica_groups=mesh['z'=16,'c'=2,'y'=4,'x'=4] {'c'}, dimensions={0}, use_global_device_ids=true | all-gather | bytes 24576 | tf_op jit(solution)/shard_map/all_gather | solution.py:171
  134.5 0.6 slice_select_fusion
  (7 shorter events, 0.1 us)
Async XLA Ops:
  9.1 21.3 %copy-start.2 = (bf16[2,256,256]{2,1,0:T(8,128)(2,1)S(1)}, bf16[2,256,256]{2,1,0:T(8,128)(2,1)}, u32[]{:S(2)}) copy-start(bf16[2,256,256]{2,1,0:T(8,128)(2,1)} %refs_3_.3) | copy-start | bytes 786436
  9.1 21.3 %copy-start.3 = (bf16[2,256,256]{2,1,0:T(8,128)(2,1)S(1)}, bf16[2,256,256]{2,1,0:T(8,128)(2,1)}, u32[]{:S(2)}) copy-start(bf16[2,256,256]{2,1,0:T(8,128)(2,1)} %refs_4_.3) | copy-start | bytes 786436
  9.1 21.3 %copy-start.4 = (bf16[2,256,128]{2,1,0:T(8,128)(2,1)S(1)}, bf16[2,256,128]{2,1,0:T(8,128)(2,1)}, u32[]{:S(2)}) copy-start(bf16[2,256,128]{2,1,0:T(8,128)(2,1)} %refs_0_.3) | copy-start | bytes 393220
  9.1 21.3 %copy-start.5 = (bf16[2,256,128]{2,1,0:T(8,128)(2,1)S(1)}, bf16[2,256,128]{2,1,0:T(8,128)(2,1)}, u32[]{:S(2)}) copy-start(bf16[2,256,128]{2,1,0:T(8,128)(2,1)} %refs_1_.3) | copy-start | bytes 393220
  9.2 21.3 %copy-start.6 = (bf16[2,256,128]{2,1,0:T(8,128)(2,1)S(1)}, bf16[2,256,128]{2,1,0:T(8,128)(2,1)}, u32[]{:S(2)}) copy-start(bf16[2,256,128]{2,1,0:T(8,128)(2,1)} %refs_2_.3) | copy-start | bytes 393220
  9.2 21.3 %copy-start.9 = (bf16[2,256]{1,0:T(2,128)(2,1)S(1)}, bf16[2,256]{1,0:T(2,128)(2,1)}, u32[]{:S(2)}) copy-start(bf16[2,256]{1,0:T(2,128)(2,1)} %gain_ref.3) | copy-start | bytes 3076
  9.2 35.6 %copy-start = (f32[2,6,128,256]{3,2,1,0:T(8,128)S(1)}, f32[2,6,128,256]{3,2,1,0:T(8,128)}, u32[]{:S(2)}) copy-start(f32[2,6,128,256]{3,2,1,0:T(8,128)} %state_ref.3) | copy-start | bytes 4718596
  9.2 35.6 %copy-start.7 = (f32[2,6,128]{2,0,1:T(2,128)S(1)}, f32[2,6,128]{2,0,1:T(2,128)}, u32[]{:S(2)}) copy-start(f32[2,6,128]{2,0,1:T(2,128)} %param.17) | copy-start | bytes 18436
  9.2 35.6 %copy-start.8 = (f32[2,128]{1,0:T(2,128)S(1)}, f32[2,128]{1,0:T(2,128)}, u32[]{:S(2)}) copy-start(f32[2,128]{1,0:T(2,128)} %shift_ref.3) | copy-start | bytes 3076
  30.5 24.2 %copy-start.1 = (bf16[2,256,256]{2,1,0:T(8,128)(2,1)S(1)}, bf16[2,256,256]{2,1,0:T(8,128)(2,1)}, u32[]{:S(2)}) copy-start(bf16[2,256,256]{2,1,0:T(8,128)(2,1)} %weight_ref.3) | copy-start | bytes 786436
  112.2 15.4 %all-to-all-start.7 = ((bf16[16,8,256]{2,1,0:T(8,128)(2,1)}), bf16[16,8,256]{2,1,0:T(8,128)(2,1)S(1)}, u32[]{:S(2)}, u32[]{:S(2)}) async-start(bf16[16,8,256]{2,1,0:T(8,128)(2,1)} %readback.3), calls=%async_computation.7 | async-start | bytes 131072 | tf_op jit(solution)/shard_map/all_to_all | solution.py:24

commit v4 on v3

--- a/solution.py
+++ b/solution.py
@@ -20,14 +20,25 @@
 SMALL = pltpu.CompilerParams(vmem_limit_bytes=12 * 1024 * 1024)
 
 
+ORDER = {
+    "z": tuple((8 + k) % 16 for k in range(16)),
+    DP: tuple((10 + k) % 16 for k in range(16)),
+}
+
+
 def exchange(parts, axis):
-    return lax.all_to_all(parts, axis, 0, 0, tiled=True)
+    return lax.all_to_all(parts, axis, 0, 0, tiled=True, axis_index_groups=[list(ORDER[axis])])
+
+
+def reordered(ref, source, target):
+    at = [ORDER[source].index(i) for i in ORDER[target]]
+    return jnp.concatenate([ref[i].astype(F32) for i in at], axis=0)
 
 
 def project_kernel(b, rows_ref, gain_ref, *refs):
     *weights, out_ref = refs
     groups, pad, width = rows_ref.shape
-    rows = rows_ref[...].astype(F32).reshape(groups * pad, width)
+    rows = reordered(rows_ref, "z", DP)
     squares = jnp.sum(rows * rows, axis=1, keepdims=True)
     hidden = (rows * gain_ref[b : b + 1, :].astype(F32)).astype(BF)
     at = 0
@@ -116,7 +127,7 @@
 
 def readback_kernel(b, gated_ref, weight_ref, out_ref):
     groups, pad, width = gated_ref.shape
-    gated = gated_ref[...].astype(F32).reshape(groups * pad, width).astype(BF)
+    gated = reordered(gated_ref, DP, "z").astype(BF)
     branch = jnp.dot(gated, weight_ref[b], preferred_element_type=F32)
     out_ref[...] = branch.reshape(groups, pad, -1).astype(BF)
 

time: 136 us -> 126 us (0.926)
  blocking collectives: 116 us -> 107 us
  waiting for transfers between devices: 9.83 us -> 1.4 us
  starting transfers between devices: 3.82 us -> 11.5 us
    all_to_all x1, waiting for transfers between devices: 9.83 us -> 1.4 us  [exchange(): lax.all_to_all(parts, axis, 0, 0, tiled=True, axis_index_groups=[list(ORD...]
    all_to_all x7, blocking collectives: 94.1 us -> 86.3 us  [exchange(): lax.all_to_all(parts, axis, 0, 0, tiled=True, axis_index_groups=[list(ORD...]
    all_to_all x1, starting transfers between devices: 3.82 us -> 11.5 us  [exchange(): lax.all_to_all(parts, axis, 0, 0, tiled=True, axis_index_groups=[list(ORD...]
where the time goes in v4:
time: 126 us
  blocking collectives  107 us (85%)
  starting transfers between devices  11.5 us (9%)
  other arithmetic  2.37 us (2%)
  Pallas kernels  2.23 us (2%)
  waiting for transfers between devices  1.4 us (1%)
    all_to_all x7, blocking collectives, exchange(): lax.all_to_all(parts, axis, 0, 0, tiled=True, axis_index_groups=[list(ORD...  86.3 us
    all_gather x2, blocking collectives, shards(): both = lax.all_gather(own, 'c', axis=0)  12.6 us
    all_to_all x1, starting transfers between devices, exchange(): lax.all_to_all(parts, axis, 0, 0, tiled=True, axis_index_groups=[list(ORD...  11.5 us
    all_gather x1, blocking collectives, shards(): stream = lax.all_gather(stream, 'c', axis=0, tiled=True)  8.47 us
  transfers between devices with their start and end apart: 1, of which 1 were waited for; matrix products, arithmetic and copies ran while one was open for 1% of the time, Pallas kernels for 0%

profile of v4, /device:TPU:1, one launch (start us, length us, event | category | flops | bytes accessed | tf_op | source)
XLA Modules:
  0.0 125.7 jit_solution(3062480243918027934)
XLA Ops:
  0.6 8.5 %all-gather.2 = bf16[2,3,256]{2,1,0:T(4,128)(2,1)S(1)} all-gather(bf16[1,3,256]{2,1,0:T(4,128)(2,1)} %bitcast.4), channel_id=1, replica_groups=mesh['z'=16,'c'=2,'y'=4,'x'=4] {'c'}, dimensions={0}, use_global_device_ids=true | all-gather | bytes 4608 | tf_op jit(solution)/shard_map/all_gather | solution.py:163
  9.1 0.0 copy-start.2
  9.1 0.0 copy-start.3
  9.1 0.0 copy-start.4
  9.1 0.0 copy-start.5
  9.2 0.0 copy-start.6
  9.2 0.0 copy-start.9
  9.2 0.0 copy-start
  9.2 0.0 copy-start.7
  9.2 0.0 copy-start.8
  9.2 17.0 %all_to_all.40.rows_ref = bf16[16,8,256]{2,1,0:T(8,128)(2,1)S(1)} all-to-all(bf16[16,8,256]{2,1,0:T(8,128)(2,1)S(1)} %spread.1), channel_id=1, replica_groups={{256,288,320,352,384,416,448,480,0,32,64,96,128,160,192,224},{257,289,3..., dimensions={0} | all-to-all | bytes 131072 | tf_op jit(solution)/shard_map/all_to_all | solution.py:30
  26.2 0.0 copy-done.2
  26.2 0.0 copy-done.3
  26.2 0.0 copy-done.4
  26.2 0.0 copy-done.5
  26.2 0.0 copy-done.6
  26.2 0.0 copy-done.9
  26.2 0.0 copy-start.1
  26.2 0.2 project.2
  26.5 11.2 %all_to_all.41.parts_ref = bf16[16,8,1024]{2,1,0:T(8,128)(2,1)S(1)} all-to-all(bf16[16,8,1024]{2,1,0:T(8,128)(2,1)S(1)} %project.2), channel_id=1, replica_groups={{10,11,12,13,14,15,0,1,2,3,4,5,6,7,8,9},{26,27,28,29,30,31,16,17,18,19,..., dimensions={0} | all-to-all | bytes 524288 | tf_op jit(solution)/shard_map/all_to_all | solution.py:30
  37.6 0.0 copy-done
  37.6 0.0 copy-done.7
  37.6 0.0 copy-done.8
  37.7 0.4 step.2
  38.1 8.9 %all_to_all.42.gated_ref = bf16[16,8,256]{2,1,0:T(8,128)(2,1)S(1)} all-to-all(bf16[16,8,256]{2,1,0:T(8,128)(2,1)S(1)} %get-tuple-element.21), channel_id=1, replica_groups={{10,11,12,13,14,15,0,1,2,3,4,5,6,7,8,9},{26,27,28,29,30,31,16,17,18,19,..., dimensions={0} | all-to-all | bytes 131072 | tf_op jit(solution)/shard_map/all_to_all | solution.py:30
  46.9 0.0 copy-done.1
  46.9 0.2 readback.2
  47.1 14.4 %all_to_all.43 = bf16[16,8,256]{2,1,0:T(8,128)(2,1)S(1)} all-to-all(bf16[16,8,256]{2,1,0:T(8,128)(2,1)S(1)} %readback.2), channel_id=1, replica_groups={{256,288,320,352,384,416,448,480,0,32,64,96,128,160,192,224},{257,289,3..., dimensions={0} | all-to-all | bytes 131072 | tf_op jit(solution)/shard_map/all_to_all | solution.py:30
  61.5 6.2 %all-gather = f32[16,256]{1,0:T(8,128)S(1)} all-gather(f32[8,256]{1,0:T(8,128)S(1)} %convert_reduce_fusion.1), channel_id=2, replica_groups=mesh['z'=16,'c'=2,'y'=4,'x'=4] {'c'}, dimensions={0}, use_global_device_ids=true | all-gather | bytes 24576 | tf_op jit(solution)/shard_map/all_gather | solution.py:182
  67.7 15.5 %all_to_all.44.rows_ref = bf16[16,8,256]{2,1,0:T(8,128)(2,1)S(1)} all-to-all(bf16[16,8,256]{2,1,0:T(8,128)(2,1)S(1)} %broadcast_in_dim.2), channel_id=1, replica_groups={{256,288,320,352,384,416,448,480,0,32,64,96,128,160,192,224},{257,289,3..., dimensions={0} | all-to-all | bytes 131072 | tf_op jit(solution)/shard_map/all_to_all | solution.py:30
  83.2 0.2 project.3
  83.4 10.6 %all_to_all.45.parts_ref = bf16[16,8,1024]{2,1,0:T(8,128)(2,1)S(1)} all-to-all(bf16[16,8,1024]{2,1,0:T(8,128)(2,1)S(1)} %project.3), channel_id=1, replica_groups={{10,11,12,13,14,15,0,1,2,3,4,5,6,7,8,9},{26,27,28,29,30,31,16,17,18,19,..., dimensions={0} | all-to-all | bytes 524288 | tf_op jit(solution)/shard_map/all_to_all | solution.py:30
  94.0 0.4 step.3
  94.4 8.9 %all_to_all.46.gated_ref = bf16[16,8,256]{2,1,0:T(8,128)(2,1)S(1)} all-to-all(bf16[16,8,256]{2,1,0:T(8,128)(2,1)S(1)} %get-tuple-element.22), channel_id=1, replica_groups={{10,11,12,13,14,15,0,1,2,3,4,5,6,7,8,9},{26,27,28,29,30,31,16,17,18,19,..., dimensions={0} | all-to-all | bytes 131072 | tf_op jit(solution)/shard_map/all_to_all | solution.py:30
  103.3 0.8 readback.3
  104.1 11.5 %all-to-all-start.7 = ((bf16[16,8,256]{2,1,0:T(8,128)(2,1)}), bf16[16,8,256]{2,1,0:T(8,128)(2,1)S(1)}, u32[]{:S(2)}, u32[]{:S(2)}) async-start(bf16[16,8,256]{2,1,0:T(8,128)(2,1)} %readback.3), calls=%async_computation.7 | async-start | bytes 131072 | tf_op jit(solution)/shard_map/all_to_all | solution.py:30
  115.5 0.5 multiply_add_fusion.1
  116.0 1.2 pad_maximum_fusion
  117.3 1.4 %all-to-all-done.7 = bf16[16,8,256]{2,1,0:T(8,128)(2,1)S(1)} async-done(((bf16[16,8,256]{2,1,0:T(8,128)(2,1)}), bf16[16,8,256]{2,1,0:T(8,128)(2,1)S(1)}, u32[]{:S(2)}, u32[]{:S(2)}) %all-to-all-start.7) | async-done | bytes 65568 | tf_op jit(solution)/shard_map/all_to_all | solution.py:30
  118.7 6.4 %all-gather.1 = f32[16,256]{1,0:T(8,128)S(1)} all-gather(f32[8,256]{1,0:T(8,128)S(1)} %convert_reduce_fusion), channel_id=3, replica_groups=mesh['z'=16,'c'=2,'y'=4,'x'=4] {'c'}, dimensions={0}, use_global_device_ids=true | all-gather | bytes 24576 | tf_op jit(solution)/shard_map/all_gather | solution.py:182
  125.1 0.6 slice_select_fusion
  (7 shorter events, 0.1 us)
Async XLA Ops:
  9.1 17.1 %copy-start.2 = (bf16[2,256,256]{2,1,0:T(8,128)(2,1)S(1)}, bf16[2,256,256]{2,1,0:T(8,128)(2,1)}, u32[]{:S(2)}) copy-start(bf16[2,256,256]{2,1,0:T(8,128)(2,1)} %refs_3_.3) | copy-start | bytes 786436
  9.1 17.1 %copy-start.3 = (bf16[2,256,256]{2,1,0:T(8,128)(2,1)S(1)}, bf16[2,256,256]{2,1,0:T(8,128)(2,1)}, u32[]{:S(2)}) copy-start(bf16[2,256,256]{2,1,0:T(8,128)(2,1)} %refs_4_.3) | copy-start | bytes 786436
  9.1 17.1 %copy-start.4 = (bf16[2,256,128]{2,1,0:T(8,128)(2,1)S(1)}, bf16[2,256,128]{2,1,0:T(8,128)(2,1)}, u32[]{:S(2)}) copy-start(bf16[2,256,128]{2,1,0:T(8,128)(2,1)} %refs_0_.3) | copy-start | bytes 393220
  9.1 17.1 %copy-start.5 = (bf16[2,256,128]{2,1,0:T(8,128)(2,1)S(1)}, bf16[2,256,128]{2,1,0:T(8,128)(2,1)}, u32[]{:S(2)}) copy-start(bf16[2,256,128]{2,1,0:T(8,128)(2,1)} %refs_1_.3) | copy-start | bytes 393220
  9.2 17.1 %copy-start.6 = (bf16[2,256,128]{2,1,0:T(8,128)(2,1)S(1)}, bf16[2,256,128]{2,1,0:T(8,128)(2,1)}, u32[]{:S(2)}) copy-start(bf16[2,256,128]{2,1,0:T(8,128)(2,1)} %refs_2_.3) | copy-start | bytes 393220
  9.2 17.1 %copy-start.9 = (bf16[2,256]{1,0:T(2,128)(2,1)S(1)}, bf16[2,256]{1,0:T(2,128)(2,1)}, u32[]{:S(2)}) copy-start(bf16[2,256]{1,0:T(2,128)(2,1)} %gain_ref.3) | copy-start | bytes 3076
  9.2 28.5 %copy-start = (f32[2,6,128,256]{3,2,1,0:T(8,128)S(1)}, f32[2,6,128,256]{3,2,1,0:T(8,128)}, u32[]{:S(2)}) copy-start(f32[2,6,128,256]{3,2,1,0:T(8,128)} %state_ref.3) | copy-start | bytes 4718596
  9.2 28.4 %copy-start.7 = (f32[2,6,128]{2,0,1:T(2,128)S(1)}, f32[2,6,128]{2,0,1:T(2,128)}, u32[]{:S(2)}) copy-start(f32[2,6,128]{2,0,1:T(2,128)} %param.17) | copy-start | bytes 18436
  9.2 28.4 %copy-start.8 = (f32[2,128]{1,0:T(2,128)S(1)}, f32[2,128]{1,0:T(2,128)}, u32[]{:S(2)}) copy-start(f32[2,128]{1,0:T(2,128)} %shift_ref.3) | copy-start | bytes 3076
  26.2 20.7 %copy-start.1 = (bf16[2,256,256]{2,1,0:T(8,128)(2,1)S(1)}, bf16[2,256,256]{2,1,0:T(8,128)(2,1)}, u32[]{:S(2)}) copy-start(bf16[2,256,256]{2,1,0:T(8,128)(2,1)} %weight_ref.3) | copy-start | bytes 786436
  104.1 14.6 %all-to-all-start.7 = ((bf16[16,8,256]{2,1,0:T(8,128)(2,1)}), bf16[16,8,256]{2,1,0:T(8,128)(2,1)S(1)}, u32[]{:S(2)}, u32[]{:S(2)}) async-start(bf16[16,8,256]{2,1,0:T(8,128)(2,1)} %readback.3), calls=%async_computation.7 | async-start | bytes 131072 | tf_op jit(solution)/shard_map/all_to_all | solution.py:30

commit v5 on v4

--- a/solution.py
+++ b/solution.py
@@ -24,6 +24,8 @@
     "z": tuple((8 + k) % 16 for k in range(16)),
     DP: tuple((10 + k) % 16 for k in range(16)),
 }
+ORDER[TP] = tuple(2 * z + c for z in ORDER["z"] for c in (1, 0))
+HALF = PAD // 2
 
 
 def exchange(parts, axis):
@@ -66,14 +68,14 @@
 
 def spread_kernel(rows_ref, out_ref):
     rows = rows_ref[...].astype(F32)
-    rows = jnp.concatenate([rows, jnp.zeros((PAD - rows.shape[0], rows.shape[1]), F32)], axis=0)
+    rows = jnp.concatenate([rows, jnp.zeros((HALF - rows.shape[0], rows.shape[1]), F32)], axis=0)
     out_ref[...] = jnp.broadcast_to(rows[None], out_ref.shape).astype(BF)
 
 
 def spread(rows, n):
     return pl.pallas_call(
         spread_kernel,
-        out_shape=jax.ShapeDtypeStruct((n, PAD, rows.shape[1]), BF),
+        out_shape=jax.ShapeDtypeStruct((n, HALF, rows.shape[1]), BF),
         in_specs=[VMEM],
         out_specs=VMEM,
         compiler_params=SMALL,
@@ -84,13 +86,15 @@
 
 def step_kernel(b, seqs, kc, vc, parts_ref, shift_ref, fade_ref, state_ref, out_ref, d_ref, k_ref, v_ref):
     total = jnp.sum(parts_ref[...].astype(F32), axis=0)
+    third = seqs // 2
+    total = jnp.concatenate([total[HALF : HALF + third], total[:third]], axis=0)
     cols = 3 * kc + 2 * vc
     total = total * lax.rsqrt(total[:, cols : cols + 1] / D + 1e-06)
-    queries = total[:seqs, :kc] * DK ** (-0.5)
-    keys = total[:seqs, kc : 2 * kc]
-    pre = total[:seqs, 2 * kc : 3 * kc] + shift_ref[b : b + 1, :]
-    values = total[:seqs, 3 * kc : 3 * kc + vc]
-    gates = total[:seqs, 3 * kc + vc : cols]
+    queries = total[:, :kc] * DK ** (-0.5)
+    keys = total[:, kc : 2 * kc]
+    pre = total[:, 2 * kc : 3 * kc] + shift_ref[b : b + 1, :]
+    values = total[:, 3 * kc : 3 * kc + vc]
+    gates = total[:, 3 * kc + vc : cols]
     log_sigmoid = jnp.minimum(pre, 0.0) - jnp.log1p(jnp.exp(-jnp.abs(pre)))
     decay = jnp.exp(log_sigmoid / 16.0 + fade_ref[:, b, :])
     fresh_part = jnp.sum(queries * keys, axis=1, keepdims=True) * values
@@ -100,7 +104,8 @@
     ]
     readout = jnp.concatenate(old, axis=0) + fresh_part
     gated = readout * (gates / (1.0 + jnp.exp(-gates)))
-    gated = jnp.concatenate([gated, jnp.zeros((PAD - seqs, vc), F32)], axis=0)
+    blank = jnp.zeros((HALF - third, vc), F32)
+    gated = jnp.concatenate([gated[third:], blank, gated[:third], blank], axis=0)
     out_ref[...] = jnp.broadcast_to(gated[None], out_ref.shape).astype(BF)
     d_ref[...] = decay
     k_ref[...] = keys
@@ -158,34 +163,40 @@
 ):
     weights = (probe_lift, address_lift, forget_lift, content_lift, filter_lift)
     depth = lax.axis_size("z")
-    third = incoming_embeddings.shape[0]
-    stream, first_core = lax.optimization_barrier((incoming_embeddings, lax.axis_index("c") == 0))
-    stream = lax.all_gather(stream, "c", axis=0, tiled=True)
+    third, width = incoming_embeddings.shape
+    place = lax.rem(lax.axis_index("z") + depth - ORDER["z"][0], depth).astype(jnp.uint32)
+    stream, north, place = lax.optimization_barrier(
+        (incoming_embeddings, lax.axis_index("c") == 1, place)
+    )
     fade = jnp.transpose(surplus_fade, (1, 0, 2))
     kept = []
     for b in range(BLOCKS):
         if b == 0:
-            rows = exchange(spread(stream, depth), "z")
-            stream = jnp.pad(stream, ((0, PAD - stream.shape[0]), (0, 0)))
+            rows = exchange(spread(stream, 2 * depth), TP).reshape(depth, PAD, width)
+            old = lax.dynamic_index_in_dim(rows, place, 0, keepdims=False)
+            rows, old = lax.optimization_barrier((rows, old))
         else:
             rows = exchange(jnp.broadcast_to(stream[None], (depth, *stream.shape)), "z")
         parts = exchange(project(b, rows, rescale_factors, weights), DP)
         gated, *small = step(b, parts, forget_shift, fade, memory_tensor)
+        kept.append(small)
         gathered = exchange(gated, DP)
-        if b == BLOCKS - 1:
-            kept.append(small)
-            gathered, kept = lax.optimization_barrier((gathered, kept))
+        if b == 0:
+            heads = exchange(readback(b, gathered, readback_lift), "z")
+            own = jnp.sum(heads.astype(F32), axis=0)
+            both = lax.all_gather(own, "c", axis=0)
+            stream = (old.astype(F32) + (both[0] + both[1])).astype(BF)
+            rest = jnp.where(north, stream[:third], stream[HALF : HALF + third]).astype(F32)
+            stream, rest = lax.optimization_barrier((stream, rest))
         else:
-            kept.append(small)
-        heads = exchange(readback(b, gathered, readback_lift), "z")
-        own = jnp.sum(heads.astype(F32), axis=0)
-        both = lax.all_gather(own, "c", axis=0)
-        stream = (stream.astype(F32) + (both[0] + both[1])).astype(BF)
+            gathered, kept, rest = lax.optimization_barrier((gathered, kept, rest))
+            parts = readback(b, gathered, readback_lift).reshape(2 * depth, HALF, width)
+            branch = jnp.sum(exchange(parts, TP).astype(F32), axis=0)[:third]
+            mixed = (rest + branch).astype(BF)
     fresh = [
         memory_tensor[b] * d[:, :, None] + k[:, :, None] * v[:, None, :]
         for b, (d, k, v) in enumerate(kept)
     ]
-    mixed = jnp.where(first_core, stream[:third], stream[third : 2 * third])
     return mixed, jnp.stack(fresh)
 
 

time: 126 us -> 124 us (0.984)
  blocking collectives: 107 us -> 100 us
  starting transfers between devices: 11.5 us -> 15 us
  local copies, waits for them, and re-layouts: 0.08 us -> 1.41 us
    all_gather x1 -> x0, blocking collectives: 8.47 us -> none  [shards(): stream = lax.all_gather(stream, 'c', axis=0, tiled=True)]
    all_to_all x7, blocking collectives: 86.3 us -> 94.4 us  [exchange(): lax.all_to_all(parts, axis, 0, 0, tiled=True, axis_index_groups=[list(ORD...]
    all_gather x2 -> x1, blocking collectives: 12.6 us -> 5.7 us  [shards(): both = lax.all_gather(own, 'c', axis=0)]
    all_to_all x1, starting transfers between devices: 11.5 us -> 15 us  [exchange(): lax.all_to_all(parts, axis, 0, 0, tiled=True, axis_index_groups=[list(ORD...]
where the time goes in v5:
time: 124 us
  blocking collectives  100 us (81%)
  starting transfers between devices  15 us (12%)
  other arithmetic  2.43 us (2%)
  waiting for transfers between devices  2.3 us (2%)
  Pallas kernels  1.62 us (1%)
  local copies, waits for them, and re-layouts  1.41 us (1%)
    all_to_all x7, blocking collectives, exchange(): lax.all_to_all(parts, axis, 0, 0, tiled=True, axis_index_groups=[list(ORD...  94.4 us
    all_to_all x1, starting transfers between devices, exchange(): lax.all_to_all(parts, axis, 0, 0, tiled=True, axis_index_groups=[list(ORD...  15 us
    all_gather x1, blocking collectives, shards(): both = lax.all_gather(own, 'c', axis=0)  5.7 us
  transfers between devices with their start and end apart: 1, of which 1 were waited for; matrix products, arithmetic and copies ran while one was open for 1% of the time, Pallas kernels for 0%

profile of v5, /device:TPU:1, one launch (start us, length us, event | category | flops | bytes accessed | tf_op | source)
XLA Modules:
  0.0 123.7 jit_solution(11103954173143184531)
XLA Ops:
  0.6 0.0 copy-start.10
  0.6 0.7 copy-done.10
  1.3 0.0 copy-start.2
  1.3 0.0 copy-start.3
  1.3 0.0 copy-start.4
  1.3 0.0 copy-start.5
  1.3 0.0 copy-start.6
  1.3 0.0 copy-start.9
  1.4 0.0 copy-start
  1.4 0.0 copy-start.7
  1.4 0.0 copy-start.8
  1.4 23.8 %all_to_all.40 = bf16[32,4,256]{2,1,0:T(4,128)(2,1)S(1)} all-to-all(bf16[32,4,256]{2,1,0:T(4,128)(2,1)S(1)} %spread.1), channel_id=1, replica_groups={{272,256,304,288,336,320,368,352,400,384,432,416,464,448,496,480,16,0,4..., dimensions={0} | all-to-all | bytes 131072 | tf_op jit(solution)/shard_map/all_to_all | solution.py:32
  25.3 0.0 copy-done.2
  25.3 0.0 copy-done.3
  25.3 0.0 copy-done.4
  25.3 0.0 copy-done.5
  25.3 0.0 copy-done.6
  25.3 0.0 copy-done.9
  25.3 0.0 copy-start.1
  25.3 0.2 project.2
  25.6 11.1 %all_to_all.41.parts_ref = bf16[16,8,1024]{2,1,0:T(8,128)(2,1)S(1)} all-to-all(bf16[16,8,1024]{2,1,0:T(8,128)(2,1)S(1)} %project.2), channel_id=1, replica_groups={{10,11,12,13,14,15,0,1,2,3,4,5,6,7,8,9},{26,27,28,29,30,31,16,17,18,19,..., dimensions={0} | all-to-all | bytes 524288 | tf_op jit(solution)/shard_map/all_to_all | solution.py:32
  36.7 0.0 copy-done
  36.7 0.0 copy-done.7
  36.7 0.0 copy-done.8
  36.7 0.4 step.2
  37.1 8.8 %all_to_all.42.gated_ref = bf16[16,8,256]{2,1,0:T(8,128)(2,1)S(1)} all-to-all(bf16[16,8,256]{2,1,0:T(8,128)(2,1)S(1)} %get-tuple-element.29), channel_id=1, replica_groups={{10,11,12,13,14,15,0,1,2,3,4,5,6,7,8,9},{26,27,28,29,30,31,16,17,18,19,..., dimensions={0} | all-to-all | bytes 131072 | tf_op jit(solution)/shard_map/all_to_all | solution.py:32
  45.9 0.0 copy-done.1
  45.9 0.2 readback.2
  46.1 15.7 %all_to_all.43 = bf16[16,8,256]{2,1,0:T(8,128)(2,1)S(1)} all-to-all(bf16[16,8,256]{2,1,0:T(8,128)(2,1)S(1)} %readback.2), channel_id=1, replica_groups={{256,288,320,352,384,416,448,480,0,32,64,96,128,160,192,224},{257,289,3..., dimensions={0} | all-to-all | bytes 131072 | tf_op jit(solution)/shard_map/all_to_all | solution.py:32
  61.8 5.7 %all-gather = f32[16,256]{1,0:T(8,128)S(1)} all-gather(f32[8,256]{1,0:T(8,128)S(1)} %convert_reduce_fusion.1), channel_id=2, replica_groups=mesh['z'=16,'c'=2,'y'=4,'x'=4] {'c'}, dimensions={0}, use_global_device_ids=true | all-gather | bytes 24576 | tf_op jit(solution)/shard_map/all_gather | solution.py:187
  67.5 15.5 %all_to_all.44.rows_ref = bf16[16,8,256]{2,1,0:T(8,128)(2,1)S(1)} all-to-all(bf16[16,8,256]{2,1,0:T(8,128)(2,1)S(1)} %broadcast_in_dim.2), channel_id=1, replica_groups={{256,288,320,352,384,416,448,480,0,32,64,96,128,160,192,224},{257,289,3..., dimensions={0} | all-to-all | bytes 131072 | tf_op jit(solution)/shard_map/all_to_all | solution.py:32
  83.0 0.2 project.3
  83.2 10.7 %all_to_all.45.parts_ref = bf16[16,8,1024]{2,1,0:T(8,128)(2,1)S(1)} all-to-all(bf16[16,8,1024]{2,1,0:T(8,128)(2,1)S(1)} %project.3), channel_id=1, replica_groups={{10,11,12,13,14,15,0,1,2,3,4,5,6,7,8,9},{26,27,28,29,30,31,16,17,18,19,..., dimensions={0} | all-to-all | bytes 524288 | tf_op jit(solution)/shard_map/all_to_all | solution.py:32
  93.9 0.4 step.3
  94.3 8.9 %all_to_all.46.gated_ref = bf16[16,8,256]{2,1,0:T(8,128)(2,1)S(1)} all-to-all(bf16[16,8,256]{2,1,0:T(8,128)(2,1)S(1)} %get-tuple-element.32), channel_id=1, replica_groups={{10,11,12,13,14,15,0,1,2,3,4,5,6,7,8,9},{26,27,28,29,30,31,16,17,18,19,..., dimensions={0} | all-to-all | bytes 131072 | tf_op jit(solution)/shard_map/all_to_all | solution.py:32
  103.2 0.2 readback.3
  103.3 0.7 reshape.25
  104.0 15.0 %all-to-all-start.7 = ((bf16[32,4,256]{2,1,0:T(4,128)(2,1)}), bf16[32,4,256]{2,1,0:T(4,128)(2,1)S(1)}, u32[]{:S(2)}, u32[]{:S(2)}) async-start(bf16[32,4,256]{2,1,0:T(4,128)(2,1)} %reshape.25), calls=%async_computation.7 | async-start | bytes 131072 | tf_op jit(solution)/shard_map/all_to_all | solution.py:32
  119.0 0.5 multiply_add_fusion.1
  119.5 1.3 %pad_maximum_fusion = f32[2,6,128,256]{3,2,1,0:T(8,128)} fusion(f32[1,6,128,256]{3,2,1,0:T(8,128)S(1)} %get-tuple-element.49, f32[1,6,128,256]{3,2,1,0:T(8,128)S(1)} %get-tuple-element.48), kind=kLoop, calls=%fused_computation | loop fusion | flops 393216 | bytes 3145728 | tf_op jit(solution)/shard_map/stack | solution.py:200
  120.8 2.3 %all-to-all-done.7 = bf16[32,4,256]{2,1,0:T(4,128)(2,1)S(1)} async-done(((bf16[32,4,256]{2,1,0:T(4,128)(2,1)}), bf16[32,4,256]{2,1,0:T(4,128)(2,1)S(1)}, u32[]{:S(2)}, u32[]{:S(2)}) %all-to-all-start.7) | async-done | bytes 65568 | tf_op jit(solution)/shard_map/all_to_all | solution.py:32
  123.1 0.1 convert_reduce_fusion
  123.1 0.6 fusion.2
  (7 shorter events, 0.1 us)
Async XLA Ops:
  0.6 0.7 copy-start.10
  1.3 24.0 %copy-start.2 = (bf16[2,256,256]{2,1,0:T(8,128)(2,1)S(1)}, bf16[2,256,256]{2,1,0:T(8,128)(2,1)}, u32[]{:S(2)}) copy-start(bf16[2,256,256]{2,1,0:T(8,128)(2,1)} %refs_3_.3) | copy-start | bytes 786436
  1.3 24.0 %copy-start.3 = (bf16[2,256,256]{2,1,0:T(8,128)(2,1)S(1)}, bf16[2,256,256]{2,1,0:T(8,128)(2,1)}, u32[]{:S(2)}) copy-start(bf16[2,256,256]{2,1,0:T(8,128)(2,1)} %refs_4_.3) | copy-start | bytes 786436
  1.3 24.0 %copy-start.4 = (bf16[2,256,128]{2,1,0:T(8,128)(2,1)S(1)}, bf16[2,256,128]{2,1,0:T(8,128)(2,1)}, u32[]{:S(2)}) copy-start(bf16[2,256,128]{2,1,0:T(8,128)(2,1)} %refs_0_.3) | copy-start | bytes 393220
  1.3 24.0 %copy-start.5 = (bf16[2,256,128]{2,1,0:T(8,128)(2,1)S(1)}, bf16[2,256,128]{2,1,0:T(8,128)(2,1)}, u32[]{:S(2)}) copy-start(bf16[2,256,128]{2,1,0:T(8,128)(2,1)} %refs_1_.3) | copy-start | bytes 393220
  1.3 24.0 %copy-start.6 = (bf16[2,256,128]{2,1,0:T(8,128)(2,1)S(1)}, bf16[2,256,128]{2,1,0:T(8,128)(2,1)}, u32[]{:S(2)}) copy-start(bf16[2,256,128]{2,1,0:T(8,128)(2,1)} %refs_2_.3) | copy-start | bytes 393220
  1.3 24.0 %copy-start.9 = (bf16[2,256]{1,0:T(2,128)(2,1)S(1)}, bf16[2,256]{1,0:T(2,128)(2,1)}, u32[]{:S(2)}) copy-start(bf16[2,256]{1,0:T(2,128)(2,1)} %gain_ref.3) | copy-start | bytes 3076
  1.4 35.3 %copy-start = (f32[2,6,128,256]{3,2,1,0:T(8,128)S(1)}, f32[2,6,128,256]{3,2,1,0:T(8,128)}, u32[]{:S(2)}) copy-start(f32[2,6,128,256]{3,2,1,0:T(8,128)} %state_ref.3) | copy-start | bytes 4718596
  1.4 35.3 %copy-start.7 = (f32[2,6,128]{2,0,1:T(2,128)S(1)}, f32[2,6,128]{2,0,1:T(2,128)}, u32[]{:S(2)}) copy-start(f32[2,6,128]{2,0,1:T(2,128)} %param.17) | copy-start | bytes 18436
  1.4 35.3 %copy-start.8 = (f32[2,128]{1,0:T(2,128)S(1)}, f32[2,128]{1,0:T(2,128)}, u32[]{:S(2)}) copy-start(f32[2,128]{1,0:T(2,128)} %shift_ref.3) | copy-start | bytes 3076
  25.3 20.6 %copy-start.1 = (bf16[2,256,256]{2,1,0:T(8,128)(2,1)S(1)}, bf16[2,256,256]{2,1,0:T(8,128)(2,1)}, u32[]{:S(2)}) copy-start(bf16[2,256,256]{2,1,0:T(8,128)(2,1)} %weight_ref.3) | copy-start | bytes 786436
  104.0 19.1 %all-to-all-start.7 = ((bf16[32,4,256]{2,1,0:T(4,128)(2,1)}), bf16[32,4,256]{2,1,0:T(4,128)(2,1)S(1)}, u32[]{:S(2)}, u32[]{:S(2)}) async-start(bf16[32,4,256]{2,1,0:T(4,128)(2,1)} %reshape.25), calls=%async_computation.7 | async-start | bytes 131072 | tf_op jit(solution)/shard_map/all_to_all | solution.py:32

commit v6 on v5

--- a/solution.py
+++ b/solution.py
@@ -164,40 +164,31 @@
     weights = (probe_lift, address_lift, forget_lift, content_lift, filter_lift)
     depth = lax.axis_size("z")
     third, width = incoming_embeddings.shape
-    place = lax.rem(lax.axis_index("z") + depth - ORDER["z"][0], depth).astype(jnp.uint32)
-    stream, north, place = lax.optimization_barrier(
-        (incoming_embeddings, lax.axis_index("c") == 1, place)
-    )
     fade = jnp.transpose(surplus_fade, (1, 0, 2))
+    stream = incoming_embeddings
     kept = []
     for b in range(BLOCKS):
         if b == 0:
-            rows = exchange(spread(stream, 2 * depth), TP).reshape(depth, PAD, width)
-            old = lax.dynamic_index_in_dim(rows, place, 0, keepdims=False)
-            rows, old = lax.optimization_barrier((rows, old))
+            copies = spread(stream, 2 * depth)
         else:
-            rows = exchange(jnp.broadcast_to(stream[None], (depth, *stream.shape)), "z")
+            copies = jnp.broadcast_to(
+                jnp.pad(stream, ((0, HALF - third), (0, 0)))[None], (2 * depth, HALF, width)
+            )
+        rows = exchange(copies, TP).reshape(depth, PAD, width)
         parts = exchange(project(b, rows, rescale_factors, weights), DP)
         gated, *small = step(b, parts, forget_shift, fade, memory_tensor)
         kept.append(small)
         gathered = exchange(gated, DP)
-        if b == 0:
-            heads = exchange(readback(b, gathered, readback_lift), "z")
-            own = jnp.sum(heads.astype(F32), axis=0)
-            both = lax.all_gather(own, "c", axis=0)
-            stream = (old.astype(F32) + (both[0] + both[1])).astype(BF)
-            rest = jnp.where(north, stream[:third], stream[HALF : HALF + third]).astype(F32)
-            stream, rest = lax.optimization_barrier((stream, rest))
-        else:
-            gathered, kept, rest = lax.optimization_barrier((gathered, kept, rest))
-            parts = readback(b, gathered, readback_lift).reshape(2 * depth, HALF, width)
-            branch = jnp.sum(exchange(parts, TP).astype(F32), axis=0)[:third]
-            mixed = (rest + branch).astype(BF)
+        if b == BLOCKS - 1:
+            gathered, kept = lax.optimization_barrier((gathered, kept))
+        heads = readback(b, gathered, readback_lift).reshape(2 * depth, HALF, width)
+        branch = jnp.sum(exchange(heads, TP).astype(F32), axis=0)[:third]
+        stream = (stream.astype(F32) + branch).astype(BF)
     fresh = [
         memory_tensor[b] * d[:, :, None] + k[:, :, None] * v[:, None, :]
         for b, (d, k, v) in enumerate(kept)
     ]
-    return mixed, jnp.stack(fresh)
+    return stream, jnp.stack(fresh)
 
 
 def solution(mesh):

time: 124 us -> 123 us (level)
  blocking collectives: 100 us -> 98.3 us
    all_gather x1 -> x0, blocking collectives: 5.7 us -> none  [shards(): both = lax.all_gather(own, 'c', axis=0)]
    all_to_all x7, blocking collectives: 94.4 us -> 98.3 us  [exchange(): lax.all_to_all(parts, axis, 0, 0, tiled=True, axis_index_groups=[list(ORD...]
where the time goes in v6:
time: 123 us; the launch traced here: 122 us
  blocking collectives  98.3 us (80%)
  starting transfers between devices  15.3 us (12%)
  other arithmetic  2.42 us (2%)
  waiting for transfers between devices  2.34 us (2%)
  Pallas kernels  1.61 us (1%)
  local copies, waits for them, and re-layouts  1.54 us (1%)
    all_to_all x7, blocking collectives, exchange(): lax.all_to_all(parts, axis, 0, 0, tiled=True, axis_index_groups=[list(ORD...  98.3 us
    all_to_all x1, starting transfers between devices, exchange(): lax.all_to_all(parts, axis, 0, 0, tiled=True, axis_index_groups=[list(ORD...  15.3 us
  transfers between devices with their start and end apart: 1, of which 1 were waited for; matrix products, arithmetic and copies ran while one was open for 1% of the time, Pallas kernels for 0%

profile of v6, /device:TPU:1, one launch (start us, length us, event | category | flops | bytes accessed | tf_op | source)
XLA Modules:
  0.0 122.4 jit_solution(16348475171507515005)
XLA Ops:
  0.6 0.0 copy-start.3
  0.6 0.0 copy-start.2
  0.7 0.0 copy-start.6
  0.7 0.0 copy-start.5
  0.7 0.0 copy-start.4
  0.7 0.0 copy-start.9
  0.7 0.0 copy-start.10
  0.7 0.7 copy-done.10
  1.5 0.0 copy-start
  1.5 0.0 copy-start.7
  1.5 0.0 copy-start.8
  1.5 23.8 %all_to_all.40 = bf16[32,4,256]{2,1,0:T(4,128)(2,1)S(1)} all-to-all(bf16[32,4,256]{2,1,0:T(4,128)(2,1)S(1)} %spread.1), channel_id=1, replica_groups={{272,256,304,288,336,320,368,352,400,384,432,416,464,448,496,480,16,0,4..., dimensions={0} | all-to-all | bytes 131072 | tf_op jit(solution)/shard_map/all_to_all | solution.py:32
  25.3 0.0 copy-done.3
  25.4 0.0 copy-done.2
  25.4 0.0 copy-done.6
  25.4 0.0 copy-done.5
  25.4 0.0 copy-done.4
  25.4 0.0 copy-done.9
  25.4 0.0 copy-start.1
  25.4 0.2 project.2
  25.7 0.0 copy-start.11
  25.7 11.1 %all_to_all.41.parts_ref = bf16[16,8,1024]{2,1,0:T(8,128)(2,1)S(1)} all-to-all(bf16[16,8,1024]{2,1,0:T(8,128)(2,1)S(1)} %project.2), channel_id=1, replica_groups={{10,11,12,13,14,15,0,1,2,3,4,5,6,7,8,9},{26,27,28,29,30,31,16,17,18,19,..., dimensions={0} | all-to-all | bytes 524288 | tf_op jit(solution)/shard_map/all_to_all | solution.py:32
  36.8 0.0 copy-done
  36.8 0.0 copy-done.7
  36.8 0.0 copy-done.8
  36.8 0.4 step.2
  37.2 8.8 %all_to_all.42.gated_ref = bf16[16,8,256]{2,1,0:T(8,128)(2,1)S(1)} all-to-all(bf16[16,8,256]{2,1,0:T(8,128)(2,1)S(1)} %get-tuple-element.17), channel_id=1, replica_groups={{10,11,12,13,14,15,0,1,2,3,4,5,6,7,8,9},{26,27,28,29,30,31,16,17,18,19,..., dimensions={0} | all-to-all | bytes 131072 | tf_op jit(solution)/shard_map/all_to_all | solution.py:32
  46.0 0.0 copy-done.1
  46.0 0.2 readback.2
  46.2 19.2 %all_to_all.43 = bf16[32,4,256]{2,1,0:T(4,128)(2,1)S(1)} all-to-all(bf16[32,4,256]{2,1,0:T(4,128)(2,1)S(1)} %reshape.30), channel_id=1, replica_groups={{272,256,304,288,336,320,368,352,400,384,432,416,464,448,496,480,16,0,4..., dimensions={0} | all-to-all | bytes 131072 | tf_op jit(solution)/shard_map/all_to_all | solution.py:32
  65.3 0.1 convert_reduce_fusion.1
  65.4 0.0 copy-done.11
  65.5 16.1 %all_to_all.44 = bf16[32,4,256]{2,1,0:T(4,128)(2,1)S(1)} all-to-all(bf16[32,4,256]{2,1,0:T(4,128)(2,1)S(1)} %broadcast_in_dim.2), channel_id=1, replica_groups={{272,256,304,288,336,320,368,352,400,384,432,416,464,448,496,480,16,0,4..., dimensions={0} | all-to-all | bytes 131072 | tf_op jit(solution)/shard_map/all_to_all | solution.py:32
  81.6 0.2 project.3
  81.8 10.5 %all_to_all.45.parts_ref = bf16[16,8,1024]{2,1,0:T(8,128)(2,1)S(1)} all-to-all(bf16[16,8,1024]{2,1,0:T(8,128)(2,1)S(1)} %project.3), channel_id=1, replica_groups={{10,11,12,13,14,15,0,1,2,3,4,5,6,7,8,9},{26,27,28,29,30,31,16,17,18,19,..., dimensions={0} | all-to-all | bytes 524288 | tf_op jit(solution)/shard_map/all_to_all | solution.py:32
  92.4 0.4 step.3
  92.8 8.8 %all_to_all.46.gated_ref = bf16[16,8,256]{2,1,0:T(8,128)(2,1)S(1)} all-to-all(bf16[16,8,256]{2,1,0:T(8,128)(2,1)S(1)} %get-tuple-element.18), channel_id=1, replica_groups={{10,11,12,13,14,15,0,1,2,3,4,5,6,7,8,9},{26,27,28,29,30,31,16,17,18,19,..., dimensions={0} | all-to-all | bytes 131072 | tf_op jit(solution)/shard_map/all_to_all | solution.py:32
  101.6 0.2 readback.3
  101.7 0.6 reshape.32
  102.4 15.3 %all-to-all-start.7 = ((bf16[32,4,256]{2,1,0:T(4,128)(2,1)}), bf16[32,4,256]{2,1,0:T(4,128)(2,1)S(1)}, u32[]{:S(2)}, u32[]{:S(2)}) async-start(bf16[32,4,256]{2,1,0:T(4,128)(2,1)} %reshape.32), calls=%async_computation.7 | async-start | bytes 131072 | tf_op jit(solution)/shard_map/all_to_all | solution.py:32
  117.7 0.5 multiply_add_fusion.1
  118.2 1.2 %pad_maximum_fusion = f32[2,6,128,256]{3,2,1,0:T(8,128)} fusion(f32[1,6,128,256]{3,2,1,0:T(8,128)S(1)} %get-tuple-element.33, f32[1,6,128,256]{3,2,1,0:T(8,128)S(1)} %get-tuple-element.32), kind=kLoop, calls=%fused_computation | loop fusion | flops 393216 | bytes 3145728 | tf_op jit(solution)/shard_map/stack | solution.py:191
  119.4 2.3 %all-to-all-done.7 = bf16[32,4,256]{2,1,0:T(4,128)(2,1)S(1)} async-done(((bf16[32,4,256]{2,1,0:T(4,128)(2,1)}), bf16[32,4,256]{2,1,0:T(4,128)(2,1)S(1)}, u32[]{:S(2)}, u32[]{:S(2)}) %all-to-all-start.7) | async-done | bytes 65568 | tf_op jit(solution)/shard_map/all_to_all | solution.py:32
  121.7 0.1 convert_reduce_fusion
  121.8 0.6 fusion
  (7 shorter events, 0.1 us)
Async XLA Ops:
  0.6 24.7 %copy-start.3 = (bf16[2,256,256]{2,1,0:T(8,128)(2,1)S(1)}, bf16[2,256,256]{2,1,0:T(8,128)(2,1)}, u32[]{:S(2)}) copy-start(bf16[2,256,256]{2,1,0:T(8,128)(2,1)} %refs_4_.3) | copy-start | bytes 786436
  0.6 24.7 %copy-start.2 = (bf16[2,256,256]{2,1,0:T(8,128)(2,1)S(1)}, bf16[2,256,256]{2,1,0:T(8,128)(2,1)}, u32[]{:S(2)}) copy-start(bf16[2,256,256]{2,1,0:T(8,128)(2,1)} %refs_3_.3) | copy-start | bytes 786436
  0.7 24.7 %copy-start.6 = (bf16[2,256,128]{2,1,0:T(8,128)(2,1)S(1)}, bf16[2,256,128]{2,1,0:T(8,128)(2,1)}, u32[]{:S(2)}) copy-start(bf16[2,256,128]{2,1,0:T(8,128)(2,1)} %refs_2_.3) | copy-start | bytes 393220
  0.7 24.7 %copy-start.5 = (bf16[2,256,128]{2,1,0:T(8,128)(2,1)S(1)}, bf16[2,256,128]{2,1,0:T(8,128)(2,1)}, u32[]{:S(2)}) copy-start(bf16[2,256,128]{2,1,0:T(8,128)(2,1)} %refs_1_.3) | copy-start | bytes 393220
  0.7 24.7 %copy-start.4 = (bf16[2,256,128]{2,1,0:T(8,128)(2,1)S(1)}, bf16[2,256,128]{2,1,0:T(8,128)(2,1)}, u32[]{:S(2)}) copy-start(bf16[2,256,128]{2,1,0:T(8,128)(2,1)} %refs_0_.3) | copy-start | bytes 393220
  0.7 24.7 %copy-start.9 = (bf16[2,256]{1,0:T(2,128)(2,1)S(1)}, bf16[2,256]{1,0:T(2,128)(2,1)}, u32[]{:S(2)}) copy-start(bf16[2,256]{1,0:T(2,128)(2,1)} %gain_ref.3) | copy-start | bytes 3076
  0.7 0.8 copy-start.10
  1.5 35.3 %copy-start = (f32[2,6,128,256]{3,2,1,0:T(8,128)S(1)}, f32[2,6,128,256]{3,2,1,0:T(8,128)}, u32[]{:S(2)}) copy-start(f32[2,6,128,256]{3,2,1,0:T(8,128)} %state_ref.3) | copy-start | bytes 4718596
  1.5 35.3 %copy-start.7 = (f32[2,6,128]{2,0,1:T(2,128)S(1)}, f32[2,6,128]{2,0,1:T(2,128)}, u32[]{:S(2)}) copy-start(f32[2,6,128]{2,0,1:T(2,128)} %param.17) | copy-start | bytes 18436
  1.5 35.3 %copy-start.8 = (f32[2,128]{1,0:T(2,128)S(1)}, f32[2,128]{1,0:T(2,128)}, u32[]{:S(2)}) copy-start(f32[2,128]{1,0:T(2,128)} %shift_ref.3) | copy-start | bytes 3076
  25.4 20.6 %copy-start.1 = (bf16[2,256,256]{2,1,0:T(8,128)(2,1)S(1)}, bf16[2,256,256]{2,1,0:T(8,128)(2,1)}, u32[]{:S(2)}) copy-start(bf16[2,256,256]{2,1,0:T(8,128)(2,1)} %weight_ref.3) | copy-start | bytes 786436
  25.7 39.7 %copy-start.11 = (bf16[3,256]{1,0:T(4,128)(2,1)S(1)}, bf16[3,256]{1,0:T(4,128)(2,1)}, u32[]{:S(2)}) copy-start(bf16[3,256]{1,0:T(4,128)(2,1)} %rows_ref.1) | copy-start | bytes 4612
  102.4 19.4 %all-to-all-start.7 = ((bf16[32,4,256]{2,1,0:T(4,128)(2,1)}), bf16[32,4,256]{2,1,0:T(4,128)(2,1)S(1)}, u32[]{:S(2)}, u32[]{:S(2)}) async-start(bf16[32,4,256]{2,1,0:T(4,128)(2,1)} %reshape.32), calls=%async_computation.7 | async-start | bytes 131072 | tf_op jit(solution)/shard_map/all_to_all | solution.py:32

commit v7 on v6

--- a/solution.py
+++ b/solution.py
@@ -21,8 +21,8 @@
 
 
 ORDER = {
-    "z": tuple((8 + k) % 16 for k in range(16)),
-    DP: tuple((10 + k) % 16 for k in range(16)),
+    "z": (8, 0, 9, 1, 10, 2, 11, 3, 12, 4, 13, 5, 14, 6, 15, 7),
+    DP: (10, 0, 11, 1, 8, 2, 9, 3, 14, 4, 15, 5, 12, 6, 13, 7),
 }
 ORDER[TP] = tuple(2 * z + c for z in ORDER["z"] for c in (1, 0))
 HALF = PAD // 2

time: 123 us -> 123 us (level)
  no operation moved by 1% of the time
where the time goes in v7:
time: 123 us
  blocking collectives  99.4 us (81%)
  starting transfers between devices  14.4 us (12%)
  waiting for transfers between devices  2.46 us (2%)
  other arithmetic  2.42 us (2%)
  Pallas kernels  1.61 us (1%)
  local copies, waits for them, and re-layouts  1.54 us (1%)
    all_to_all x7, blocking collectives, exchange(): lax.all_to_all(parts, axis, 0, 0, tiled=True, axis_index_groups=[list(ORD...  99.4 us
    all_to_all x1, starting transfers between devices, exchange(): lax.all_to_all(parts, axis, 0, 0, tiled=True, axis_index_groups=[list(ORD...  14.4 us
    all_to_all x1, waiting for transfers between devices, exchange(): lax.all_to_all(parts, axis, 0, 0, tiled=True, axis_index_groups=[list(ORD...  2.46 us
  transfers between devices with their start and end apart: 1, of which 1 were waited for; matrix products, arithmetic and copies ran while one was open for 1% of the time, Pallas kernels for 0%

profile of v7, /device:TPU:1, one launch (start us, length us, event | category | flops | bytes accessed | tf_op | source)
XLA Modules:
  0.0 122.7 jit_solution(8049732201292828453)
XLA Ops:
  0.6 0.0 copy-start.3
  0.6 0.0 copy-start.2
  0.7 0.0 copy-start.6
  0.7 0.0 copy-start.5
  0.7 0.0 copy-start.4
  0.7 0.0 copy-start.9
  0.7 0.0 copy-start.10
  0.7 0.7 copy-done.10
  1.5 0.0 copy-start
  1.5 0.0 copy-start.7
  1.5 0.0 copy-start.8
  1.5 23.9 %all_to_all.40 = bf16[32,4,256]{2,1,0:T(4,128)(2,1)S(1)} all-to-all(bf16[32,4,256]{2,1,0:T(4,128)(2,1)S(1)} %spread.1), channel_id=1, replica_groups={{272,256,16,0,304,288,48,32,336,320,80,64,368,352,112,96,400,384,144,12..., dimensions={0} | all-to-all | bytes 131072 | tf_op jit(solution)/shard_map/all_to_all | solution.py:32
  25.4 0.0 copy-done.3
  25.4 0.0 copy-done.2
  25.5 0.0 copy-done.6
  25.5 0.0 copy-done.5
  25.5 0.0 copy-done.4
  25.5 0.0 copy-done.9
  25.5 0.0 copy-start.1
  25.5 0.2 project.2
  25.8 0.0 copy-start.11
  25.8 11.8 %all_to_all.41.parts_ref = bf16[16,8,1024]{2,1,0:T(8,128)(2,1)S(1)} all-to-all(bf16[16,8,1024]{2,1,0:T(8,128)(2,1)S(1)} %project.2), channel_id=1, replica_groups={{10,0,11,1,8,2,9,3,14,4,15,5,12,6,13,7},{26,16,27,17,24,18,25,19,30,20,..., dimensions={0} | all-to-all | bytes 524288 | tf_op jit(solution)/shard_map/all_to_all | solution.py:32
  37.6 0.0 copy-done
  37.6 0.0 copy-done.7
  37.6 0.0 copy-done.8
  37.6 0.4 step.2
  38.0 9.0 %all_to_all.42.gated_ref = bf16[16,8,256]{2,1,0:T(8,128)(2,1)S(1)} all-to-all(bf16[16,8,256]{2,1,0:T(8,128)(2,1)S(1)} %get-tuple-element.17), channel_id=1, replica_groups={{10,0,11,1,8,2,9,3,14,4,15,5,12,6,13,7},{26,16,27,17,24,18,25,19,30,20,..., dimensions={0} | all-to-all | bytes 131072 | tf_op jit(solution)/shard_map/all_to_all | solution.py:32
  47.0 0.0 copy-done.1
  47.0 0.2 readback.2
  47.2 18.4 %all_to_all.43 = bf16[32,4,256]{2,1,0:T(4,128)(2,1)S(1)} all-to-all(bf16[32,4,256]{2,1,0:T(4,128)(2,1)S(1)} %reshape.30), channel_id=1, replica_groups={{272,256,16,0,304,288,48,32,336,320,80,64,368,352,112,96,400,384,144,12..., dimensions={0} | all-to-all | bytes 131072 | tf_op jit(solution)/shard_map/all_to_all | solution.py:32
  65.5 0.1 convert_reduce_fusion.1
  65.6 0.0 copy-done.11
  65.6 16.1 %all_to_all.44 = bf16[32,4,256]{2,1,0:T(4,128)(2,1)S(1)} all-to-all(bf16[32,4,256]{2,1,0:T(4,128)(2,1)S(1)} %broadcast_in_dim.2), channel_id=1, replica_groups={{272,256,16,0,304,288,48,32,336,320,80,64,368,352,112,96,400,384,144,12..., dimensions={0} | all-to-all | bytes 131072 | tf_op jit(solution)/shard_map/all_to_all | solution.py:32
  81.8 0.2 project.3
  82.0 11.3 %all_to_all.45.parts_ref = bf16[16,8,1024]{2,1,0:T(8,128)(2,1)S(1)} all-to-all(bf16[16,8,1024]{2,1,0:T(8,128)(2,1)S(1)} %project.3), channel_id=1, replica_groups={{10,0,11,1,8,2,9,3,14,4,15,5,12,6,13,7},{26,16,27,17,24,18,25,19,30,20,..., dimensions={0} | all-to-all | bytes 524288 | tf_op jit(solution)/shard_map/all_to_all | solution.py:32
  93.3 0.4 step.3
  93.7 9.0 %all_to_all.46.gated_ref = bf16[16,8,256]{2,1,0:T(8,128)(2,1)S(1)} all-to-all(bf16[16,8,256]{2,1,0:T(8,128)(2,1)S(1)} %get-tuple-element.18), channel_id=1, replica_groups={{10,0,11,1,8,2,9,3,14,4,15,5,12,6,13,7},{26,16,27,17,24,18,25,19,30,20,..., dimensions={0} | all-to-all | bytes 131072 | tf_op jit(solution)/shard_map/all_to_all | solution.py:32
  102.7 0.2 readback.3
  102.9 0.6 reshape.32
  103.5 14.4 %all-to-all-start.7 = ((bf16[32,4,256]{2,1,0:T(4,128)(2,1)}), bf16[32,4,256]{2,1,0:T(4,128)(2,1)S(1)}, u32[]{:S(2)}, u32[]{:S(2)}) async-start(bf16[32,4,256]{2,1,0:T(4,128)(2,1)} %reshape.32), calls=%async_computation.7 | async-start | bytes 131072 | tf_op jit(solution)/shard_map/all_to_all | solution.py:32
  117.9 0.5 multiply_add_fusion.1
  118.4 1.2 %pad_maximum_fusion = f32[2,6,128,256]{3,2,1,0:T(8,128)} fusion(f32[1,6,128,256]{3,2,1,0:T(8,128)S(1)} %get-tuple-element.33, f32[1,6,128,256]{3,2,1,0:T(8,128)S(1)} %get-tuple-element.32), kind=kLoop, calls=%fused_computation | loop fusion | flops 393216 | bytes 3145728 | tf_op jit(solution)/shard_map/stack | solution.py:191
  119.6 2.5 %all-to-all-done.7 = bf16[32,4,256]{2,1,0:T(4,128)(2,1)S(1)} async-done(((bf16[32,4,256]{2,1,0:T(4,128)(2,1)}), bf16[32,4,256]{2,1,0:T(4,128)(2,1)S(1)}, u32[]{:S(2)}, u32[]{:S(2)}) %all-to-all-start.7) | async-done | bytes 65568 | tf_op jit(solution)/shard_map/all_to_all | solution.py:32
  122.1 0.1 convert_reduce_fusion
  122.2 0.6 fusion
  (7 shorter events, 0.1 us)
Async XLA Ops:
  0.6 24.8 %copy-start.3 = (bf16[2,256,256]{2,1,0:T(8,128)(2,1)S(1)}, bf16[2,256,256]{2,1,0:T(8,128)(2,1)}, u32[]{:S(2)}) copy-start(bf16[2,256,256]{2,1,0:T(8,128)(2,1)} %refs_4_.3) | copy-start | bytes 786436
  0.6 24.8 %copy-start.2 = (bf16[2,256,256]{2,1,0:T(8,128)(2,1)S(1)}, bf16[2,256,256]{2,1,0:T(8,128)(2,1)}, u32[]{:S(2)}) copy-start(bf16[2,256,256]{2,1,0:T(8,128)(2,1)} %refs_3_.3) | copy-start | bytes 786436
  0.7 24.8 %copy-start.6 = (bf16[2,256,128]{2,1,0:T(8,128)(2,1)S(1)}, bf16[2,256,128]{2,1,0:T(8,128)(2,1)}, u32[]{:S(2)}) copy-start(bf16[2,256,128]{2,1,0:T(8,128)(2,1)} %refs_2_.3) | copy-start | bytes 393220
  0.7 24.8 %copy-start.5 = (bf16[2,256,128]{2,1,0:T(8,128)(2,1)S(1)}, bf16[2,256,128]{2,1,0:T(8,128)(2,1)}, u32[]{:S(2)}) copy-start(bf16[2,256,128]{2,1,0:T(8,128)(2,1)} %refs_1_.3) | copy-start | bytes 393220
  0.7 24.8 %copy-start.4 = (bf16[2,256,128]{2,1,0:T(8,128)(2,1)S(1)}, bf16[2,256,128]{2,1,0:T(8,128)(2,1)}, u32[]{:S(2)}) copy-start(bf16[2,256,128]{2,1,0:T(8,128)(2,1)} %refs_0_.3) | copy-start | bytes 393220
  0.7 24.8 %copy-start.9 = (bf16[2,256]{1,0:T(2,128)(2,1)S(1)}, bf16[2,256]{1,0:T(2,128)(2,1)}, u32[]{:S(2)}) copy-start(bf16[2,256]{1,0:T(2,128)(2,1)} %gain_ref.3) | copy-start | bytes 3076
  0.7 0.8 copy-start.10
  1.5 36.1 %copy-start = (f32[2,6,128,256]{3,2,1,0:T(8,128)S(1)}, f32[2,6,128,256]{3,2,1,0:T(8,128)}, u32[]{:S(2)}) copy-start(f32[2,6,128,256]{3,2,1,0:T(8,128)} %state_ref.3) | copy-start | bytes 4718596
  1.5 36.1 %copy-start.7 = (f32[2,6,128]{2,0,1:T(2,128)S(1)}, f32[2,6,128]{2,0,1:T(2,128)}, u32[]{:S(2)}) copy-start(f32[2,6,128]{2,0,1:T(2,128)} %param.17) | copy-start | bytes 18436
  1.5 36.1 %copy-start.8 = (f32[2,128]{1,0:T(2,128)S(1)}, f32[2,128]{1,0:T(2,128)}, u32[]{:S(2)}) copy-start(f32[2,128]{1,0:T(2,128)} %shift_ref.3) | copy-start | bytes 3076
  25.5 21.5 %copy-start.1 = (bf16[2,256,256]{2,1,0:T(8,128)(2,1)S(1)}, bf16[2,256,256]{2,1,0:T(8,128)(2,1)}, u32[]{:S(2)}) copy-start(bf16[2,256,256]{2,1,0:T(8,128)(2,1)} %weight_ref.3) | copy-start | bytes 786436
  25.8 39.8 %copy-start.11 = (bf16[3,256]{1,0:T(4,128)(2,1)S(1)}, bf16[3,256]{1,0:T(4,128)(2,1)}, u32[]{:S(2)}) copy-start(bf16[3,256]{1,0:T(4,128)(2,1)} %rows_ref.1) | copy-start | bytes 4612
  103.5 18.6 %all-to-all-start.7 = ((bf16[32,4,256]{2,1,0:T(4,128)(2,1)}), bf16[32,4,256]{2,1,0:T(4,128)(2,1)S(1)}, u32[]{:S(2)}, u32[]{:S(2)}) async-start(bf16[32,4,256]{2,1,0:T(4,128)(2,1)} %reshape.32), calls=%async_computation.7 | async-start | bytes 131072 | tf_op jit(solution)/shard_map/all_to_all | solution.py:32

commit v8 on v6

v8 whole, which is shorter than its diff:
```python
import functools

import jax
import jax.numpy as jnp
from jax import lax
from jax.experimental import pallas as pl
from jax.experimental.pallas import tpu as pltpu
from jax.sharding import Mesh, PartitionSpec as P

D = 4096
DK = 128
BLOCKS = 2
PAD = 8
LANES = 128
BF = jnp.bfloat16
F32 = jnp.float32
DP = ("y", "x")
TP = ("z", "c")
VMEM = pl.BlockSpec(memory_space=pltpu.VMEM)
SMALL = pltpu.CompilerParams(vmem_limit_bytes=12 * 1024 * 1024)


ORDER = {
    "z": tuple((8 + k) % 16 for k in range(16)),
    DP: tuple((10 + k) % 16 for k in range(16)),
}
ORDER[TP] = tuple(2 * z + c for z in ORDER["z"] for c in (1, 0))
SEQ_OF_ROW = (3, 0, 4, 1, 5, 2)


def exchange(parts, axis):
    return lax.all_to_all(parts, axis, 0, 0, tiled=True, axis_index_groups=[list(ORDER[axis])])


def shift_between():
    return (ORDER[DP][0] - ORDER["z"][0]) % len(ORDER["z"])


def project_kernel(b, pieces_ref, gain_ref, *refs):
    *weights, out_ref = refs
    groups = pieces_ref.shape[0] // 2
    pieces = pieces_ref[...].astype(F32)
    first, second = pieces[:, 0, :], pieces[:, 1, :]
    at = 2 * LANES
    mixed = jnp.concatenate([first[:, at:], second[:, :LANES]], axis=1)
    rows = jnp.concatenate([first[:, :at], mixed, second[:, LANES:]], axis=0).astype(BF)
    i = lax.broadcasted_iota(jnp.int32, (groups * PAD, rows.shape[0]), 0)
    column = lax.broadcasted_iota(jnp.int32, (groups * PAD, rows.shape[0]), 1)
    piece = 2 * (((i >> 3) + shift_between()) & (groups - 1)) + (i & 1)
    chosen = jnp.where(column == ((i & 7) >> 1) * 2 * groups + piece, 1.0, 0.0).astype(BF)
    rows = jnp.dot(chosen, rows, preferred_element_type=F32)
    squares = jnp.sum(rows * rows, axis=1, keepdims=True)
    hidden = (rows * gain_ref[b : b + 1, :].astype(F32)).astype(BF)
    tiles = []
    for w in weights:
        part = jnp.dot(hidden, w[b], preferred_element_type=F32)
        tiles += [part[:, k : k + LANES] for k in range(0, part.shape[1], LANES)]
    last = tiles.pop()
    row = lax.broadcasted_iota(jnp.int32, last.shape, 0) & 7
    lane = lax.broadcasted_iota(jnp.int32, last.shape, 1)
    spread_squares = jnp.broadcast_to(squares, last.shape)
    moved = [pltpu.roll(spread_squares, k, 0) for k in (6, 4, 2)]
    extra = [pltpu.roll(last, k, 0) for k in (6, 4, 2)]
    extra.append(jnp.where(lane == 0, moved[0], jnp.where(lane == 1, moved[1], moved[2])))
    for k, tile in enumerate(tiles):
        if k < len(extra):
            tile = jnp.where(row >= 6, extra[k], tile)
        out_ref[:, :, k * LANES : (k + 1) * LANES] = tile.reshape(groups, PAD, LANES).astype(BF)


def project(b, pieces, gain, weights):
    cols = sum(w.shape[2] for w in weights) - LANES
    return pl.pallas_call(
        functools.partial(project_kernel, b),
        out_shape=jax.ShapeDtypeStruct((pieces.shape[0] // 2, PAD, cols), BF),
        in_specs=[VMEM] * (2 + len(weights)),
        out_specs=VMEM,
        compiler_params=SMALL,
        name="project",
    )(pieces, gain, *weights)


def spread_kernel(rows_ref, out_ref, own_ref):
    rows = rows_ref[...].astype(F32)
    first = jnp.concatenate([rows[0:1], rows[1:2, :LANES]], axis=1)
    second = jnp.concatenate([rows[1:2, LANES:], rows[2:3]], axis=1)
    own = jnp.concatenate([first, second], axis=0)
    own_ref[...] = own.astype(BF)
    out_ref[...] = jnp.broadcast_to(own[None], out_ref.shape).astype(BF)


def spread(rows, n):
    piece = (2, rows.size // 2)
    return pl.pallas_call(
        spread_kernel,
        out_shape=(jax.ShapeDtypeStruct((n, *piece), BF), jax.ShapeDtypeStruct(piece, BF)),
        in_specs=[VMEM],
        out_specs=(VMEM, VMEM),
        compiler_params=SMALL,
        cost_estimate=pl.CostEstimate(flops=10**10, bytes_accessed=10**7, transcendentals=0),
        name="spread",
    )(rows)


def step_kernel(b, seqs, kc, vc, parts_ref, shift_ref, fade_ref, state_ref, out_ref, d_ref, k_ref, v_ref):
    total = jnp.sum(parts_ref[...].astype(F32), axis=0)
    tiles = [total[:, k : k + LANES] for k in range(0, total.shape[1], LANES)]
    row = lax.broadcasted_iota(jnp.int32, tiles[0].shape, 0)
    lane = lax.broadcasted_iota(jnp.int32, tiles[0].shape, 1)

    def from_blank(first, second, third):
        second, third = pltpu.roll(second, 4, 0), pltpu.roll(third, 6, 0)
        return jnp.where(row < 2, pltpu.roll(first, 2, 0), jnp.where(row < 4, second, third))

    tiles.append(from_blank(*tiles[:3]))
    squares = jnp.where(lane == row >> 1, from_blank(*tiles[3:4] * 3), 0.0)
    inv_rms = lax.rsqrt(jnp.sum(squares, axis=1, keepdims=True)[:seqs] / D + 1e-06)
    total = jnp.concatenate(tiles, axis=1)[:seqs] * inv_rms
    cols = 3 * kc + 2 * vc
    queries = total[:, :kc] * DK ** (-0.5)
    keys = total[:, kc : 2 * kc]
    pre = total[:, 2 * kc : 3 * kc] + shift_ref[b : b + 1, :]
    values = total[:, 3 * kc : 3 * kc + vc]
    gates = total[:, 3 * kc + vc : cols]
    log_sigmoid = jnp.minimum(pre, 0.0) - jnp.log1p(jnp.exp(-jnp.abs(pre)))
    fade = jnp.concatenate([fade_ref[s : s + 1, b, :] for s in SEQ_OF_ROW], axis=0)
    decay = jnp.exp(log_sigmoid / 16.0 + fade)
    fresh_part = jnp.sum(queries * keys, axis=1, keepdims=True) * values
    columns = jnp.concatenate([queries * decay, jnp.zeros((PAD - seqs, kc), F32)], axis=0).T
    old = [
        jnp.sum(columns[:, j : j + 1] * state_ref[b, s], axis=0, keepdims=True)
        for j, s in enumerate(SEQ_OF_ROW)
    ]
    readout = jnp.concatenate(old, axis=0) + fresh_part
    gated = readout * (gates / (1.0 + jnp.exp(-gates)))
    gated = jnp.concatenate([gated, jnp.zeros((PAD - seqs, vc), F32)], axis=0)
    out_ref[...] = jnp.broadcast_to(gated[None], out_ref.shape).astype(BF)
    for j, s in enumerate(SEQ_OF_ROW):
        d_ref[s : s + 1] = decay[j : j + 1]
        k_ref[s : s + 1] = keys[j : j + 1]
        v_ref[s : s + 1] = values[j : j + 1]


def step(b, parts, shift, fade, state):
    seqs, _, kc = fade.shape
    vc = state.shape[3]
    return pl.pallas_call(
        functools.partial(step_kernel, b, seqs, kc, vc),
        out_shape=(
            jax.ShapeDtypeStruct((parts.shape[0], PAD, vc), BF),
            jax.ShapeDtypeStruct((seqs, kc), F32),
            jax.ShapeDtypeStruct((seqs, kc), F32),
            jax.ShapeDtypeStruct((seqs, vc), F32),
        ),
        in_specs=[VMEM] * 4,
        out_specs=(VMEM,) * 4,
        compiler_params=SMALL,
        name="step",
    )(parts, shift, fade, state)


def readback_kernel(b, gated_ref, weight_ref, out_ref):
    groups, pad, width = gated_ref.shape
    gated = gated_ref[...].astype(F32).reshape(groups * pad, width).astype(BF)
    n = 6 * groups
    i = lax.broadcasted_iota(jnp.int32, (n, groups * pad), 0)
    column = lax.broadcasted_iota(jnp.int32, (n, groups * pad), 1)
    piece = lax.rem(i, 2 * groups)
    group = ((piece >> 1) + groups - shift_between()) & (groups - 1)
    source = group * pad + 2 * lax.div(i, 2 * groups) + (piece & 1)
    chosen = jnp.where(column == source, 1.0, 0.0).astype(BF)
    gated = jnp.dot(chosen, gated, preferred_element_type=F32).astype(BF)
    branch = jnp.dot(gated, weight_ref[b], preferred_element_type=F32)
    one, two, three = (branch[k * 2 * groups : (k + 1) * 2 * groups] for k in range(3))
    first = jnp.concatenate([one, two[:, :LANES]], axis=1)
    second = jnp.concatenate([two[:, LANES:], three], axis=1)
    out_ref[...] = jnp.stack([first, second], axis=1).astype(BF)


def readback(b, gated, weight):
    groups = gated.shape[0]
    return pl.pallas_call(
        functools.partial(readback_kernel, b),
        out_shape=jax.ShapeDtypeStruct((2 * groups, 2, 3 * weight.shape[2] // 2), BF),
        in_specs=[VMEM] * 2,
        out_specs=VMEM,
        compiler_params=SMALL,
        name="readback",
    )(gated, weight)


def shards(
    incoming_embeddings,
    rescale_factors,
    probe_lift,
    address_lift,
    forget_lift,
    forget_shift,
    surplus_fade,
    content_lift,
    filter_lift,
    readback_lift,
    memory_tensor,
):
    weights = (probe_lift, address_lift, forget_lift, content_lift, filter_lift)
    depth = lax.axis_size("z")
    fade = jnp.transpose(surplus_fade, (1, 0, 2))
    copies, stream = spread(incoming_embeddings, 2 * depth)
    kept = []
    for b in range(BLOCKS):
        pieces = exchange(copies, TP)
        parts = exchange(project(b, pieces, rescale_factors, weights), DP)
        gated, *small = step(b, parts, forget_shift, fade, memory_tensor)
        kept.append(small)
        gathered = exchange(gated, DP)
        if b == BLOCKS - 1:
            gathered, kept = lax.optimization_barrier((gathered, kept))
        heads = exchange(readback(b, gathered, readback_lift), TP)
        branch = jnp.sum(heads.astype(F32), axis=0)
        stream = (stream.astype(F32) + branch).astype(BF)
        copies = jnp.broadcast_to(stream[None], copies.shape)
    fresh = [
        memory_tensor[b] * d[:, :, None] + k[:, :, None] * v[:, None, :]
        for b, (d, k, v) in enumerate(kept)
    ]
    return stream.reshape(incoming_embeddings.shape), jnp.stack(fresh)


def solution(mesh):
    z = mesh.shape["tp"] // 2
    fine = Mesh(mesh.devices.reshape(z, 2, 4, 4), ("z", "c", "y", "x"))
    in_specs = (
        P(TP, DP),
        P(None, DP),
        P(None, DP, TP),
        P(None, DP, TP),
        P(None, DP, TP),
        P(None, TP),
        P(None, DP, TP),
        P(None, DP, TP),
        P(None, DP, TP),
        P(None, TP, DP),
        P(None, DP, None, TP),
    )
    out_specs = (P(TP, DP), P(None, DP, None, TP))
    return jax.shard_map(shards, mesh=fine, in_specs=in_specs, out_specs=out_specs, check_vma=False)
```

time: 123 us -> 120 us (0.976)
  blocking collectives: 98.3 us -> 96 us
  Pallas kernels: 1.61 us -> 2.97 us
    all_to_all x7, blocking collectives: 98.3 us -> 96 us  [exchange(): lax.all_to_all(parts, axis, 0, 0, tiled=True, axis_index_groups=[list(ORD...]
where the time goes in v8:
time: 120 us
  blocking collectives  96 us (80%)
  starting transfers between devices  14.7 us (12%)
  Pallas kernels  2.97 us (2%)
  waiting for transfers between devices  1.92 us (2%)
  other arithmetic  1.87 us (2%)
  local copies, waits for them, and re-layouts  1.42 us (1%)
    all_to_all x7, blocking collectives, exchange(): lax.all_to_all(parts, axis, 0, 0, tiled=True, axis_index_groups=[list(ORD...  96 us
    all_to_all x1, starting transfers between devices, exchange(): lax.all_to_all(parts, axis, 0, 0, tiled=True, axis_index_groups=[list(ORD...  14.7 us
  transfers between devices with their start and end apart: 1, of which 1 were waited for; matrix products, arithmetic and copies ran while one was open for 1% of the time, Pallas kernels for 0%

profile of v8, /device:TPU:1, one launch (start us, length us, event | category | flops | bytes accessed | tf_op | source)
XLA Modules:
  0.0 119.7 jit_solution(9036485988432639116)
XLA Ops:
  0.6 0.0 copy-start.3
  0.6 0.0 copy-start.2
  0.7 0.0 copy-start.6
  0.7 0.0 copy-start.5
  0.7 0.0 copy-start.4
  0.7 0.0 copy-start.9
  0.7 0.0 copy-start.10
  0.7 0.7 copy-done.10
  1.5 0.0 copy-start
  1.5 0.0 copy-start.7
  1.5 0.0 copy-start.8
  1.5 23.1 %all_to_all.40.pieces_ref = bf16[32,2,384]{2,1,0:T(2,128)(2,1)S(1)} all-to-all(bf16[32,2,384]{2,1,0:T(2,128)(2,1)S(1)} %get-tuple-element.20), channel_id=1, replica_groups={{272,256,304,288,336,320,368,352,400,384,432,416,464,448,496,480,16,0,4..., dimensions={0} | all-to-all | bytes 98304 | tf_op jit(solution)/shard_map/all_to_all | solution.py:32
  24.6 0.0 copy-done.3
  24.6 0.0 copy-done.2
  24.6 0.0 copy-done.6
  24.6 0.0 copy-done.5
  24.7 0.0 copy-done.4
  24.7 0.0 copy-done.9
  24.7 0.0 copy-start.1
  24.7 0.4 project.2
  25.1 10.8 %all_to_all.41.parts_ref = bf16[16,8,768]{2,1,0:T(8,128)(2,1)S(1)} all-to-all(bf16[16,8,768]{2,1,0:T(8,128)(2,1)S(1)} %project.2), channel_id=1, replica_groups={{10,11,12,13,14,15,0,1,2,3,4,5,6,7,8,9},{26,27,28,29,30,31,16,17,18,19,..., dimensions={0} | all-to-all | bytes 393216 | tf_op jit(solution)/shard_map/all_to_all | solution.py:32
  36.0 0.0 copy-done
  36.0 0.0 copy-done.7
  36.0 0.0 copy-done.8
  36.0 0.4 step.2
  36.4 9.2 %all_to_all.42.gated_ref = bf16[16,8,256]{2,1,0:T(8,128)(2,1)S(1)} all-to-all(bf16[16,8,256]{2,1,0:T(8,128)(2,1)S(1)} %get-tuple-element.21), channel_id=1, replica_groups={{10,11,12,13,14,15,0,1,2,3,4,5,6,7,8,9},{26,27,28,29,30,31,16,17,18,19,..., dimensions={0} | all-to-all | bytes 131072 | tf_op jit(solution)/shard_map/all_to_all | solution.py:32
  45.6 0.0 copy-done.1
  45.6 0.3 readback.2
  45.9 17.9 %all_to_all.43 = bf16[32,2,384]{2,1,0:T(2,128)(2,1)S(1)} all-to-all(bf16[32,2,384]{2,1,0:T(2,128)(2,1)S(1)} %readback.2), channel_id=1, replica_groups={{272,256,304,288,336,320,368,352,400,384,432,416,464,448,496,480,16,0,4..., dimensions={0} | all-to-all | bytes 98304 | tf_op jit(solution)/shard_map/all_to_all | solution.py:32
  63.8 0.1 convert_reduce_fusion.1
  63.9 15.5 %all_to_all.44.pieces_ref = bf16[32,2,384]{2,1,0:T(2,128)(2,1)S(1)} all-to-all(bf16[32,2,384]{2,1,0:T(2,128)(2,1)S(1)} %broadcast_in_dim.2), channel_id=1, replica_groups={{272,256,304,288,336,320,368,352,400,384,432,416,464,448,496,480,16,0,4..., dimensions={0} | all-to-all | bytes 98304 | tf_op jit(solution)/shard_map/all_to_all | solution.py:32
  79.4 0.4 project.3
  79.8 10.3 %all_to_all.45.parts_ref = bf16[16,8,768]{2,1,0:T(8,128)(2,1)S(1)} all-to-all(bf16[16,8,768]{2,1,0:T(8,128)(2,1)S(1)} %project.3), channel_id=1, replica_groups={{10,11,12,13,14,15,0,1,2,3,4,5,6,7,8,9},{26,27,28,29,30,31,16,17,18,19,..., dimensions={0} | all-to-all | bytes 393216 | tf_op jit(solution)/shard_map/all_to_all | solution.py:32
  90.1 0.4 step.3
  90.5 9.2 %all_to_all.46.gated_ref = bf16[16,8,256]{2,1,0:T(8,128)(2,1)S(1)} all-to-all(bf16[16,8,256]{2,1,0:T(8,128)(2,1)S(1)} %get-tuple-element.22), channel_id=1, replica_groups={{10,11,12,13,14,15,0,1,2,3,4,5,6,7,8,9},{26,27,28,29,30,31,16,17,18,19,..., dimensions={0} | all-to-all | bytes 131072 | tf_op jit(solution)/shard_map/all_to_all | solution.py:32
  99.7 1.0 readback.3
  100.7 14.7 %all-to-all-start.7 = ((bf16[32,2,384]{2,1,0:T(2,128)(2,1)}), bf16[32,2,384]{2,1,0:T(2,128)(2,1)S(1)}, u32[]{:S(2)}, u32[]{:S(2)}) async-start(bf16[32,2,384]{2,1,0:T(2,128)(2,1)} %readback.3), calls=%async_computation.7 | async-start | bytes 98304 | tf_op jit(solution)/shard_map/all_to_all | solution.py:32
  115.4 0.5 multiply_add_fusion.1
  115.9 1.2 %pad_maximum_fusion = f32[2,6,128,256]{3,2,1,0:T(8,128)} fusion(f32[1,6,128,256]{3,2,1,0:T(8,128)S(1)} %get-tuple-element.37, f32[1,6,128,256]{3,2,1,0:T(8,128)S(1)} %get-tuple-element.36), kind=kLoop, calls=%fused_computation | loop fusion | flops 393216 | bytes 3145728 | tf_op jit(solution)/shard_map/stack | solution.py:226
  117.1 1.9 %all-to-all-done.7 = bf16[32,2,384]{2,1,0:T(2,128)(2,1)S(1)} async-done(((bf16[32,2,384]{2,1,0:T(2,128)(2,1)}), bf16[32,2,384]{2,1,0:T(2,128)(2,1)S(1)}, u32[]{:S(2)}, u32[]{:S(2)}) %all-to-all-start.7) | async-done | bytes 49184 | tf_op jit(solution)/shard_map/all_to_all | solution.py:32
  119.1 0.1 convert_reduce_fusion
  119.1 0.6 reshape.20
  (4 shorter events, 0.1 us)
Async XLA Ops:
  0.6 24.0 %copy-start.3 = (bf16[2,256,256]{2,1,0:T(8,128)(2,1)S(1)}, bf16[2,256,256]{2,1,0:T(8,128)(2,1)}, u32[]{:S(2)}) copy-start(bf16[2,256,256]{2,1,0:T(8,128)(2,1)} %refs_4_.3) | copy-start | bytes 786436
  0.6 24.0 %copy-start.2 = (bf16[2,256,256]{2,1,0:T(8,128)(2,1)S(1)}, bf16[2,256,256]{2,1,0:T(8,128)(2,1)}, u32[]{:S(2)}) copy-start(bf16[2,256,256]{2,1,0:T(8,128)(2,1)} %refs_3_.3) | copy-start | bytes 786436
  0.7 24.0 %copy-start.6 = (bf16[2,256,128]{2,1,0:T(8,128)(2,1)S(1)}, bf16[2,256,128]{2,1,0:T(8,128)(2,1)}, u32[]{:S(2)}) copy-start(bf16[2,256,128]{2,1,0:T(8,128)(2,1)} %refs_2_.3) | copy-start | bytes 393220
  0.7 24.0 %copy-start.5 = (bf16[2,256,128]{2,1,0:T(8,128)(2,1)S(1)}, bf16[2,256,128]{2,1,0:T(8,128)(2,1)}, u32[]{:S(2)}) copy-start(bf16[2,256,128]{2,1,0:T(8,128)(2,1)} %refs_1_.3) | copy-start | bytes 393220
  0.7 24.0 %copy-start.4 = (bf16[2,256,128]{2,1,0:T(8,128)(2,1)S(1)}, bf16[2,256,128]{2,1,0:T(8,128)(2,1)}, u32[]{:S(2)}) copy-start(bf16[2,256,128]{2,1,0:T(8,128)(2,1)} %refs_0_.3) | copy-start | bytes 393220
  0.7 24.0 %copy-start.9 = (bf16[2,256]{1,0:T(2,128)(2,1)S(1)}, bf16[2,256]{1,0:T(2,128)(2,1)}, u32[]{:S(2)}) copy-start(bf16[2,256]{1,0:T(2,128)(2,1)} %gain_ref.3) | copy-start | bytes 3076
  0.7 0.8 copy-start.10
  1.5 34.5 %copy-start = (f32[2,6,128,256]{3,2,1,0:T(8,128)S(1)}, f32[2,6,128,256]{3,2,1,0:T(8,128)}, u32[]{:S(2)}) copy-start(f32[2,6,128,256]{3,2,1,0:T(8,128)} %state_ref.3) | copy-start | bytes 4718596
  1.5 34.5 %copy-start.7 = (f32[2,6,128]{2,0,1:T(2,128)S(1)}, f32[2,6,128]{2,0,1:T(2,128)}, u32[]{:S(2)}) copy-start(f32[2,6,128]{2,0,1:T(2,128)} %param.17) | copy-start | bytes 18436
  1.5 34.5 %copy-start.8 = (f32[2,128]{1,0:T(2,128)S(1)}, f32[2,128]{1,0:T(2,128)}, u32[]{:S(2)}) copy-start(f32[2,128]{1,0:T(2,128)} %shift_ref.3) | copy-start | bytes 3076
  24.7 20.9 %copy-start.1 = (bf16[2,256,256]{2,1,0:T(8,128)(2,1)S(1)}, bf16[2,256,256]{2,1,0:T(8,128)(2,1)}, u32[]{:S(2)}) copy-start(bf16[2,256,256]{2,1,0:T(8,128)(2,1)} %weight_ref.3) | copy-start | bytes 786436
  100.7 18.4 %all-to-all-start.7 = ((bf16[32,2,384]{2,1,0:T(2,128)(2,1)}), bf16[32,2,384]{2,1,0:T(2,128)(2,1)S(1)}, u32[]{:S(2)}, u32[]{:S(2)}) async-start(bf16[32,2,384]{2,1,0:T(2,128)(2,1)} %readback.3), calls=%async_computation.7 | async-start | bytes 98304 | tf_op jit(solution)/shard_map/all_to_all | solution.py:32

commit v9 on v8

--- a/solution.py
+++ b/solution.py
@@ -97,9 +97,44 @@
         in_specs=[VMEM],
         out_specs=(VMEM, VMEM),
         compiler_params=SMALL,
-        cost_estimate=pl.CostEstimate(flops=10**10, bytes_accessed=10**7, transcendentals=0),
         name="spread",
     )(rows)
+
+
+def hold_kernel(in_ref, out_ref):
+    out_ref[0] = in_ref[0]
+
+
+def hold(copies):
+    return pl.pallas_call(
+        hold_kernel,
+        out_shape=jax.ShapeDtypeStruct(copies.shape, copies.dtype),
+        in_specs=[VMEM],
+        out_specs=VMEM,
+        input_output_aliases={0: 0},
+        compiler_params=SMALL,
+        cost_estimate=pl.CostEstimate(flops=10**10, bytes_accessed=10**7, transcendentals=0),
+        name="hold",
+    )(copies)
+
+
+def finish_kernel(heads_ref, stream_ref, out_ref):
+    total = jnp.sum(heads_ref[...].astype(F32), axis=0) + stream_ref[...].astype(F32)
+    first, second = total[0:1], total[1:2]
+    at = 2 * LANES
+    middle = jnp.concatenate([first[:, at:], second[:, :LANES]], axis=1)
+    out_ref[...] = jnp.concatenate([first[:, :at], middle, second[:, LANES:]], axis=0).astype(BF)
+
+
+def finish(heads, stream, shape):
+    return pl.pallas_call(
+        finish_kernel,
+        out_shape=jax.ShapeDtypeStruct(shape, BF),
+        in_specs=[VMEM] * 2,
+        out_specs=VMEM,
+        compiler_params=SMALL,
+        name="finish",
+    )(heads, stream)
 
 
 def step_kernel(b, seqs, kc, vc, parts_ref, shift_ref, fade_ref, state_ref, out_ref, d_ref, k_ref, v_ref):
@@ -206,6 +241,7 @@
     depth = lax.axis_size("z")
     fade = jnp.transpose(surplus_fade, (1, 0, 2))
     copies, stream = spread(incoming_embeddings, 2 * depth)
+    copies = hold(copies)
     kept = []
     for b in range(BLOCKS):
         pieces = exchange(copies, TP)
@@ -216,6 +252,9 @@
         if b == BLOCKS - 1:
             gathered, kept = lax.optimization_barrier((gathered, kept))
         heads = exchange(readback(b, gathered, readback_lift), TP)
+        if b == BLOCKS - 1:
+            mixed = finish(heads, stream, incoming_embeddings.shape)
+            break
         branch = jnp.sum(heads.astype(F32), axis=0)
         stream = (stream.astype(F32) + branch).astype(BF)
         copies = jnp.broadcast_to(stream[None], copies.shape)
@@ -223,7 +262,7 @@
         memory_tensor[b] * d[:, :, None] + k[:, :, None] * v[:, None, :]
         for b, (d, k, v) in enumerate(kept)
     ]
-    return stream.reshape(incoming_embeddings.shape), jnp.stack(fresh)
+    return mixed, jnp.stack(fresh)
 
 
 def solution(mesh):

time: 120 us -> 120 us (level)
  no operation moved by 1% of the time
where the time goes in v9:
time: 120 us
  blocking collectives  96 us (80%)
  starting transfers between devices  14.7 us (12%)
  Pallas kernels  3.6 us (3%)
  waiting for transfers between devices  1.9 us (2%)
  other arithmetic  1.81 us (2%)
    all_to_all x7, blocking collectives, exchange(): lax.all_to_all(parts, axis, 0, 0, tiled=True, axis_index_groups=[list(ORD...  96 us
    all_to_all x1, starting transfers between devices, exchange(): lax.all_to_all(parts, axis, 0, 0, tiled=True, axis_index_groups=[list(ORD...  14.7 us
  transfers between devices with their start and end apart: 1, of which 1 were waited for; matrix products, arithmetic and copies ran while one was open for 1% of the time, Pallas kernels for 0%

profile of v9, /device:TPU:1, one launch (start us, length us, event | category | flops | bytes accessed | tf_op | source)
XLA Modules:
  0.0 119.6 jit_solution(3637723488104167781)
XLA Ops:
  0.6 0.0 copy-start.10
  0.6 0.7 copy-done.10
  1.3 0.0 copy-start.2
  1.4 0.0 copy-start.3
  1.4 0.0 copy-start.4
  1.4 0.0 copy-start.5
  1.4 0.0 copy-start.6
  1.4 0.0 copy-start.9
  1.4 0.0 copy-start
  1.4 0.0 copy-start.7
  1.4 0.0 copy-start.8
  1.5 23.1 %all_to_all.40.pieces_ref = bf16[32,2,384]{2,1,0:T(2,128)(2,1)S(1)} all-to-all(bf16[32,2,384]{2,1,0:T(2,128)(2,1)S(1)} %hold.1), channel_id=1, replica_groups={{272,256,304,288,336,320,368,352,400,384,432,416,464,448,496,480,16,0,4..., dimensions={0} | all-to-all | bytes 98304 | tf_op jit(solution)/shard_map/all_to_all | solution.py:32
  24.6 0.0 copy-done.2
  24.6 0.0 copy-done.3
  24.6 0.0 copy-done.4
  24.6 0.0 copy-done.5
  24.6 0.0 copy-done.6
  24.6 0.0 copy-done.9
  24.6 0.0 copy-start.1
  24.6 0.4 project.2
  25.1 10.8 %all_to_all.41.parts_ref = bf16[16,8,768]{2,1,0:T(8,128)(2,1)S(1)} all-to-all(bf16[16,8,768]{2,1,0:T(8,128)(2,1)S(1)} %project.2), channel_id=1, replica_groups={{10,11,12,13,14,15,0,1,2,3,4,5,6,7,8,9},{26,27,28,29,30,31,16,17,18,19,..., dimensions={0} | all-to-all | bytes 393216 | tf_op jit(solution)/shard_map/all_to_all | solution.py:32
  35.9 0.0 copy-done
  35.9 0.0 copy-done.7
  35.9 0.0 copy-done.8
  35.9 0.4 step.2
  36.3 9.2 %all_to_all.42.gated_ref = bf16[16,8,256]{2,1,0:T(8,128)(2,1)S(1)} all-to-all(bf16[16,8,256]{2,1,0:T(8,128)(2,1)S(1)} %get-tuple-element.21), channel_id=1, replica_groups={{10,11,12,13,14,15,0,1,2,3,4,5,6,7,8,9},{26,27,28,29,30,31,16,17,18,19,..., dimensions={0} | all-to-all | bytes 131072 | tf_op jit(solution)/shard_map/all_to_all | solution.py:32
  45.5 0.0 copy-done.1
  45.5 0.3 readback.2
  45.9 17.9 %all_to_all.43 = bf16[32,2,384]{2,1,0:T(2,128)(2,1)S(1)} all-to-all(bf16[32,2,384]{2,1,0:T(2,128)(2,1)S(1)} %readback.2), channel_id=1, replica_groups={{272,256,304,288,336,320,368,352,400,384,432,416,464,448,496,480,16,0,4..., dimensions={0} | all-to-all | bytes 98304 | tf_op jit(solution)/shard_map/all_to_all | solution.py:32
  63.8 0.1 convert_reduce_fusion
  63.9 15.5 %all_to_all.44.pieces_ref = bf16[32,2,384]{2,1,0:T(2,128)(2,1)S(1)} all-to-all(bf16[32,2,384]{2,1,0:T(2,128)(2,1)S(1)} %broadcast_in_dim.2), channel_id=1, replica_groups={{272,256,304,288,336,320,368,352,400,384,432,416,464,448,496,480,16,0,4..., dimensions={0} | all-to-all | bytes 98304 | tf_op jit(solution)/shard_map/all_to_all | solution.py:32
  79.4 0.4 project.3
  79.8 10.3 %all_to_all.45.parts_ref = bf16[16,8,768]{2,1,0:T(8,128)(2,1)S(1)} all-to-all(bf16[16,8,768]{2,1,0:T(8,128)(2,1)S(1)} %project.3), channel_id=1, replica_groups={{10,11,12,13,14,15,0,1,2,3,4,5,6,7,8,9},{26,27,28,29,30,31,16,17,18,19,..., dimensions={0} | all-to-all | bytes 393216 | tf_op jit(solution)/shard_map/all_to_all | solution.py:32
  90.1 0.4 step.3
  90.5 9.2 %all_to_all.46.gated_ref = bf16[16,8,256]{2,1,0:T(8,128)(2,1)S(1)} all-to-all(bf16[16,8,256]{2,1,0:T(8,128)(2,1)S(1)} %get-tuple-element.22), channel_id=1, replica_groups={{10,11,12,13,14,15,0,1,2,3,4,5,6,7,8,9},{26,27,28,29,30,31,16,17,18,19,..., dimensions={0} | all-to-all | bytes 131072 | tf_op jit(solution)/shard_map/all_to_all | solution.py:32
  99.7 1.0 readback.3
  100.6 14.7 %all-to-all-start.7 = ((bf16[32,2,384]{2,1,0:T(2,128)(2,1)}), bf16[32,2,384]{2,1,0:T(2,128)(2,1)S(1)}, u32[]{:S(2)}, u32[]{:S(2)}) async-start(bf16[32,2,384]{2,1,0:T(2,128)(2,1)} %readback.3), calls=%async_computation.7 | async-start | bytes 98304 | tf_op jit(solution)/shard_map/all_to_all | solution.py:32
  115.4 0.5 multiply_add_fusion.1
  115.9 1.2 %pad_maximum_fusion = f32[2,6,128,256]{3,2,1,0:T(8,128)} fusion(f32[1,6,128,256]{3,2,1,0:T(8,128)S(1)} %get-tuple-element.37, f32[1,6,128,256]{3,2,1,0:T(8,128)S(1)} %get-tuple-element.36), kind=kLoop, calls=%fused_computation | loop fusion | flops 393216 | bytes 3145728 | tf_op jit(solution)/shard_map/stack | solution.py:265
  117.1 1.9 %all-to-all-done.7.heads_ref = bf16[32,2,384]{2,1,0:T(2,128)(2,1)S(1)} async-done(((bf16[32,2,384]{2,1,0:T(2,128)(2,1)}), bf16[32,2,384]{2,1,0:T(2,128)(2,1)S(1)}, u32[]{:S(2)}, u32[]{:S(2)}) %all-to-all-start.7) | async-done | bytes 49184 | tf_op jit(solution)/shard_map/all_to_all | solution.py:32
  119.0 0.6 finish.1
  (4 shorter events, 0.1 us)
Async XLA Ops:
  0.6 0.7 copy-start.10
  1.3 23.3 %copy-start.2 = (bf16[2,256,256]{2,1,0:T(8,128)(2,1)S(1)}, bf16[2,256,256]{2,1,0:T(8,128)(2,1)}, u32[]{:S(2)}) copy-start(bf16[2,256,256]{2,1,0:T(8,128)(2,1)} %refs_3_.3) | copy-start | bytes 786436
  1.4 23.2 %copy-start.3 = (bf16[2,256,256]{2,1,0:T(8,128)(2,1)S(1)}, bf16[2,256,256]{2,1,0:T(8,128)(2,1)}, u32[]{:S(2)}) copy-start(bf16[2,256,256]{2,1,0:T(8,128)(2,1)} %refs_4_.3) | copy-start | bytes 786436
  1.4 23.2 %copy-start.4 = (bf16[2,256,128]{2,1,0:T(8,128)(2,1)S(1)}, bf16[2,256,128]{2,1,0:T(8,128)(2,1)}, u32[]{:S(2)}) copy-start(bf16[2,256,128]{2,1,0:T(8,128)(2,1)} %refs_0_.3) | copy-start | bytes 393220
  1.4 23.2 %copy-start.5 = (bf16[2,256,128]{2,1,0:T(8,128)(2,1)S(1)}, bf16[2,256,128]{2,1,0:T(8,128)(2,1)}, u32[]{:S(2)}) copy-start(bf16[2,256,128]{2,1,0:T(8,128)(2,1)} %refs_1_.3) | copy-start | bytes 393220
  1.4 23.2 %copy-start.6 = (bf16[2,256,128]{2,1,0:T(8,128)(2,1)S(1)}, bf16[2,256,128]{2,1,0:T(8,128)(2,1)}, u32[]{:S(2)}) copy-start(bf16[2,256,128]{2,1,0:T(8,128)(2,1)} %refs_2_.3) | copy-start | bytes 393220
  1.4 23.2 %copy-start.9 = (bf16[2,256]{1,0:T(2,128)(2,1)S(1)}, bf16[2,256]{1,0:T(2,128)(2,1)}, u32[]{:S(2)}) copy-start(bf16[2,256]{1,0:T(2,128)(2,1)} %gain_ref.3) | copy-start | bytes 3076
  1.4 34.5 %copy-start = (f32[2,6,128,256]{3,2,1,0:T(8,128)S(1)}, f32[2,6,128,256]{3,2,1,0:T(8,128)}, u32[]{:S(2)}) copy-start(f32[2,6,128,256]{3,2,1,0:T(8,128)} %state_ref.3) | copy-start | bytes 4718596
  1.4 34.5 %copy-start.7 = (f32[2,6,128]{2,0,1:T(2,128)S(1)}, f32[2,6,128]{2,0,1:T(2,128)}, u32[]{:S(2)}) copy-start(f32[2,6,128]{2,0,1:T(2,128)} %param.17) | copy-start | bytes 18436
  1.4 34.5 %copy-start.8 = (f32[2,128]{1,0:T(2,128)S(1)}, f32[2,128]{1,0:T(2,128)}, u32[]{:S(2)}) copy-start(f32[2,128]{1,0:T(2,128)} %shift_ref.3) | copy-start | bytes 3076
  24.6 20.9 %copy-start.1 = (bf16[2,256,256]{2,1,0:T(8,128)(2,1)S(1)}, bf16[2,256,256]{2,1,0:T(8,128)(2,1)}, u32[]{:S(2)}) copy-start(bf16[2,256,256]{2,1,0:T(8,128)(2,1)} %weight_ref.3) | copy-start | bytes 786436
  100.6 18.4 %all-to-all-start.7 = ((bf16[32,2,384]{2,1,0:T(2,128)(2,1)}), bf16[32,2,384]{2,1,0:T(2,128)(2,1)S(1)}, u32[]{:S(2)}, u32[]{:S(2)}) async-start(bf16[32,2,384]{2,1,0:T(2,128)(2,1)} %readback.3), calls=%async_computation.7 | async-start | bytes 98304 | tf_op jit(solution)/shard_map/all_to_all | solution.py:32

commit v10 on v9

--- a/solution.py
+++ b/solution.py
@@ -168,8 +168,9 @@
     ]
     readout = jnp.concatenate(old, axis=0) + fresh_part
     gated = readout * (gates / (1.0 + jnp.exp(-gates)))
-    gated = jnp.concatenate([gated, jnp.zeros((PAD - seqs, vc), F32)], axis=0)
-    out_ref[...] = jnp.broadcast_to(gated[None], out_ref.shape).astype(BF)
+    chunks = [gated[j : j + 1, k : k + LANES] for j in range(seqs) for k in range(0, vc, LANES)]
+    packed = [jnp.concatenate(chunks[k : k + 3], axis=1) for k in range(0, len(chunks), 3)]
+    out_ref[...] = jnp.broadcast_to(jnp.concatenate(packed, axis=0)[None], out_ref.shape).astype(BF)
     for j, s in enumerate(SEQ_OF_ROW):
         d_ref[s : s + 1] = decay[j : j + 1]
         k_ref[s : s + 1] = keys[j : j + 1]
@@ -182,7 +183,7 @@
     return pl.pallas_call(
         functools.partial(step_kernel, b, seqs, kc, vc),
         out_shape=(
-            jax.ShapeDtypeStruct((parts.shape[0], PAD, vc), BF),
+            jax.ShapeDtypeStruct((parts.shape[0], seqs * vc // (3 * LANES), 3 * LANES), BF),
             jax.ShapeDtypeStruct((seqs, kc), F32),
             jax.ShapeDtypeStruct((seqs, kc), F32),
             jax.ShapeDtypeStruct((seqs, vc), F32),
@@ -195,16 +196,21 @@
 
 
 def readback_kernel(b, gated_ref, weight_ref, out_ref):
-    groups, pad, width = gated_ref.shape
-    gated = gated_ref[...].astype(F32).reshape(groups * pad, width).astype(BF)
-    n = 6 * groups
-    i = lax.broadcasted_iota(jnp.int32, (n, groups * pad), 0)
-    column = lax.broadcasted_iota(jnp.int32, (n, groups * pad), 1)
+    groups, packed, width = gated_ref.shape
+    flat = gated_ref[...].astype(F32).reshape(groups * packed, width).astype(BF)
+    chunks = jnp.concatenate([flat[:, k : k + LANES] for k in range(0, width, LANES)], axis=0)
+    i = lax.broadcasted_iota(jnp.int32, (6 * groups, chunks.shape[0]), 0)
+    column = lax.broadcasted_iota(jnp.int32, (6 * groups, chunks.shape[0]), 1)
     piece = lax.rem(i, 2 * groups)
     group = ((piece >> 1) + groups - shift_between()) & (groups - 1)
-    source = group * pad + 2 * lax.div(i, 2 * groups) + (piece & 1)
-    chosen = jnp.where(column == source, 1.0, 0.0).astype(BF)
-    gated = jnp.dot(chosen, gated, preferred_element_type=F32).astype(BF)
+    halves = []
+    for half in (0, 1):
+        chunk = 4 * lax.div(i, 2 * groups) + 2 * (piece & 1) + half
+        row = (chunk * 11) >> 5
+        source = ((chunk - 3 * row) * groups + group) * packed + row
+        chosen = jnp.where(column == source, 1.0, 0.0).astype(BF)
+        halves.append(jnp.dot(chosen, chunks, preferred_element_type=F32))
+    gated = jnp.concatenate(halves, axis=1).astype(BF)
     branch = jnp.dot(gated, weight_ref[b], preferred_element_type=F32)
     one, two, three = (branch[k * 2 * groups : (k + 1) * 2 * groups] for k in range(3))
     first = jnp.concatenate([one, two[:, :LANES]], axis=1)

time: 120 us -> 120 us (level)
  no operation moved by 1% of the time
where the time goes in v10:
time: 120 us
  blocking collectives  95.6 us (80%)
  starting transfers between devices  15 us (12%)
  Pallas kernels  3.69 us (3%)
  waiting for transfers between devices  1.9 us (2%)
  other arithmetic  1.81 us (2%)
    all_to_all x7, blocking collectives, exchange(): lax.all_to_all(parts, axis, 0, 0, tiled=True, axis_index_groups=[list(ORD...  95.6 us
    all_to_all x1, starting transfers between devices, exchange(): lax.all_to_all(parts, axis, 0, 0, tiled=True, axis_index_groups=[list(ORD...  15 us
  transfers between devices with their start and end apart: 1, of which 1 were waited for; matrix products, arithmetic and copies ran while one was open for 1% of the time, Pallas kernels for 0%

profile of v10, /device:TPU:1, one launch (start us, length us, event | category | flops | bytes accessed | tf_op | source)
XLA Modules:
  0.0 119.6 jit_solution(3187792192406798888)
XLA Ops:
  0.6 0.0 copy-start.10
  0.6 0.7 copy-done.10
  1.3 0.0 copy-start.2
  1.4 0.0 copy-start.3
  1.4 0.0 copy-start.4
  1.4 0.0 copy-start.5
  1.4 0.0 copy-start.6
  1.4 0.0 copy-start.9
  1.4 0.0 copy-start
  1.4 0.0 copy-start.7
  1.4 0.0 copy-start.8
  1.5 23.1 %all_to_all.40.pieces_ref = bf16[32,2,384]{2,1,0:T(2,128)(2,1)S(1)} all-to-all(bf16[32,2,384]{2,1,0:T(2,128)(2,1)S(1)} %hold.1), channel_id=1, replica_groups={{272,256,304,288,336,320,368,352,400,384,432,416,464,448,496,480,16,0,4..., dimensions={0} | all-to-all | bytes 98304 | tf_op jit(solution)/shard_map/all_to_all | solution.py:32
  24.6 0.0 copy-done.2
  24.6 0.0 copy-done.3
  24.6 0.0 copy-done.4
  24.6 0.0 copy-done.5
  24.6 0.0 copy-done.6
  24.6 0.0 copy-done.9
  24.6 0.0 copy-start.1
  24.6 0.4 project.2
  25.1 10.8 %all_to_all.41.parts_ref = bf16[16,8,768]{2,1,0:T(8,128)(2,1)S(1)} all-to-all(bf16[16,8,768]{2,1,0:T(8,128)(2,1)S(1)} %project.2), channel_id=1, replica_groups={{10,11,12,13,14,15,0,1,2,3,4,5,6,7,8,9},{26,27,28,29,30,31,16,17,18,19,..., dimensions={0} | all-to-all | bytes 393216 | tf_op jit(solution)/shard_map/all_to_all | solution.py:32
  35.9 0.0 copy-done
  35.9 0.0 copy-done.7
  35.9 0.0 copy-done.8
  35.9 0.4 step.2
  36.3 8.8 %all_to_all.42.gated_ref = bf16[16,4,384]{2,1,0:T(4,128)(2,1)S(1)} all-to-all(bf16[16,4,384]{2,1,0:T(4,128)(2,1)S(1)} %get-tuple-element.21), channel_id=1, replica_groups={{10,11,12,13,14,15,0,1,2,3,4,5,6,7,8,9},{26,27,28,29,30,31,16,17,18,19,..., dimensions={0} | all-to-all | bytes 98304 | tf_op jit(solution)/shard_map/all_to_all | solution.py:32
  45.2 0.0 copy-done.1
  45.2 0.4 readback.2
  45.6 18.2 %all_to_all.43 = bf16[32,2,384]{2,1,0:T(2,128)(2,1)S(1)} all-to-all(bf16[32,2,384]{2,1,0:T(2,128)(2,1)S(1)} %readback.2), channel_id=1, replica_groups={{272,256,304,288,336,320,368,352,400,384,432,416,464,448,496,480,16,0,4..., dimensions={0} | all-to-all | bytes 98304 | tf_op jit(solution)/shard_map/all_to_all | solution.py:32
  63.7 0.1 convert_reduce_fusion
  63.8 15.5 %all_to_all.44.pieces_ref = bf16[32,2,384]{2,1,0:T(2,128)(2,1)S(1)} all-to-all(bf16[32,2,384]{2,1,0:T(2,128)(2,1)S(1)} %broadcast_in_dim.2), channel_id=1, replica_groups={{272,256,304,288,336,320,368,352,400,384,432,416,464,448,496,480,16,0,4..., dimensions={0} | all-to-all | bytes 98304 | tf_op jit(solution)/shard_map/all_to_all | solution.py:32
  79.3 0.4 project.3
  79.7 10.3 %all_to_all.45.parts_ref = bf16[16,8,768]{2,1,0:T(8,128)(2,1)S(1)} all-to-all(bf16[16,8,768]{2,1,0:T(8,128)(2,1)S(1)} %project.3), channel_id=1, replica_groups={{10,11,12,13,14,15,0,1,2,3,4,5,6,7,8,9},{26,27,28,29,30,31,16,17,18,19,..., dimensions={0} | all-to-all | bytes 393216 | tf_op jit(solution)/shard_map/all_to_all | solution.py:32
  90.1 0.4 step.3
  90.5 8.9 %all_to_all.46.gated_ref = bf16[16,4,384]{2,1,0:T(4,128)(2,1)S(1)} all-to-all(bf16[16,4,384]{2,1,0:T(4,128)(2,1)S(1)} %get-tuple-element.22), channel_id=1, replica_groups={{10,11,12,13,14,15,0,1,2,3,4,5,6,7,8,9},{26,27,28,29,30,31,16,17,18,19,..., dimensions={0} | all-to-all | bytes 98304 | tf_op jit(solution)/shard_map/all_to_all | solution.py:32
  99.4 1.0 readback.3
  100.3 15.0 %all-to-all-start.7 = ((bf16[32,2,384]{2,1,0:T(2,128)(2,1)}), bf16[32,2,384]{2,1,0:T(2,128)(2,1)S(1)}, u32[]{:S(2)}, u32[]{:S(2)}) async-start(bf16[32,2,384]{2,1,0:T(2,128)(2,1)} %readback.3), calls=%async_computation.7 | async-start | bytes 98304 | tf_op jit(solution)/shard_map/all_to_all | solution.py:32
  115.3 0.5 multiply_add_fusion.1
  115.8 1.2 %pad_maximum_fusion = f32[2,6,128,256]{3,2,1,0:T(8,128)} fusion(f32[1,6,128,256]{3,2,1,0:T(8,128)S(1)} %get-tuple-element.37, f32[1,6,128,256]{3,2,1,0:T(8,128)S(1)} %get-tuple-element.36), kind=kLoop, calls=%fused_computation | loop fusion | flops 393216 | bytes 3145728 | tf_op jit(solution)/shard_map/stack | solution.py:271
  117.1 1.9 %all-to-all-done.7.heads_ref = bf16[32,2,384]{2,1,0:T(2,128)(2,1)S(1)} async-done(((bf16[32,2,384]{2,1,0:T(2,128)(2,1)}), bf16[32,2,384]{2,1,0:T(2,128)(2,1)S(1)}, u32[]{:S(2)}, u32[]{:S(2)}) %all-to-all-start.7) | async-done | bytes 49184 | tf_op jit(solution)/shard_map/all_to_all | solution.py:32
  119.0 0.6 finish.1
  (4 shorter events, 0.1 us)
Async XLA Ops:
  0.6 0.7 copy-start.10
  1.3 23.3 %copy-start.2 = (bf16[2,256,256]{2,1,0:T(8,128)(2,1)S(1)}, bf16[2,256,256]{2,1,0:T(8,128)(2,1)}, u32[]{:S(2)}) copy-start(bf16[2,256,256]{2,1,0:T(8,128)(2,1)} %refs_3_.3) | copy-start | bytes 786436
  1.4 23.2 %copy-start.3 = (bf16[2,256,256]{2,1,0:T(8,128)(2,1)S(1)}, bf16[2,256,256]{2,1,0:T(8,128)(2,1)}, u32[]{:S(2)}) copy-start(bf16[2,256,256]{2,1,0:T(8,128)(2,1)} %refs_4_.3) | copy-start | bytes 786436
  1.4 23.2 %copy-start.4 = (bf16[2,256,128]{2,1,0:T(8,128)(2,1)S(1)}, bf16[2,256,128]{2,1,0:T(8,128)(2,1)}, u32[]{:S(2)}) copy-start(bf16[2,256,128]{2,1,0:T(8,128)(2,1)} %refs_0_.3) | copy-start | bytes 393220
  1.4 23.2 %copy-start.5 = (bf16[2,256,128]{2,1,0:T(8,128)(2,1)S(1)}, bf16[2,256,128]{2,1,0:T(8,128)(2,1)}, u32[]{:S(2)}) copy-start(bf16[2,256,128]{2,1,0:T(8,128)(2,1)} %refs_1_.3) | copy-start | bytes 393220
  1.4 23.2 %copy-start.6 = (bf16[2,256,128]{2,1,0:T(8,128)(2,1)S(1)}, bf16[2,256,128]{2,1,0:T(8,128)(2,1)}, u32[]{:S(2)}) copy-start(bf16[2,256,128]{2,1,0:T(8,128)(2,1)} %refs_2_.3) | copy-start | bytes 393220
  1.4 23.2 %copy-start.9 = (bf16[2,256]{1,0:T(2,128)(2,1)S(1)}, bf16[2,256]{1,0:T(2,128)(2,1)}, u32[]{:S(2)}) copy-start(bf16[2,256]{1,0:T(2,128)(2,1)} %gain_ref.3) | copy-start | bytes 3076
  1.4 34.5 %copy-start = (f32[2,6,128,256]{3,2,1,0:T(8,128)S(1)}, f32[2,6,128,256]{3,2,1,0:T(8,128)}, u32[]{:S(2)}) copy-start(f32[2,6,128,256]{3,2,1,0:T(8,128)} %state_ref.3) | copy-start | bytes 4718596
  1.4 34.5 %copy-start.7 = (f32[2,6,128]{2,0,1:T(2,128)S(1)}, f32[2,6,128]{2,0,1:T(2,128)}, u32[]{:S(2)}) copy-start(f32[2,6,128]{2,0,1:T(2,128)} %param.17) | copy-start | bytes 18436
  1.4 34.5 %copy-start.8 = (f32[2,128]{1,0:T(2,128)S(1)}, f32[2,128]{1,0:T(2,128)}, u32[]{:S(2)}) copy-start(f32[2,128]{1,0:T(2,128)} %shift_ref.3) | copy-start | bytes 3076
  24.6 20.6 %copy-start.1 = (bf16[2,256,256]{2,1,0:T(8,128)(2,1)S(1)}, bf16[2,256,256]{2,1,0:T(8,128)(2,1)}, u32[]{:S(2)}) copy-start(bf16[2,256,256]{2,1,0:T(8,128)(2,1)} %weight_ref.3) | copy-start | bytes 786436
  100.3 18.6 %all-to-all-start.7 = ((bf16[32,2,384]{2,1,0:T(2,128)(2,1)}), bf16[32,2,384]{2,1,0:T(2,128)(2,1)S(1)}, u32[]{:S(2)}, u32[]{:S(2)}) async-start(bf16[32,2,384]{2,1,0:T(2,128)(2,1)} %readback.3), calls=%async_computation.7 | async-start | bytes 98304 | tf_op jit(solution)/shard_map/all_to_all | solution.py:32

commit v11 on v10

--- a/solution.py
+++ b/solution.py
@@ -264,11 +264,9 @@
         branch = jnp.sum(heads.astype(F32), axis=0)
         stream = (stream.astype(F32) + branch).astype(BF)
         copies = jnp.broadcast_to(stream[None], copies.shape)
-    fresh = [
-        memory_tensor[b] * d[:, :, None] + k[:, :, None] * v[:, None, :]
-        for b, (d, k, v) in enumerate(kept)
-    ]
-    return mixed, jnp.stack(fresh)
+    decays, keys, values = (jnp.stack(both) for both in zip(*kept))
+    fresh = memory_tensor * decays[..., None] + keys[..., None] * values[:, :, None, :]
+    return mixed, fresh
 
 
 def solution(mesh):

time: 120 us -> 120 us (level)
    another operation x1 -> x2, other arithmetic: 1.25 us -> 0.01 us  [shards(): decays, keys, values = (jnp.stack(both) for both in zip(*kept))]
where the time goes in v11:
time: 120 us
  blocking collectives  95.6 us (80%)
  starting transfers between devices  15 us (12%)
  Pallas kernels  3.69 us (3%)
  waiting for transfers between devices  1.98 us (2%)
  other arithmetic  1.72 us (1%)
    all_to_all x7, blocking collectives, exchange(): lax.all_to_all(parts, axis, 0, 0, tiled=True, axis_index_groups=[list(ORD...  95.6 us
    all_to_all x1, starting transfers between devices, exchange(): lax.all_to_all(parts, axis, 0, 0, tiled=True, axis_index_groups=[list(ORD...  15 us
  transfers between devices with their start and end apart: 1, of which 1 were waited for; matrix products, arithmetic and copies ran while one was open for 1% of the time, Pallas kernels for 0%

profile of v11, /device:TPU:1, one launch (start us, length us, event | category | flops | bytes accessed | tf_op | source)
XLA Modules:
  0.0 119.6 jit_solution(9468673000732674459)
XLA Ops:
  0.6 0.0 copy-start.10
  0.6 0.7 copy-done.10
  1.3 0.0 copy-start.2
  1.4 0.0 copy-start.3
  1.4 0.0 copy-start.4
  1.4 0.0 copy-start.5
  1.4 0.0 copy-start.6
  1.4 0.0 copy-start.9
  1.4 0.0 copy-start
  1.4 0.0 copy-start.7
  1.4 0.0 copy-start.8
  1.5 23.1 %all_to_all.40.pieces_ref = bf16[32,2,384]{2,1,0:T(2,128)(2,1)S(1)} all-to-all(bf16[32,2,384]{2,1,0:T(2,128)(2,1)S(1)} %hold.1), channel_id=1, replica_groups={{272,256,304,288,336,320,368,352,400,384,432,416,464,448,496,480,16,0,4..., dimensions={0} | all-to-all | bytes 98304 | tf_op jit(solution)/shard_map/all_to_all | solution.py:32
  24.6 0.0 copy-done.2
  24.6 0.0 copy-done.3
  24.6 0.0 copy-done.4
  24.6 0.0 copy-done.5
  24.6 0.0 copy-done.6
  24.6 0.0 copy-done.9
  24.6 0.0 copy-start.1
  24.6 0.4 project.2
  25.1 10.8 %all_to_all.41.parts_ref = bf16[16,8,768]{2,1,0:T(8,128)(2,1)S(1)} all-to-all(bf16[16,8,768]{2,1,0:T(8,128)(2,1)S(1)} %project.2), channel_id=1, replica_groups={{10,11,12,13,14,15,0,1,2,3,4,5,6,7,8,9},{26,27,28,29,30,31,16,17,18,19,..., dimensions={0} | all-to-all | bytes 393216 | tf_op jit(solution)/shard_map/all_to_all | solution.py:32
  35.9 0.0 copy-done
  35.9 0.0 copy-done.7
  35.9 0.0 copy-done.8
  35.9 0.4 step.2
  36.3 8.8 %all_to_all.42.gated_ref = bf16[16,4,384]{2,1,0:T(4,128)(2,1)S(1)} all-to-all(bf16[16,4,384]{2,1,0:T(4,128)(2,1)S(1)} %get-tuple-element.21), channel_id=1, replica_groups={{10,11,12,13,14,15,0,1,2,3,4,5,6,7,8,9},{26,27,28,29,30,31,16,17,18,19,..., dimensions={0} | all-to-all | bytes 98304 | tf_op jit(solution)/shard_map/all_to_all | solution.py:32
  45.2 0.0 copy-done.1
  45.2 0.4 readback.2
  45.6 18.2 %all_to_all.43 = bf16[32,2,384]{2,1,0:T(2,128)(2,1)S(1)} all-to-all(bf16[32,2,384]{2,1,0:T(2,128)(2,1)S(1)} %readback.2), channel_id=1, replica_groups={{272,256,304,288,336,320,368,352,400,384,432,416,464,448,496,480,16,0,4..., dimensions={0} | all-to-all | bytes 98304 | tf_op jit(solution)/shard_map/all_to_all | solution.py:32
  63.7 0.1 convert_reduce_fusion
  63.8 15.5 %all_to_all.44.pieces_ref = bf16[32,2,384]{2,1,0:T(2,128)(2,1)S(1)} all-to-all(bf16[32,2,384]{2,1,0:T(2,128)(2,1)S(1)} %broadcast_in_dim.2), channel_id=1, replica_groups={{272,256,304,288,336,320,368,352,400,384,432,416,464,448,496,480,16,0,4..., dimensions={0} | all-to-all | bytes 98304 | tf_op jit(solution)/shard_map/all_to_all | solution.py:32
  79.3 0.4 project.3
  79.7 10.3 %all_to_all.45.parts_ref = bf16[16,8,768]{2,1,0:T(8,128)(2,1)S(1)} all-to-all(bf16[16,8,768]{2,1,0:T(8,128)(2,1)S(1)} %project.3), channel_id=1, replica_groups={{10,11,12,13,14,15,0,1,2,3,4,5,6,7,8,9},{26,27,28,29,30,31,16,17,18,19,..., dimensions={0} | all-to-all | bytes 393216 | tf_op jit(solution)/shard_map/all_to_all | solution.py:32
  90.1 0.4 step.3
  90.5 8.9 %all_to_all.46.gated_ref = bf16[16,4,384]{2,1,0:T(4,128)(2,1)S(1)} all-to-all(bf16[16,4,384]{2,1,0:T(4,128)(2,1)S(1)} %get-tuple-element.22), channel_id=1, replica_groups={{10,11,12,13,14,15,0,1,2,3,4,5,6,7,8,9},{26,27,28,29,30,31,16,17,18,19,..., dimensions={0} | all-to-all | bytes 98304 | tf_op jit(solution)/shard_map/all_to_all | solution.py:32
  99.4 1.0 readback.3
  100.3 15.0 %all-to-all-start.7 = ((bf16[32,2,384]{2,1,0:T(2,128)(2,1)}), bf16[32,2,384]{2,1,0:T(2,128)(2,1)S(1)}, u32[]{:S(2)}, u32[]{:S(2)}) async-start(bf16[32,2,384]{2,1,0:T(2,128)(2,1)} %readback.3), calls=%async_computation.7 | async-start | bytes 98304 | tf_op jit(solution)/shard_map/all_to_all | solution.py:32
  115.3 1.6 %multiply_add_fusion = f32[2,6,128,256]{3,2,1,0:T(8,128)} fusion(f32[2,6,128,256]{3,2,1,0:T(8,128)S(1)} %copy-done, f32[2,6,256]{2,1,0:T(8,128)S(1)} %pad_maximum_fusion, f32[2,6,128]{2,1,0:T(8,128)S(1)} %get-tuple-element.37, f32[2,6,128]{2,1,0:T(8,128)S(1)} %get-tuple-element.36), kind=kLoop, calls=%fused_computation | loop fusion | flops 1179648 | bytes 3170304 | tf_op jit(solution)/shard_map/add | solution.py:268
  117.0 2.0 %all-to-all-done.7.heads_ref = bf16[32,2,384]{2,1,0:T(2,128)(2,1)S(1)} async-done(((bf16[32,2,384]{2,1,0:T(2,128)(2,1)}), bf16[32,2,384]{2,1,0:T(2,128)(2,1)S(1)}, u32[]{:S(2)}, u32[]{:S(2)}) %all-to-all-start.7) | async-done | bytes 49184 | tf_op jit(solution)/shard_map/all_to_all | solution.py:32
  119.0 0.6 finish.1
  (6 shorter events, 0.1 us)
Async XLA Ops:
  0.6 0.7 copy-start.10
  1.3 23.3 %copy-start.2 = (bf16[2,256,256]{2,1,0:T(8,128)(2,1)S(1)}, bf16[2,256,256]{2,1,0:T(8,128)(2,1)}, u32[]{:S(2)}) copy-start(bf16[2,256,256]{2,1,0:T(8,128)(2,1)} %refs_3_.3) | copy-start | bytes 786436
  1.4 23.2 %copy-start.3 = (bf16[2,256,256]{2,1,0:T(8,128)(2,1)S(1)}, bf16[2,256,256]{2,1,0:T(8,128)(2,1)}, u32[]{:S(2)}) copy-start(bf16[2,256,256]{2,1,0:T(8,128)(2,1)} %refs_4_.3) | copy-start | bytes 786436
  1.4 23.2 %copy-start.4 = (bf16[2,256,128]{2,1,0:T(8,128)(2,1)S(1)}, bf16[2,256,128]{2,1,0:T(8,128)(2,1)}, u32[]{:S(2)}) copy-start(bf16[2,256,128]{2,1,0:T(8,128)(2,1)} %refs_0_.3) | copy-start | bytes 393220
  1.4 23.2 %copy-start.5 = (bf16[2,256,128]{2,1,0:T(8,128)(2,1)S(1)}, bf16[2,256,128]{2,1,0:T(8,128)(2,1)}, u32[]{:S(2)}) copy-start(bf16[2,256,128]{2,1,0:T(8,128)(2,1)} %refs_1_.3) | copy-start | bytes 393220
  1.4 23.2 %copy-start.6 = (bf16[2,256,128]{2,1,0:T(8,128)(2,1)S(1)}, bf16[2,256,128]{2,1,0:T(8,128)(2,1)}, u32[]{:S(2)}) copy-start(bf16[2,256,128]{2,1,0:T(8,128)(2,1)} %refs_2_.3) | copy-start | bytes 393220
  1.4 23.2 %copy-start.9 = (bf16[2,256]{1,0:T(2,128)(2,1)S(1)}, bf16[2,256]{1,0:T(2,128)(2,1)}, u32[]{:S(2)}) copy-start(bf16[2,256]{1,0:T(2,128)(2,1)} %gain_ref.3) | copy-start | bytes 3076
  1.4 34.5 %copy-start = (f32[2,6,128,256]{3,2,1,0:T(8,128)S(1)}, f32[2,6,128,256]{3,2,1,0:T(8,128)}, u32[]{:S(2)}) copy-start(f32[2,6,128,256]{3,2,1,0:T(8,128)} %state_ref.3) | copy-start | bytes 4718596
  1.4 34.5 %copy-start.7 = (f32[2,6,128]{2,0,1:T(2,128)S(1)}, f32[2,6,128]{2,0,1:T(2,128)}, u32[]{:S(2)}) copy-start(f32[2,6,128]{2,0,1:T(2,128)} %param.17) | copy-start | bytes 18436
  1.4 34.5 %copy-start.8 = (f32[2,128]{1,0:T(2,128)S(1)}, f32[2,128]{1,0:T(2,128)}, u32[]{:S(2)}) copy-start(f32[2,128]{1,0:T(2,128)} %shift_ref.3) | copy-start | bytes 3076
  24.6 20.6 %copy-start.1 = (bf16[2,256,256]{2,1,0:T(8,128)(2,1)S(1)}, bf16[2,256,256]{2,1,0:T(8,128)(2,1)}, u32[]{:S(2)}) copy-start(bf16[2,256,256]{2,1,0:T(8,128)(2,1)} %weight_ref.3) | copy-start | bytes 786436
  100.3 18.6 %all-to-all-start.7 = ((bf16[32,2,384]{2,1,0:T(2,128)(2,1)}), bf16[32,2,384]{2,1,0:T(2,128)(2,1)S(1)}, u32[]{:S(2)}, u32[]{:S(2)}) async-start(bf16[32,2,384]{2,1,0:T(2,128)(2,1)} %readback.3), calls=%async_computation.7 | async-start | bytes 98304 | tf_op jit(solution)/shard_map/all_to_all | solution.py:32

commit v12 on v10

--- a/solution.py
+++ b/solution.py
@@ -24,8 +24,8 @@
     "z": tuple((8 + k) % 16 for k in range(16)),
     DP: tuple((10 + k) % 16 for k in range(16)),
 }
-ORDER[TP] = tuple(2 * z + c for z in ORDER["z"] for c in (1, 0))
-SEQ_OF_ROW = (3, 0, 4, 1, 5, 2)
+ORDER[TP] = tuple(2 * z + c for z in ORDER["z"] for c in (0, 1))
+SEQ_OF_ROW = (0, 3, 1, 4, 2, 5)
 
 
 def exchange(parts, axis):

time: 120 us -> 124 us (1.033)
  blocking collectives: 95.6 us -> 99.3 us
    all_to_all x7, blocking collectives: 95.6 us -> 99.3 us  [exchange(): lax.all_to_all(parts, axis, 0, 0, tiled=True, axis_index_groups=[list(ORD...]
where the time goes in v12:
time: 124 us
  blocking collectives  99.3 us (80%)
  starting transfers between devices  15.7 us (13%)
  Pallas kernels  3.69 us (3%)
  waiting for transfers between devices  1.93 us (2%)
  other arithmetic  1.81 us (1%)
    all_to_all x7, blocking collectives, exchange(): lax.all_to_all(parts, axis, 0, 0, tiled=True, axis_index_groups=[list(ORD...  99.3 us
    all_to_all x1, starting transfers between devices, exchange(): lax.all_to_all(parts, axis, 0, 0, tiled=True, axis_index_groups=[list(ORD...  15.7 us
  transfers between devices with their start and end apart: 1, of which 1 were waited for; matrix products, arithmetic and copies ran while one was open for 1% of the time, Pallas kernels for 0%

profile of v12, /device:TPU:1, one launch (start us, length us, event | category | flops | bytes accessed | tf_op | source)
XLA Modules:
  0.0 124.0 jit_solution(16760215737332493795)
XLA Ops:
  0.6 0.0 copy-start.10
  0.6 0.7 copy-done.10
  1.3 0.0 copy-start.2
  1.4 0.0 copy-start.3
  1.4 0.0 copy-start.4
  1.4 0.0 copy-start.5
  1.4 0.0 copy-start.6
  1.4 0.0 copy-start.9
  1.4 0.0 copy-start
  1.4 0.0 copy-start.7
  1.4 0.0 copy-start.8
  1.5 23.7 %all_to_all.40.pieces_ref = bf16[32,2,384]{2,1,0:T(2,128)(2,1)S(1)} all-to-all(bf16[32,2,384]{2,1,0:T(2,128)(2,1)S(1)} %hold.1), channel_id=1, replica_groups={{256,272,288,304,320,336,352,368,384,400,416,432,448,464,480,496,0,16,3..., dimensions={0} | all-to-all | bytes 98304 | tf_op jit(solution)/shard_map/all_to_all | solution.py:32
  25.1 0.0 copy-done.2
  25.2 0.0 copy-done.3
  25.2 0.0 copy-done.4
  25.2 0.0 copy-done.5
  25.2 0.0 copy-done.6
  25.2 0.0 copy-done.9
  25.2 0.0 copy-start.1
  25.2 0.4 project.2
  25.6 10.7 %all_to_all.41.parts_ref = bf16[16,8,768]{2,1,0:T(8,128)(2,1)S(1)} all-to-all(bf16[16,8,768]{2,1,0:T(8,128)(2,1)S(1)} %project.2), channel_id=1, replica_groups={{10,11,12,13,14,15,0,1,2,3,4,5,6,7,8,9},{26,27,28,29,30,31,16,17,18,19,..., dimensions={0} | all-to-all | bytes 393216 | tf_op jit(solution)/shard_map/all_to_all | solution.py:32
  36.4 0.0 copy-done
  36.4 0.0 copy-done.7
  36.4 0.0 copy-done.8
  36.4 0.4 step.2
  36.8 9.8 %all_to_all.42.gated_ref = bf16[16,4,384]{2,1,0:T(4,128)(2,1)S(1)} all-to-all(bf16[16,4,384]{2,1,0:T(4,128)(2,1)S(1)} %get-tuple-element.21), channel_id=1, replica_groups={{10,11,12,13,14,15,0,1,2,3,4,5,6,7,8,9},{26,27,28,29,30,31,16,17,18,19,..., dimensions={0} | all-to-all | bytes 98304 | tf_op jit(solution)/shard_map/all_to_all | solution.py:32
  46.6 0.0 copy-done.1
  46.6 0.4 readback.2
  47.0 18.5 %all_to_all.43 = bf16[32,2,384]{2,1,0:T(2,128)(2,1)S(1)} all-to-all(bf16[32,2,384]{2,1,0:T(2,128)(2,1)S(1)} %readback.2), channel_id=1, replica_groups={{256,272,288,304,320,336,352,368,384,400,416,432,448,464,480,496,0,16,3..., dimensions={0} | all-to-all | bytes 98304 | tf_op jit(solution)/shard_map/all_to_all | solution.py:32
  65.5 0.1 convert_reduce_fusion
  65.6 16.6 %all_to_all.44.pieces_ref = bf16[32,2,384]{2,1,0:T(2,128)(2,1)S(1)} all-to-all(bf16[32,2,384]{2,1,0:T(2,128)(2,1)S(1)} %broadcast_in_dim.2), channel_id=1, replica_groups={{256,272,288,304,320,336,352,368,384,400,416,432,448,464,480,496,0,16,3..., dimensions={0} | all-to-all | bytes 98304 | tf_op jit(solution)/shard_map/all_to_all | solution.py:32
  82.2 0.4 project.3
  82.6 10.2 %all_to_all.45.parts_ref = bf16[16,8,768]{2,1,0:T(8,128)(2,1)S(1)} all-to-all(bf16[16,8,768]{2,1,0:T(8,128)(2,1)S(1)} %project.3), channel_id=1, replica_groups={{10,11,12,13,14,15,0,1,2,3,4,5,6,7,8,9},{26,27,28,29,30,31,16,17,18,19,..., dimensions={0} | all-to-all | bytes 393216 | tf_op jit(solution)/shard_map/all_to_all | solution.py:32
  92.8 0.4 step.3
  93.2 9.8 %all_to_all.46.gated_ref = bf16[16,4,384]{2,1,0:T(4,128)(2,1)S(1)} all-to-all(bf16[16,4,384]{2,1,0:T(4,128)(2,1)S(1)} %get-tuple-element.22), channel_id=1, replica_groups={{10,11,12,13,14,15,0,1,2,3,4,5,6,7,8,9},{26,27,28,29,30,31,16,17,18,19,..., dimensions={0} | all-to-all | bytes 98304 | tf_op jit(solution)/shard_map/all_to_all | solution.py:32
  103.0 1.0 readback.3
  104.0 15.7 %all-to-all-start.7 = ((bf16[32,2,384]{2,1,0:T(2,128)(2,1)}), bf16[32,2,384]{2,1,0:T(2,128)(2,1)S(1)}, u32[]{:S(2)}, u32[]{:S(2)}) async-start(bf16[32,2,384]{2,1,0:T(2,128)(2,1)} %readback.3), calls=%async_computation.7 | async-start | bytes 98304 | tf_op jit(solution)/shard_map/all_to_all | solution.py:32
  119.7 0.5 multiply_add_fusion.1
  120.2 1.2 %pad_maximum_fusion = f32[2,6,128,256]{3,2,1,0:T(8,128)} fusion(f32[1,6,128,256]{3,2,1,0:T(8,128)S(1)} %get-tuple-element.37, f32[1,6,128,256]{3,2,1,0:T(8,128)S(1)} %get-tuple-element.36), kind=kLoop, calls=%fused_computation | loop fusion | flops 393216 | bytes 3145728 | tf_op jit(solution)/shard_map/stack | solution.py:271
  121.4 1.9 %all-to-all-done.7.heads_ref = bf16[32,2,384]{2,1,0:T(2,128)(2,1)S(1)} async-done(((bf16[32,2,384]{2,1,0:T(2,128)(2,1)}), bf16[32,2,384]{2,1,0:T(2,128)(2,1)S(1)}, u32[]{:S(2)}, u32[]{:S(2)}) %all-to-all-start.7) | async-done | bytes 49184 | tf_op jit(solution)/shard_map/all_to_all | solution.py:32
  123.4 0.6 finish.1
  (4 shorter events, 0.1 us)
Async XLA Ops:
  0.6 0.7 copy-start.10
  1.3 23.8 %copy-start.2 = (bf16[2,256,256]{2,1,0:T(8,128)(2,1)S(1)}, bf16[2,256,256]{2,1,0:T(8,128)(2,1)}, u32[]{:S(2)}) copy-start(bf16[2,256,256]{2,1,0:T(8,128)(2,1)} %refs_3_.3) | copy-start | bytes 786436
  1.4 23.8 %copy-start.3 = (bf16[2,256,256]{2,1,0:T(8,128)(2,1)S(1)}, bf16[2,256,256]{2,1,0:T(8,128)(2,1)}, u32[]{:S(2)}) copy-start(bf16[2,256,256]{2,1,0:T(8,128)(2,1)} %refs_4_.3) | copy-start | bytes 786436
  1.4 23.8 %copy-start.4 = (bf16[2,256,128]{2,1,0:T(8,128)(2,1)S(1)}, bf16[2,256,128]{2,1,0:T(8,128)(2,1)}, u32[]{:S(2)}) copy-start(bf16[2,256,128]{2,1,0:T(8,128)(2,1)} %refs_0_.3) | copy-start | bytes 393220
  1.4 23.8 %copy-start.5 = (bf16[2,256,128]{2,1,0:T(8,128)(2,1)S(1)}, bf16[2,256,128]{2,1,0:T(8,128)(2,1)}, u32[]{:S(2)}) copy-start(bf16[2,256,128]{2,1,0:T(8,128)(2,1)} %refs_1_.3) | copy-start | bytes 393220
  1.4 23.8 %copy-start.6 = (bf16[2,256,128]{2,1,0:T(8,128)(2,1)S(1)}, bf16[2,256,128]{2,1,0:T(8,128)(2,1)}, u32[]{:S(2)}) copy-start(bf16[2,256,128]{2,1,0:T(8,128)(2,1)} %refs_2_.3) | copy-start | bytes 393220
  1.4 23.8 %copy-start.9 = (bf16[2,256]{1,0:T(2,128)(2,1)S(1)}, bf16[2,256]{1,0:T(2,128)(2,1)}, u32[]{:S(2)}) copy-start(bf16[2,256]{1,0:T(2,128)(2,1)} %gain_ref.3) | copy-start | bytes 3076
  1.4 34.9 %copy-start = (f32[2,6,128,256]{3,2,1,0:T(8,128)S(1)}, f32[2,6,128,256]{3,2,1,0:T(8,128)}, u32[]{:S(2)}) copy-start(f32[2,6,128,256]{3,2,1,0:T(8,128)} %state_ref.3) | copy-start | bytes 4718596
  1.4 34.9 %copy-start.7 = (f32[2,6,128]{2,0,1:T(2,128)S(1)}, f32[2,6,128]{2,0,1:T(2,128)}, u32[]{:S(2)}) copy-start(f32[2,6,128]{2,0,1:T(2,128)} %param.17) | copy-start | bytes 18436
  1.4 34.9 %copy-start.8 = (f32[2,128]{1,0:T(2,128)S(1)}, f32[2,128]{1,0:T(2,128)}, u32[]{:S(2)}) copy-start(f32[2,128]{1,0:T(2,128)} %shift_ref.3) | copy-start | bytes 3076
  25.2 21.4 %copy-start.1 = (bf16[2,256,256]{2,1,0:T(8,128)(2,1)S(1)}, bf16[2,256,256]{2,1,0:T(8,128)(2,1)}, u32[]{:S(2)}) copy-start(bf16[2,256,256]{2,1,0:T(8,128)(2,1)} %weight_ref.3) | copy-start | bytes 786436
  104.0 19.4 %all-to-all-start.7 = ((bf16[32,2,384]{2,1,0:T(2,128)(2,1)}), bf16[32,2,384]{2,1,0:T(2,128)(2,1)S(1)}, u32[]{:S(2)}, u32[]{:S(2)}) async-start(bf16[32,2,384]{2,1,0:T(2,128)(2,1)} %readback.3), calls=%async_computation.7 | async-start | bytes 98304 | tf_op jit(solution)/shard_map/all_to_all | solution.py:32
